TPU v7x, 512 devices: a whole 4x4x16 slice. The times are simulated.
512 devices in a mesh: sp: 32 (over z, core), tp: 16 (over y, x).
Axes of the slice: x: 4, y: 4, z: 16, core: 2. Of those that a mesh axis runs over, the one named last changes fastest.
Arguments:
- residual: bfloat16 [8192, 4096], P('sp', 'tp'), may hold values from -6 to 6
- pool_in: bfloat16 [8192, 2048], P('sp', 'tp'), may hold values from -6 to 6
- docs: int32 [8192], P('sp'), may hold values from 0 to 15, never falling along the last dimension, each value on 1 to 1024 neighbouring positions
- pool_weight: bfloat16 [16, 128, 128], P('tp'), may hold values from -0.5 to 0.5
- pool_gain: float32 [2048], P('tp'), may hold values from 0.1 to 1.9
- out_weight: bfloat16 [2048, 4096], P(None, 'tp'), may hold values from -0.125 to 0.125
- norm_gain: float32 [4096], replicated, may hold values from 0.1 to 1.9
- routes: int32 [8192, 2], P('sp'), may hold values from 0 to 31, all different within a row; in each aligned block of 256 rows (0 to 255, 256 to 511, ...) at most 24 rows name the same one
- route_weights: float32 [8192, 2], P('sp'), may hold values from 0.25 to 1
- w_gate: bfloat16 [32, 4096, 2048], P('sp', None, 'tp'), may hold values from -0.09375 to 0.09375
- w_up: bfloat16 [32, 4096, 2048], P('sp', None, 'tp'), may hold values from -0.09375 to 0.09375
- w_down: bfloat16 [32, 2048, 4096], P('sp', None, 'tp'), may hold values from -0.125 to 0.125
Outputs:
- layer_out: bfloat16 [8192, 4096], P('sp', 'tp')
Inputs may be any that keep to these rules, and one draw needn't show every extreme that they name: `docs`: document numbers never fall along the sequence; each document has at most 1024 positions. `routes`: each token names 2 different experts; among the tokens of one index of sp (aligned blocks of 256 rows) no expert is named more than 24 times, a bound that some block reaches.
All inputs are finite; a program needn't handle non-finite values.
Results may differ from a plain program's by a relative error of at most 0.012.
Values may be sent and summed in bfloat16 or wider, within the bound.
No kernel may reach another device: no remote copies, remote signals or barrier semaphores. Data moves between devices by JAX's collectives and lax.ppermute only.
A program may use at most 64 MiB of HBM per device.

v0:
```python
import jax
import jax.numpy as jnp
import numpy as np
from jax import lax
from jax.experimental import pallas as pl
from jax.experimental.pallas import tpu as pltpu
from jax.sharding import Mesh
from jax.sharding import PartitionSpec as P


TOPK = 2
SP = ("z", "c")
TP = ("y", "x")
PLANE = ("c", "y", "x")
EPS = 1e-06
F32 = jnp.float32
BF16 = jnp.bfloat16
VMEM_BYTES = 20 * 2**20


def blocks_of(shift):
    return [
        [(2 * v + shift + i) % 4 * 4 + (2 * h + shift + j) % 4 for i in (0, 1) for j in (0, 1)]
        for v in (0, 1)
        for h in (0, 1)
    ]


GATHER = [blocks_of(1), blocks_of(0)]
SCATTER = [blocks_of(0), blocks_of(1)]


def both_cores(groups):
    return groups[0] + [[16 + m for m in group] for group in groups[1]]


def group_with(groups, member):
    return next(group for group in groups if member in group)


def tables():
    table = np.zeros((2, 16, 56), np.int32)
    for core in range(2):
        for me in range(16):
            gather, scatter = group_with(GATHER[core], me), group_with(SCATTER[core], me)
            p, q = scatter.index(me), gather.index(me)
            row = []
            for by in range(4):
                row += group_with(GATHER[core], scatter[(p + by) % 4])
            for by in range(4):
                row += group_with(SCATTER[core], gather[(q + by) % 4])
            channels = sum((group_with(GATHER[core], member) for member in scatter), [])
            table[core, me, :54] = row + gather + [p, q] + channels
    return table


FEATURES, HIDDEN, GAINS, IN_SCATTER, IN_GATHER, CHANNELS = 0, 16, 32, 36, 37, 38


def a2a(blocks, groups):
    return lax.all_to_all(blocks, PLANE, 0, 0, tiled=True, axis_index_groups=both_cores(groups))


def turns(cuts, groups):
    got = [cuts[0]]
    for by in range(1, 4):
        pairs = [(g[i], g[(i + by) % 4]) for g in both_cores(groups) for i in range(4)]
        got.append(lax.ppermute(cuts[by], PLANE, pairs))
    return got


def shape(*dims, dtype=BF16):
    return jax.ShapeDtypeStruct(dims, dtype)


def call(kernel, outs, *args, flops, scratch=()):
    single = len(outs) == 1
    moved = sum(a.size * a.dtype.itemsize for a in (*args, *outs))
    vmem = pl.BlockSpec(memory_space=pltpu.VMEM)
    return pl.pallas_call(
        kernel,
        out_shape=outs[0] if single else tuple(outs),
        in_specs=[pl.BlockSpec(memory_space=pltpu.SMEM) if a.dtype == jnp.int32 else vmem for a in args],
        out_specs=vmem if single else (vmem,) * len(outs),
        scratch_shapes=list(scratch),
        compiler_params=pltpu.CompilerParams(vmem_limit_bytes=VMEM_BYTES),
        cost_estimate=pl.CostEstimate(flops=flops, bytes_accessed=moved, transcendentals=0),
    )(*args)


def cut_first(where, gate, up, *outs):
    for by in range(4):
        for i in range(4):
            block = where[FEATURES + 4 * by + i]
            src = pl.ds(pl.multiple_of(block * 256, 256), 256)
            outs[by][pl.ds(256 * i, 256), pl.ds(0, 128)] = gate[src, :]
            outs[by][pl.ds(256 * i, 256), pl.ds(128, 128)] = up[src, :]


def cut_second(where, down, *outs):
    for by in range(4):
        for i in range(4):
            block = where[HIDDEN + 4 * by + i]
            outs[by][pl.ds(128 * i, 128), :] = down[pl.ds(pl.multiple_of(block * 128, 128), 128), :]


def project(where, pooled, weight, residual, out):
    total = residual[...].astype(F32)
    for j in range(4):
        rows = []
        for i in range(4):
            block = where[CHANNELS + 4 * j + i]
            rows.append(weight[pl.ds(pl.multiple_of(block * 128, 128), 128), :])
        part = jnp.concatenate([pooled[j, i] for i in range(4)], axis=1)
        total = total + jnp.dot(part, jnp.concatenate(rows, axis=0), preferred_element_type=F32)
    out[...] = total.astype(BF16)


def gate_up(where, got, gain, w0, w1, w2, w3, out, rows):
    count = got.shape[1]
    ones = jnp.ones((8, 256), BF16)
    tiles = count // 256
    for i in range(tiles):
        tile = pl.ds(256 * i, 256)
        total = jnp.zeros((8, 256), F32)
        for g in range(4):
            value = got[g, tile, :].astype(F32)
            rows[tile, pl.ds(256 * g, 256)] = (value * gain[pl.ds(where[GAINS + g], 1), :]).astype(BF16)
            square = value * value
            high = square.astype(BF16)
            low = (square - high.astype(F32)).astype(BF16)
            for part in (high, low):
                total = total + lax.dot_general(ones, part, (((1,), (1,)), ((), ())), preferred_element_type=F32)
        high = total.astype(BF16)
        low = (total - high.astype(F32)).astype(BF16)
        for j in range(4):
            out[j, pl.ds(count + 2 * i, 1), :] = high[:1]
            out[j, pl.ds(count + 2 * i + 1, 1), :] = low[:1]
    for by, first in enumerate((w0, w1, w2, w3)):
        to = lax.rem(where[IN_SCATTER] + 4 - by, 4)
        out[to, pl.ds(count + 2 * tiles, 8 - 2 * tiles), :] = jnp.zeros((8 - 2 * tiles, 256), BF16)
        for i in range(tiles):
            tile = pl.ds(256 * i, 256)
            out[to, tile, :] = jnp.dot(rows[tile, :], first[...], preferred_element_type=F32).astype(BF16)


def activate(parts, out):
    count = out.shape[1]
    extra = jnp.concatenate([parts[j, pl.ds(count, 8), :].astype(F32) for j in range(4)], axis=0)
    line = lax.broadcasted_iota(jnp.int32, (32, 128), 0) % 8
    for i in range(count // 256):
        tile = pl.ds(256 * i, 256)
        pick = ((line == 2 * i) | (line == 2 * i + 1)).astype(F32)
        total = lax.dot_general(extra, pick, (((0,), (0,)), ((), ())), preferred_element_type=F32)
        scale = lax.rsqrt(total / 4096 + EPS)
        gate = parts[0, tile, pl.ds(0, 128)].astype(F32)
        up = parts[0, tile, pl.ds(128, 128)].astype(F32)
        for j in range(1, 4):
            gate = gate + parts[j, tile, pl.ds(0, 128)].astype(F32)
            up = up + parts[j, tile, pl.ds(128, 128)].astype(F32)
        gate, up = gate * scale, up * scale
        act = (gate * jax.nn.sigmoid(gate) * up).astype(BF16)
        for j in range(4):
            out[j, tile, :] = act


def down_rows(where, acts, w0, w1, w2, w3, out, rows):
    count = acts.shape[1]
    for h in range(4):
        rows[:, pl.ds(128 * h, 128)] = acts[h]
    for by, second in enumerate((w0, w1, w2, w3)):
        to = lax.rem(where[IN_GATHER] + 4 - by, 4)
        for i in range(count // 256):
            tile = pl.ds(256 * i, 256)
            out[to, tile, :] = jnp.dot(rows[tile, :], second[...], preferred_element_type=F32).astype(BF16)


def experts(arrived, first, second, where, gain):
    count = arrived.shape[0]
    got = a2a(jnp.broadcast_to(arrived[None], (4, *arrived.shape)), GATHER)
    part = call(
        gate_up,
        [shape(4, count + 8, 256)],
        where,
        got,
        gain,
        *first,
        flops=2**21 * count,
        scratch=[pltpu.VMEM((count, 1024), BF16)],
    )
    parts = a2a(part, SCATTER)
    acts = a2a(call(activate, [shape(4, count, 128)], parts, flops=2**16 * count), SCATTER)
    part = call(
        down_rows,
        [shape(4, count, 256)],
        where,
        acts,
        *second,
        flops=2**20 * count,
        scratch=[pltpu.VMEM((count, 512), BF16)],
    )
    parts = a2a(part, GATHER)
    return jnp.sum(parts.astype(F32), axis=0).astype(BF16)


def pool(pool_in, docs, pool_weight, pool_gain):
    length, width = pool_in.shape
    sp_index = lax.axis_index(SP)
    group = lax.axis_index(TP)
    size = lax.axis_size(SP)
    reach = 15
    tail = docs[length - 16 :].astype(BF16)
    edge = jnp.concatenate([pool_in[length - reach :], jnp.pad(tail, (0, width - 16))[None]], axis=0)
    prev = lax.ppermute(edge, SP, [(i, i + 1) for i in range(size - 1)])
    extended = jnp.concatenate([prev[:reach], pool_in], axis=0).astype(F32)
    own_docs = docs.astype(F32)
    ext_docs = jnp.concatenate([prev[reach, 1:16].astype(F32), own_docs])
    places = sp_index * length + jnp.arange(length)
    span = 2 ** (1 + group % 4)
    totals = jnp.zeros((length, width), F32)
    counts = jnp.zeros((length,), F32)
    for offset in range(16):
        shifted = extended[reach - offset : reach - offset + length]
        prior = ext_docs[reach - offset : reach - offset + length]
        same = ((places >= offset) & (prior == own_docs) & (offset < span)).astype(F32)
        totals = totals + same[:, None] * shifted
        counts = counts + same
    diff = (totals / counts[:, None] - extended[reach:]).astype(BF16)
    mixed = jnp.dot(diff, pool_weight[0], preferred_element_type=F32)
    return (mixed * pool_gain).astype(BF16)


def split(value):
    high = lax.reduce_precision(value, 8, 7)
    return high.astype(BF16), (value - high).astype(BF16)


def layer(
    residual, pool_in, docs, pool_weight, pool_gain, out_weight, norm_gain, routes, route_weights, w_gate, w_up, w_down
):
    length, cols = residual.shape
    n_exp = lax.axis_size(SP)
    cap = length * TOPK * 3 // (2 * n_exp)
    slots = n_exp * cap
    where = lax.dynamic_slice(
        jnp.asarray(tables()), (lax.axis_index("c"), lax.axis_index(TP), 0), (1, 1, 56)
    ).reshape(56)
    pooled = pool(pool_in, docs, pool_weight, pool_gain)
    ids = routes.reshape(-1)
    onehot = (ids[:, None] == jnp.arange(n_exp)[None, :]).astype(jnp.int32)
    rank = jnp.sum(onehot * (jnp.cumsum(onehot, axis=0) - 1), axis=1)
    place = (ids * cap + rank).reshape(length, TOPK)
    places = jnp.arange(slots)
    take = (place[:, 0][None, :] == places[:, None]) | (place[:, 1][None, :] == places[:, None])
    low = jnp.where(place[:, 0][:, None] == places[None, :], route_weights[:, 0][:, None], 0.0)
    mix = low + jnp.where(place[:, 1][:, None] == places[None, :], route_weights[:, 1][:, None], 0.0)
    mix_high, mix_low = split(mix)

    cuts_first = call(cut_first, [shape(1024, 256)] * 4, where, w_gate[0], w_up[0], flops=2**22)
    cuts_second = call(cut_second, [shape(512, 256)] * 4, where, w_down[0], flops=2**21)

    near = a2a(jnp.broadcast_to(pooled[None], (4, *pooled.shape)), GATHER)
    pooled_all = a2a(jnp.broadcast_to(near[None], (4, *near.shape)), SCATTER)
    updated = call(project, [shape(length, cols)], where, pooled_all, out_weight, residual, flops=2**28)

    send = jnp.dot(take.astype(BF16), updated, preferred_element_type=F32).astype(BF16)
    arrived = lax.all_to_all(send.reshape(n_exp, cap, cols), SP, 0, 0, tiled=True).reshape(slots, cols)
    first = turns(cuts_first, SCATTER)
    second = turns(cuts_second, GATHER)
    made = experts(arrived, first, second, where, norm_gain.reshape(16, 256))
    back = lax.all_to_all(made.reshape(n_exp, cap, cols), SP, 0, 0, tiled=True).reshape(slots, cols)
    summed = jnp.dot(mix_high, back, preferred_element_type=F32) + jnp.dot(
        mix_low, back, preferred_element_type=F32
    )
    return (updated.astype(F32) + summed).astype(BF16)


def solution(mesh):
    torus = Mesh(mesh.devices.reshape(-1, 2, 4, 4), ("z", *PLANE))
    in_specs = (
        P(SP, TP),
        P(SP, TP),
        P(SP),
        P(TP, None, None),
        P(TP),
        P(None, TP),
        P(),
        P(SP, None),
        P(SP, None),
        P(SP, None, TP),
        P(SP, None, TP),
        P(SP, None, TP),
    )
    return jax.shard_map(layer, mesh=torus, in_specs=in_specs, out_specs=P(SP, TP), check_vma=False)
```

profile of v0, /device:TPU:1, one launch (start us, length us, event | category | flops | bytes accessed | tf_op | source)
XLA Modules:
  0.0 213.4 jit_solution(15329443900865132923)
XLA Ops:
  1.5 4.9 %collective-permute-start = (bf16[16,128]{1,0:T(8,128)(2,1)S(1)}, bf16[16,128]{1,0:T(8,128)(2,1)S(1)}, u32[]{:S(2)}, u32[]{:S(2)}) collective-permute-start(bf16[16,128]{1,0:T(8,128)(2,1)S(1)} %pad_maximum_fusion), channel_id=1, source_target_pairs={{0,16},{16,32},{32,48},{48,64},{64,80},{80,96},{96,112},{112,128},... | collective-permute-start | bytes 12296 | tf_op jit(solution)/shard_map/ppermute | solution.py:214
  7.7 2.6 %collective-permute-done = bf16[16,128]{1,0:T(8,128)(2,1)S(1)} collective-permute-done((bf16[16,128]{1,0:T(8,128)(2,1)S(1)}, bf16[16,128]{1,0:T(8,128)(2,1)S(1)}, u32[]{:S(2)}, u32[]{:S(2)}) %collective-permute-start) | collective-permute-done | bytes 4128 | tf_op jit(solution)/shard_map/ppermute | solution.py:214
  12.1 1.7 fusion.2
  14.6 3.4 %all-to-all-start = ((bf16[4,256,128]{2,1,0:T(8,128)(2,1)}), bf16[4,256,128]{2,1,0:T(8,128)(2,1)S(1)}, u32[]{:S(2)}, u32[]{:S(2)}) async-start(bf16[4,256,128]{2,1,0:T(8,128)(2,1)} %broadcast_in_dim.33), calls=%async_computation | async-start | bytes 524288 | tf_op jit(solution)/shard_map/all_to_all | solution.py:61
  18.0 1.2 reduce-window.6
  19.2 3.0 %all-to-all-done = bf16[4,256,128]{2,1,0:T(8,128)(2,1)S(1)} async-done(((bf16[4,256,128]{2,1,0:T(8,128)(2,1)}), bf16[4,256,128]{2,1,0:T(8,128)(2,1)S(1)}, u32[]{:S(2)}, u32[]{:S(2)}) %all-to-all-start) | async-done | bytes 262176 | tf_op jit(solution)/shard_map/all_to_all | solution.py:61
  22.2 1.2 broadcast_in_dim.34
  23.4 6.2 %all-to-all-start.1 = ((bf16[4,4,256,128]{3,2,1,0:T(8,128)(2,1)}), bf16[4,4,256,128]{3,2,1,0:T(8,128)(2,1)S(1)}, u32[]{:S(2)}, u32[]{:S(2)}) async-start(bf16[4,4,256,128]{3,2,1,0:T(8,128)(2,1)} %broadcast_in_dim.34), calls=%async_computation.1 | async-start | bytes 2097152 | tf_op jit(solution)/shard_map/all_to_all | solution.py:61
  30.9 5.9 %all-to-all-done.1.pooled = bf16[4,4,256,128]{3,2,1,0:T(8,128)(2,1)S(1)} async-done(((bf16[4,4,256,128]{3,2,1,0:T(8,128)(2,1)}), bf16[4,4,256,128]{3,2,1,0:T(8,128)(2,1)S(1)}, u32[]{:S(2)}, u32[]{:S(2)}) %all-to-all-start.1) | async-done | bytes 1048608 | tf_op jit(solution)/shard_map/all_to_all | solution.py:61
  38.1 46.0 %all_to_all.40 = bf16[32,24,256]{2,1,0:T(8,128)(2,1)S(1)} all-to-all(bf16[32,24,256]{2,1,0:T(8,128)(2,1)S(1)} %bitcast.48), channel_id=1, replica_groups=mesh['z'=16,'c'=2,'y'=4,'x'=4] {'z','c'}, dimensions={0} | all-to-all | bytes 786432 | tf_op jit(solution)/shard_map/all_to_all | solution.py:267
  84.1 1.3 broadcast_in_dim.41
  85.3 3.7 %all-to-all-start.3 = ((bf16[4,768,256]{2,1,0:T(8,128)(2,1)}), bf16[4,768,256]{2,1,0:T(8,128)(2,1)S(1)}, u32[]{:S(2)}, u32[]{:S(2)}) async-start(bf16[4,768,256]{2,1,0:T(8,128)(2,1)} %broadcast_in_dim.41), calls=%async_computation.3 | async-start | bytes 3145728 | tf_op jit(solution)/shard_map/all_to_all | solution.py:61
  89.1 1.2 copy-done.3
  90.3 2.0 shard_map.128
  92.3 6.1 %collective-permute-start.1 = (bf16[1024,256]{1,0:T(8,128)(2,1)}, bf16[1024,256]{1,0:T(8,128)(2,1)S(1)}, u32[]{:S(2)}, u32[]{:S(2)}) collective-permute-start(bf16[1024,256]{1,0:T(8,128)(2,1)} %get-tuple-element.14), channel_id=1, source_target_pairs={{0,1},{1,4},{4,5},{5,0},{2,3},{3,6},{6,7},{7,2},{8,9},{9,12},{12,1... | collective-permute-start | bytes 1572872 | tf_op jit(solution)/shard_map/ppermute | solution.py:68
  98.4 2.2 %collective-permute-start.2 = (bf16[1024,256]{1,0:T(8,128)(2,1)}, bf16[1024,256]{1,0:T(8,128)(2,1)}, u32[]{:S(2)}, u32[]{:S(2)}) collective-permute-start(bf16[1024,256]{1,0:T(8,128)(2,1)} %get-tuple-element.15), channel_id=1, source_target_pairs={{0,4},{1,5},{4,0},{5,1},{2,6},{3,7},{6,2},{7,3},{8,12},{9,13},{12,... | collective-permute-start | bytes 1572872 | tf_op jit(solution)/shard_map/ppermute | solution.py:68
  100.6 2.2 %collective-permute-start.3 = (bf16[1024,256]{1,0:T(8,128)(2,1)}, bf16[1024,256]{1,0:T(8,128)(2,1)}, u32[]{:S(2)}, u32[]{:S(2)}) collective-permute-start(bf16[1024,256]{1,0:T(8,128)(2,1)} %get-tuple-element.16), channel_id=1, source_target_pairs={{0,5},{1,0},{4,1},{5,4},{2,7},{3,2},{6,3},{7,6},{8,13},{9,8},{12,9... | collective-permute-start | bytes 1572872 | tf_op jit(solution)/shard_map/ppermute | solution.py:68
  102.8 5.9 %collective-permute-done.1.w1 = bf16[1024,256]{1,0:T(8,128)(2,1)S(1)} collective-permute-done((bf16[1024,256]{1,0:T(8,128)(2,1)}, bf16[1024,256]{1,0:T(8,128)(2,1)S(1)}, u32[]{:S(2)}, u32[]{:S(2)}) %collective-permute-start.1) | collective-permute-done | bytes 524320 | tf_op jit(solution)/shard_map/ppermute | solution.py:68
  108.7 7.3 %collective-permute-done.2.w2 = bf16[1024,256]{1,0:T(8,128)(2,1)} collective-permute-done((bf16[1024,256]{1,0:T(8,128)(2,1)}, bf16[1024,256]{1,0:T(8,128)(2,1)}, u32[]{:S(2)}, u32[]{:S(2)}) %collective-permute-start.2) | collective-permute-done | bytes 524320 | tf_op jit(solution)/shard_map/ppermute | solution.py:68
  116.0 3.9 %shard_map.129 = bf16[4,776,256]{2,1,0:T(8,128)(2,1)S(1)} custom-call(s32[56]{0:T(128)S(1)} %dynamic-slice_bitcast_fusion.where, bf16[4,768,256]{2,1,0:T(8,128)(2,1)S(1)} %all-to-all-done.3.got, f32[16,256]{1,0:T(8,128)S(1)} %reshape.65.gain, bf16[1024,256]{1,0:T(8,128)(2,1)S(1)} %get-tuple-element.13.w0, bf16[1024,256]{1,0:T(8,128)(2,1)S(1)} %collective-permute-done.1.w1, ...), custom_call_target="tpu_custom_call" | custom-call | flops 1610612736 | bytes 5275872 | tf_op jit(solution)/shard_map/pallas_call | solution.py:80
  119.9 16.2 %all_to_all.41.parts = bf16[4,776,256]{2,1,0:T(8,128)(2,1)S(1)} all-to-all(bf16[4,776,256]{2,1,0:T(8,128)(2,1)S(1)} %shard_map.129), channel_id=1, replica_groups={{0,1,4,5},{2,3,6,7},{8,9,12,13},{10,11,14,15},{21,22,25,26},{23,20,27,2..., dimensions={0} | all-to-all | bytes 3178496 | tf_op jit(solution)/shard_map/all_to_all | solution.py:61
  136.1 1.3 shard_map.130
  137.4 7.9 %all-to-all-start.5 = ((bf16[4,768,128]{2,1,0:T(8,128)(2,1)}), bf16[4,768,128]{2,1,0:T(8,128)(2,1)S(1)}, u32[]{:S(2)}, u32[]{:S(2)}) async-start(bf16[4,768,128]{2,1,0:T(8,128)(2,1)} %shard_map.130), calls=%async_computation.5 | async-start | bytes 1572864 | tf_op jit(solution)/shard_map/all_to_all | solution.py:61
  146.0 1.9 collective-permute-start.4
  147.9 1.9 collective-permute-start.5
  149.8 4.3 %collective-permute-start.6 = (bf16[512,256]{1,0:T(8,128)(2,1)S(1)}, bf16[512,256]{1,0:T(8,128)(2,1)S(1)}, u32[]{:S(2)}, u32[]{:S(2)}) collective-permute-start(bf16[512,256]{1,0:T(8,128)(2,1)S(1)} %get-tuple-element.20), channel_id=1, source_target_pairs={{5,10},{6,5},{9,6},{10,9},{7,8},{4,7},{11,4},{8,11},{13,2},{14,13}... | collective-permute-start | bytes 786440 | tf_op jit(solution)/shard_map/ppermute | solution.py:68
  154.3 2.5 %collective-permute-done.5.w2 = bf16[512,256]{1,0:T(8,128)(2,1)S(1)} collective-permute-done((bf16[512,256]{1,0:T(8,128)(2,1)S(1)}, bf16[512,256]{1,0:T(8,128)(2,1)S(1)}, u32[]{:S(2)}, u32[]{:S(2)}) %collective-permute-start.5) | collective-permute-done | bytes 262176 | tf_op jit(solution)/shard_map/ppermute | solution.py:68
  156.8 1.6 collective-permute-done.6.w3
  158.4 1.5 shard_map.132
  160.0 15.0 %all_to_all.42 = bf16[4,768,256]{2,1,0:T(8,128)(2,1)S(1)} all-to-all(bf16[4,768,256]{2,1,0:T(8,128)(2,1)S(1)} %shard_map.132), channel_id=1, replica_groups={{5,6,9,10},{7,4,11,8},{13,14,1,2},{15,12,3,0},{16,17,20,21},{18,19,22,2..., dimensions={0} | all-to-all | bytes 3145728 | tf_op jit(solution)/shard_map/all_to_all | solution.py:61
  176.1 8.0 %all-to-all-start.7 = ((bf16[32,24,256]{2,1,0:T(8,128)(2,1)}), bf16[32,24,256]{2,1,0:T(8,128)(2,1)S(1)}, u32[]{:S(2)}, u32[]{:S(2)}) async-start(bf16[32,24,256]{2,1,0:T(8,128)(2,1)} %bitcast.14), calls=%async_computation.7 | async-start | bytes 786432 | tf_op jit(solution)/shard_map/all_to_all | solution.py:271
  184.1 27.8 %all-to-all-done.7 = bf16[32,24,256]{2,1,0:T(8,128)(2,1)S(1)} async-done(((bf16[32,24,256]{2,1,0:T(8,128)(2,1)}), bf16[32,24,256]{2,1,0:T(8,128)(2,1)S(1)}, u32[]{:S(2)}, u32[]{:S(2)}) %all-to-all-start.7) | async-done | bytes 393248 | tf_op jit(solution)/shard_map/all_to_all | solution.py:271
  (52 shorter events, 11.2 us)
Async XLA Ops:
  0.0 12.1 %copy-start = (bf16[1,128,128]{2,1,0:T(8,128)(2,1)S(1)}, bf16[1,128,128]{2,1,0:T(8,128)(2,1)}, u32[]{:S(2)}) copy-start(bf16[1,128,128]{2,1,0:T(8,128)(2,1)} %param.16) | copy-start | bytes 98308
  1.5 8.8 %collective-permute-start = (bf16[16,128]{1,0:T(8,128)(2,1)S(1)}, bf16[16,128]{1,0:T(8,128)(2,1)S(1)}, u32[]{:S(2)}, u32[]{:S(2)}) collective-permute-start(bf16[16,128]{1,0:T(8,128)(2,1)S(1)} %pad_maximum_fusion), channel_id=1, source_target_pairs={{0,16},{16,32},{32,48},{48,64},{64,80},{80,96},{96,112},{112,128},... | collective-permute-start | bytes 12296 | tf_op jit(solution)/shard_map/ppermute | solution.py:214
  14.6 7.6 %all-to-all-start = ((bf16[4,256,128]{2,1,0:T(8,128)(2,1)}), bf16[4,256,128]{2,1,0:T(8,128)(2,1)S(1)}, u32[]{:S(2)}, u32[]{:S(2)}) async-start(bf16[4,256,128]{2,1,0:T(8,128)(2,1)} %broadcast_in_dim.33), calls=%async_computation | async-start | bytes 524288 | tf_op jit(solution)/shard_map/all_to_all | solution.py:61
  23.4 7.5 %copy-start.7 = (s32[256,2]{0,1:T(2,128)S(1)}, s32[256,2]{0,1:T(2,128)}, u32[]{:S(2)}) copy-start(s32[256,2]{0,1:T(2,128)} %param.20) | copy-start | bytes 6148
  23.4 13.4 %copy-start.1 = (bf16[2048,256]{1,0:T(8,128)(2,1)S(1)}, bf16[2048,256]{1,0:T(8,128)(2,1)}, u32[]{:S(2)}) copy-start(bf16[2048,256]{1,0:T(8,128)(2,1)} %weight.1) | copy-start | bytes 3145732
  23.4 13.4 %copy-start.5 = (bf16[256,256]{1,0:T(8,128)(2,1)S(1)}, bf16[256,256]{1,0:T(8,128)(2,1)}, u32[]{:S(2)}) copy-start(bf16[256,256]{1,0:T(8,128)(2,1)} %residual.1) | copy-start | bytes 393220
  23.4 13.4 %all-to-all-start.1 = ((bf16[4,4,256,128]{3,2,1,0:T(8,128)(2,1)}), bf16[4,4,256,128]{3,2,1,0:T(8,128)(2,1)S(1)}, u32[]{:S(2)}, u32[]{:S(2)}) async-start(bf16[4,4,256,128]{3,2,1,0:T(8,128)(2,1)} %broadcast_in_dim.34), calls=%async_computation.1 | async-start | bytes 2097152 | tf_op jit(solution)/shard_map/all_to_all | solution.py:61
  85.3 3.7 %copy-start.2 = (bf16[1,4096,128]{2,1,0:T(8,128)(2,1)S(1)}, bf16[1,4096,128]{2,1,0:T(8,128)(2,1)}, u32[]{:S(2)}) copy-start(bf16[1,4096,128]{2,1,0:T(8,128)(2,1)} %param.22) | copy-start | bytes 3145732
  85.3 17.4 %copy-start.6 = (f32[4096]{0:T(1024)S(1)}, f32[4096]{0:T(1024)}, u32[]{:S(2)}) copy-start(f32[4096]{0:T(1024)} %param.19) | copy-start | bytes 49156
  85.3 30.7 %all-to-all-start.3 = ((bf16[4,768,256]{2,1,0:T(8,128)(2,1)}), bf16[4,768,256]{2,1,0:T(8,128)(2,1)S(1)}, u32[]{:S(2)}, u32[]{:S(2)}) async-start(bf16[4,768,256]{2,1,0:T(8,128)(2,1)} %broadcast_in_dim.41), calls=%async_computation.3 | async-start | bytes 3145728 | tf_op jit(solution)/shard_map/all_to_all | solution.py:61
  89.1 1.2 copy-start.3
  92.3 16.4 %collective-permute-start.1 = (bf16[1024,256]{1,0:T(8,128)(2,1)}, bf16[1024,256]{1,0:T(8,128)(2,1)S(1)}, u32[]{:S(2)}, u32[]{:S(2)}) collective-permute-start(bf16[1024,256]{1,0:T(8,128)(2,1)} %get-tuple-element.14), channel_id=1, source_target_pairs={{0,1},{1,4},{4,5},{5,0},{2,3},{3,6},{6,7},{7,2},{8,9},{9,12},{12,1... | collective-permute-start | bytes 1572872 | tf_op jit(solution)/shard_map/ppermute | solution.py:68
  98.4 17.6 %collective-permute-start.2 = (bf16[1024,256]{1,0:T(8,128)(2,1)}, bf16[1024,256]{1,0:T(8,128)(2,1)}, u32[]{:S(2)}, u32[]{:S(2)}) collective-permute-start(bf16[1024,256]{1,0:T(8,128)(2,1)} %get-tuple-element.15), channel_id=1, source_target_pairs={{0,4},{1,5},{4,0},{5,1},{2,6},{3,7},{6,2},{7,3},{8,12},{9,13},{12,... | collective-permute-start | bytes 1572872 | tf_op jit(solution)/shard_map/ppermute | solution.py:68
  100.6 15.4 %collective-permute-start.3 = (bf16[1024,256]{1,0:T(8,128)(2,1)}, bf16[1024,256]{1,0:T(8,128)(2,1)}, u32[]{:S(2)}, u32[]{:S(2)}) collective-permute-start(bf16[1024,256]{1,0:T(8,128)(2,1)} %get-tuple-element.16), channel_id=1, source_target_pairs={{0,5},{1,0},{4,1},{5,4},{2,7},{3,2},{6,3},{7,6},{8,13},{9,8},{12,9... | collective-permute-start | bytes 1572872 | tf_op jit(solution)/shard_map/ppermute | solution.py:68
  136.1 9.3 %copy-start.4 = (bf16[1,2048,256]{2,1,0:T(8,128)(2,1)S(1)}, bf16[1,2048,256]{2,1,0:T(8,128)(2,1)}, u32[]{:S(2)}) copy-start(bf16[1,2048,256]{2,1,0:T(8,128)(2,1)} %param.24) | copy-start | bytes 3145732
  137.4 21.0 %all-to-all-start.5 = ((bf16[4,768,128]{2,1,0:T(8,128)(2,1)}), bf16[4,768,128]{2,1,0:T(8,128)(2,1)S(1)}, u32[]{:S(2)}, u32[]{:S(2)}) async-start(bf16[4,768,128]{2,1,0:T(8,128)(2,1)} %shard_map.130), calls=%async_computation.5 | async-start | bytes 1572864 | tf_op jit(solution)/shard_map/all_to_all | solution.py:61
  146.0 8.3 %collective-permute-start.4 = (bf16[512,256]{1,0:T(8,128)(2,1)S(1)}, bf16[512,256]{1,0:T(8,128)(2,1)S(1)}, u32[]{:S(2)}, u32[]{:S(2)}) collective-permute-start(bf16[512,256]{1,0:T(8,128)(2,1)S(1)} %get-tuple-element.18), channel_id=1, source_target_pairs={{5,6},{6,9},{9,10},{10,5},{7,4},{4,11},{11,8},{8,7},{13,14},{14,1}... | collective-permute-start | bytes 786440 | tf_op jit(solution)/shard_map/ppermute | solution.py:68
  147.9 8.9 %collective-permute-start.5 = (bf16[512,256]{1,0:T(8,128)(2,1)S(1)}, bf16[512,256]{1,0:T(8,128)(2,1)S(1)}, u32[]{:S(2)}, u32[]{:S(2)}) collective-permute-start(bf16[512,256]{1,0:T(8,128)(2,1)S(1)} %get-tuple-element.19), channel_id=1, source_target_pairs={{5,9},{6,10},{9,5},{10,6},{7,11},{4,8},{11,7},{8,4},{13,1},{14,2},... | collective-permute-start | bytes 786440 | tf_op jit(solution)/shard_map/ppermute | solution.py:68
  149.8 8.6 %collective-permute-start.6 = (bf16[512,256]{1,0:T(8,128)(2,1)S(1)}, bf16[512,256]{1,0:T(8,128)(2,1)S(1)}, u32[]{:S(2)}, u32[]{:S(2)}) collective-permute-start(bf16[512,256]{1,0:T(8,128)(2,1)S(1)} %get-tuple-element.20), channel_id=1, source_target_pairs={{5,10},{6,5},{9,6},{10,9},{7,8},{4,7},{11,4},{8,11},{13,2},{14,13}... | collective-permute-start | bytes 786440 | tf_op jit(solution)/shard_map/ppermute | solution.py:68
  175.0 9.1 %copy-start.8 = (f32[256,2]{0,1:T(2,128)S(1)}, f32[256,2]{0,1:T(2,128)}, u32[]{:S(2)}) copy-start(f32[256,2]{0,1:T(2,128)} %param.21) | copy-start | bytes 6148
  176.1 35.9 %all-to-all-start.7 = ((bf16[32,24,256]{2,1,0:T(8,128)(2,1)}), bf16[32,24,256]{2,1,0:T(8,128)(2,1)S(1)}, u32[]{:S(2)}, u32[]{:S(2)}) async-start(bf16[32,24,256]{2,1,0:T(8,128)(2,1)} %bitcast.14), calls=%async_computation.7 | async-start | bytes 786432 | tf_op jit(solution)/shard_map/all_to_all | solution.py:271
where the time goes:
time: 214 us; the launch traced here: 213 us
  blocking collectives  77.2 us (36%)
  waiting for transfers between devices  56.9 us (27%)
  starting transfers between devices  52.7 us (25%)
  Pallas kernels  10.4 us (5%)
  local copies, waits for them, and re-layouts  7.47 us (3%)
  other arithmetic  4.96 us (2%)
  matrix products  3.49 us (2%)
    all_to_all x1, blocking collectives, layer(): lax.all_to_all(send.reshape(n_exp, cap, cols), SP, 0, 0, tiled=True)  46 us
    all_to_all x2, blocking collectives, a2a(): lax.all_to_all(blocks, PLANE, 0, 0, tiled=True, axis_index_groups=both_co...  31.2 us
    all_to_all x1, waiting for transfers between devices, layer(): lax.all_to_all(made.reshape(n_exp, cap, cols), SP, 0, 0, tiled=True)  27.8 us
    all_to_all x4, starting transfers between devices, a2a(): lax.all_to_all(blocks, PLANE, 0, 0, tiled=True, axis_index_groups=both_co...  21.2 us
    ppermute x6, starting transfers between devices, turns(): got.append(lax.ppermute(cuts[by], PLANE, pairs))  18.5 us
    ppermute x6, waiting for transfers between devices, turns(): got.append(lax.ppermute(cuts[by], PLANE, pairs))  17.5 us
    pallas_call x6, Pallas kernels, call(): pl.pallas_call(kernel, out_shape=outs[0] if single else tuple(outs), in_s...  10.4 us
    all_to_all x4, waiting for transfers between devices, a2a(): lax.all_to_all(blocks, PLANE, 0, 0, tiled=True, axis_index_groups=both_co...  8.89 us
  transfers between devices with their start and end apart: 12, of which 9 were waited for; matrix products, arithmetic and copies ran while one was open for 2% of the time, Pallas kernels for 1%

commit v1 on v0

--- a/solution.py
+++ b/solution.py
@@ -39,7 +39,7 @@
 
 
 def tables():
-    table = np.zeros((2, 16, 56), np.int32)
+    table = np.zeros((2, 16, 40), np.int32)
     for core in range(2):
         for me in range(16):
             gather, scatter = group_with(GATHER[core], me), group_with(SCATTER[core], me)
@@ -49,12 +49,11 @@
                 row += group_with(GATHER[core], scatter[(p + by) % 4])
             for by in range(4):
                 row += group_with(SCATTER[core], gather[(q + by) % 4])
-            channels = sum((group_with(GATHER[core], member) for member in scatter), [])
-            table[core, me, :54] = row + gather + [p, q] + channels
+            table[core, me, :38] = row + gather + [p, q]
     return table
 
 
-FEATURES, HIDDEN, GAINS, IN_SCATTER, IN_GATHER, CHANNELS = 0, 16, 32, 36, 37, 38
+FEATURES, HIDDEN, GAINS, IN_SCATTER, IN_GATHER = 0, 16, 32, 36, 37
 
 
 def a2a(blocks, groups):
@@ -102,18 +101,6 @@
         for i in range(4):
             block = where[HIDDEN + 4 * by + i]
             outs[by][pl.ds(128 * i, 128), :] = down[pl.ds(pl.multiple_of(block * 128, 128), 128), :]
-
-
-def project(where, pooled, weight, residual, out):
-    total = residual[...].astype(F32)
-    for j in range(4):
-        rows = []
-        for i in range(4):
-            block = where[CHANNELS + 4 * j + i]
-            rows.append(weight[pl.ds(pl.multiple_of(block * 128, 128), 128), :])
-        part = jnp.concatenate([pooled[j, i] for i in range(4)], axis=1)
-        total = total + jnp.dot(part, jnp.concatenate(rows, axis=0), preferred_element_type=F32)
-    out[...] = total.astype(BF16)
 
 
 def gate_up(where, got, gain, w0, w1, w2, w3, out, rows):
@@ -243,8 +230,8 @@
     cap = length * TOPK * 3 // (2 * n_exp)
     slots = n_exp * cap
     where = lax.dynamic_slice(
-        jnp.asarray(tables()), (lax.axis_index("c"), lax.axis_index(TP), 0), (1, 1, 56)
-    ).reshape(56)
+        jnp.asarray(tables()), (lax.axis_index("c"), lax.axis_index(TP), 0), (1, 1, 40)
+    ).reshape(40)
     pooled = pool(pool_in, docs, pool_weight, pool_gain)
     ids = routes.reshape(-1)
     onehot = (ids[:, None] == jnp.arange(n_exp)[None, :]).astype(jnp.int32)
@@ -259,9 +246,9 @@
     cuts_first = call(cut_first, [shape(1024, 256)] * 4, where, w_gate[0], w_up[0], flops=2**22)
     cuts_second = call(cut_second, [shape(512, 256)] * 4, where, w_down[0], flops=2**21)
 
-    near = a2a(jnp.broadcast_to(pooled[None], (4, *pooled.shape)), GATHER)
-    pooled_all = a2a(jnp.broadcast_to(near[None], (4, *near.shape)), SCATTER)
-    updated = call(project, [shape(length, cols)], where, pooled_all, out_weight, residual, flops=2**28)
+    pooled_all = lax.all_to_all(jnp.broadcast_to(pooled[None], (16, *pooled.shape)), TP, 0, 0, tiled=True)
+    proj = jnp.einsum("gtc,gcd->td", pooled_all, out_weight.reshape(16, 128, cols), preferred_element_type=F32)
+    updated = (residual.astype(F32) + proj).astype(BF16)
 
     send = jnp.dot(take.astype(BF16), updated, preferred_element_type=F32).astype(BF16)
     arrived = lax.all_to_all(send.reshape(n_exp, cap, cols), SP, 0, 0, tiled=True).reshape(slots, cols)

time: 214 us -> 214 us (level)
  waiting for transfers between devices: 56.9 us -> 62.1 us
  starting transfers between devices: 52.7 us -> 48.1 us
  blocking collectives: 77.2 us -> 74.9 us
    all_to_all x0 -> x1, waiting for transfers between devices: none -> 16.1 us  [layer(): lax.all_to_all(jnp.broadcast_to(pooled[None], (16, *pooled.shape)), TP, 0...]
    all_to_all x4 -> x2, starting transfers between devices: 21.2 us -> 11.5 us  [a2a(): lax.all_to_all(blocks, PLANE, 0, 0, tiled=True, axis_index_groups=both_co...]
    all_to_all x4 -> x2, waiting for transfers between devices: 8.89 us -> 0.01 us  [a2a(): lax.all_to_all(blocks, PLANE, 0, 0, tiled=True, axis_index_groups=both_co...]
    all_to_all x0 -> x1, starting transfers between devices: none -> 3.79 us  [layer(): lax.all_to_all(jnp.broadcast_to(pooled[None], (16, *pooled.shape)), TP, 0...]
    ppermute x6, waiting for transfers between devices: 17.5 us -> 14.5 us  [turns(): got.append(lax.ppermute(cuts[by], PLANE, pairs))]
    unnamed x19 -> x21, local copies, waits for them, and re-layouts: 2.06 us -> 4.47 us
    all_to_all x1, starting transfers between devices: 7.99 us -> 10.4 us  [layer(): lax.all_to_all(made.reshape(n_exp, cap, cols), SP, 0, 0, tiled=True)]
    all_to_all x1, blocking collectives: 46 us -> 43.7 us  [layer(): lax.all_to_all(send.reshape(n_exp, cap, cols), SP, 0, 0, tiled=True)]
  transfers between devices with their start and end apart: 12 -> 11, of which waited for: 9 -> 8; matrix products, arithmetic and copies ran while one was open for 2% -> 1% of each run, Pallas kernels for 1% -> 1%
where the time goes in v1:
time: 214 us; the launch traced here: 213 us
  blocking collectives  74.9 us (35%)
  waiting for transfers between devices  62.1 us (29%)
  starting transfers between devices  48.1 us (22%)
  Pallas kernels  9.51 us (4%)
  local copies, waits for them, and re-layouts  9.15 us (4%)
  other arithmetic  5 us (2%)
  matrix products  4.04 us (2%)
    all_to_all x1, blocking collectives, layer(): lax.all_to_all(send.reshape(n_exp, cap, cols), SP, 0, 0, tiled=True)  43.7 us
    all_to_all x2, blocking collectives, a2a(): lax.all_to_all(blocks, PLANE, 0, 0, tiled=True, axis_index_groups=both_co...  31.3 us
    all_to_all x1, waiting for transfers between devices, layer(): lax.all_to_all(made.reshape(n_exp, cap, cols), SP, 0, 0, tiled=True)  27.8 us
    ppermute x6, starting transfers between devices, turns(): got.append(lax.ppermute(cuts[by], PLANE, pairs))  17.5 us
    all_to_all x1, waiting for transfers between devices, layer(): lax.all_to_all(jnp.broadcast_to(pooled[None], (16, *pooled.shape)), TP, 0...  16.1 us
    ppermute x6, waiting for transfers between devices, turns(): got.append(lax.ppermute(cuts[by], PLANE, pairs))  14.5 us
    all_to_all x2, starting transfers between devices, a2a(): lax.all_to_all(blocks, PLANE, 0, 0, tiled=True, axis_index_groups=both_co...  11.5 us
    all_to_all x1, starting transfers between devices, layer(): lax.all_to_all(made.reshape(n_exp, cap, cols), SP, 0, 0, tiled=True)  10.4 us
  transfers between devices with their start and end apart: 11, of which 8 were waited for; matrix products, arithmetic and copies ran while one was open for 1% of the time, Pallas kernels for 1%

profile of v1, /device:TPU:1, one launch (start us, length us, event | category | flops | bytes accessed | tf_op | source)
XLA Modules:
  0.0 213.2 jit_solution(13660397012795903846)
XLA Ops:
  1.6 4.9 %collective-permute-start = (bf16[16,128]{1,0:T(8,128)(2,1)S(1)}, bf16[16,128]{1,0:T(8,128)(2,1)S(1)}, u32[]{:S(2)}, u32[]{:S(2)}) collective-permute-start(bf16[16,128]{1,0:T(8,128)(2,1)S(1)} %pad_maximum_fusion), channel_id=1, source_target_pairs={{0,16},{16,32},{32,48},{48,64},{64,80},{80,96},{96,112},{112,128},... | collective-permute-start | bytes 12296 | tf_op jit(solution)/shard_map/ppermute | solution.py:201
  6.6 3.8 %collective-permute-done = bf16[16,128]{1,0:T(8,128)(2,1)S(1)} collective-permute-done((bf16[16,128]{1,0:T(8,128)(2,1)S(1)}, bf16[16,128]{1,0:T(8,128)(2,1)S(1)}, u32[]{:S(2)}, u32[]{:S(2)}) %collective-permute-start) | collective-permute-done | bytes 4128 | tf_op jit(solution)/shard_map/ppermute | solution.py:201
  12.1 1.8 fusion.4
  14.0 1.2 broadcast_in_dim.31
  15.2 3.8 %all-to-all-start = ((bf16[16,256,128]{2,1,0:T(8,128)(2,1)}), bf16[16,256,128]{2,1,0:T(8,128)(2,1)S(1)}, u32[]{:S(2)}, u32[]{:S(2)}) async-start(bf16[16,256,128]{2,1,0:T(8,128)(2,1)} %broadcast_in_dim.31), calls=%async_computation | async-start | bytes 2097152 | tf_op jit(solution)/shard_map/all_to_all | solution.py:249
  19.4 1.2 reduce-window.6
  21.2 16.1 %all-to-all-done = bf16[16,256,128]{2,1,0:T(8,128)(2,1)S(1)} async-done(((bf16[16,256,128]{2,1,0:T(8,128)(2,1)}), bf16[16,256,128]{2,1,0:T(8,128)(2,1)S(1)}, u32[]{:S(2)}, u32[]{:S(2)}) %all-to-all-start) | async-done | bytes 1048608 | tf_op jit(solution)/shard_map/all_to_all | solution.py:249
  38.0 43.7 %all_to_all.35 = bf16[32,24,256]{2,1,0:T(8,128)(2,1)S(1)} all-to-all(bf16[32,24,256]{2,1,0:T(8,128)(2,1)S(1)} %bitcast.58), channel_id=1, replica_groups=mesh['z'=16,'c'=2,'y'=4,'x'=4] {'z','c'}, dimensions={0} | all-to-all | bytes 786432 | tf_op jit(solution)/shard_map/all_to_all | solution.py:254
  81.7 1.3 broadcast_in_dim.38
  83.0 3.7 %all-to-all-start.2 = ((bf16[4,768,256]{2,1,0:T(8,128)(2,1)}), bf16[4,768,256]{2,1,0:T(8,128)(2,1)S(1)}, u32[]{:S(2)}, u32[]{:S(2)}) async-start(bf16[4,768,256]{2,1,0:T(8,128)(2,1)} %broadcast_in_dim.38), calls=%async_computation.2 | async-start | bytes 3145728 | tf_op jit(solution)/shard_map/all_to_all | solution.py:60
  87.4 1.2 copy-done.1
  88.6 1.2 copy-done.2
  89.8 2.0 shard_map.127
  92.7 2.8 %collective-permute-start.1 = (bf16[1024,256]{1,0:T(8,128)(2,1)}, bf16[1024,256]{1,0:T(8,128)(2,1)}, u32[]{:S(2)}, u32[]{:S(2)}) collective-permute-start(bf16[1024,256]{1,0:T(8,128)(2,1)} %get-tuple-element.14), channel_id=1, source_target_pairs={{0,1},{1,4},{4,5},{5,0},{2,3},{3,6},{6,7},{7,2},{8,9},{9,12},{12,1... | collective-permute-start | bytes 1572872 | tf_op jit(solution)/shard_map/ppermute | solution.py:67
  95.5 2.2 %collective-permute-start.2 = (bf16[1024,256]{1,0:T(8,128)(2,1)}, bf16[1024,256]{1,0:T(8,128)(2,1)}, u32[]{:S(2)}, u32[]{:S(2)}) collective-permute-start(bf16[1024,256]{1,0:T(8,128)(2,1)} %get-tuple-element.15), channel_id=1, source_target_pairs={{0,4},{1,5},{4,0},{5,1},{2,6},{3,7},{6,2},{7,3},{8,12},{9,13},{12,... | collective-permute-start | bytes 1572872 | tf_op jit(solution)/shard_map/ppermute | solution.py:67
  97.7 4.4 %collective-permute-start.3 = (bf16[1024,256]{1,0:T(8,128)(2,1)}, bf16[1024,256]{1,0:T(8,128)(2,1)}, u32[]{:S(2)}, u32[]{:S(2)}) collective-permute-start(bf16[1024,256]{1,0:T(8,128)(2,1)} %get-tuple-element.16), channel_id=1, source_target_pairs={{0,5},{1,0},{4,1},{5,4},{2,7},{3,2},{6,3},{7,6},{8,13},{9,8},{12,9... | collective-permute-start | bytes 1572872 | tf_op jit(solution)/shard_map/ppermute | solution.py:67
  102.1 4.2 %collective-permute-done.1.w1 = bf16[1024,256]{1,0:T(8,128)(2,1)} collective-permute-done((bf16[1024,256]{1,0:T(8,128)(2,1)}, bf16[1024,256]{1,0:T(8,128)(2,1)}, u32[]{:S(2)}, u32[]{:S(2)}) %collective-permute-start.1) | collective-permute-done | bytes 524320 | tf_op jit(solution)/shard_map/ppermute | solution.py:67
  106.3 6.2 %collective-permute-done.2.w2 = bf16[1024,256]{1,0:T(8,128)(2,1)} collective-permute-done((bf16[1024,256]{1,0:T(8,128)(2,1)}, bf16[1024,256]{1,0:T(8,128)(2,1)}, u32[]{:S(2)}, u32[]{:S(2)}) %collective-permute-start.2) | collective-permute-done | bytes 524320 | tf_op jit(solution)/shard_map/ppermute | solution.py:67
  113.6 4.0 %shard_map.128 = bf16[4,776,256]{2,1,0:T(8,128)(2,1)S(1)} custom-call(s32[40]{0:T(128)S(1)} %dynamic-slice_bitcast_fusion.where, bf16[4,768,256]{2,1,0:T(8,128)(2,1)S(1)} %all-to-all-done.2.got, f32[16,256]{1,0:T(8,128)S(1)} %reshape.68.gain, bf16[1024,256]{1,0:T(8,128)(2,1)S(1)} %copy-done.5, bf16[1024,256]{1,0:T(8,128)(2,1)} %collective-permute-done.1.w1, ...), custom_call_target="tpu_custom_call" | custom-call | flops 1610612736 | bytes 5275808 | tf_op jit(solution)/shard_map/pallas_call | solution.py:79
  117.6 15.9 %all_to_all.36.parts = bf16[4,776,256]{2,1,0:T(8,128)(2,1)S(1)} all-to-all(bf16[4,776,256]{2,1,0:T(8,128)(2,1)S(1)} %shard_map.128), channel_id=1, replica_groups={{0,1,4,5},{2,3,6,7},{8,9,12,13},{10,11,14,15},{21,22,25,26},{23,20,27,2..., dimensions={0} | all-to-all | bytes 3178496 | tf_op jit(solution)/shard_map/all_to_all | solution.py:60
  133.6 1.3 shard_map.129
  134.9 7.8 %all-to-all-start.4 = ((bf16[4,768,128]{2,1,0:T(8,128)(2,1)}), bf16[4,768,128]{2,1,0:T(8,128)(2,1)S(1)}, u32[]{:S(2)}, u32[]{:S(2)}) async-start(bf16[4,768,128]{2,1,0:T(8,128)(2,1)} %shard_map.129), calls=%async_computation.4 | async-start | bytes 1572864 | tf_op jit(solution)/shard_map/all_to_all | solution.py:60
  143.3 1.9 collective-permute-start.4
  145.3 1.9 collective-permute-start.5
  147.2 4.3 %collective-permute-start.6 = (bf16[512,256]{1,0:T(8,128)(2,1)S(1)}, bf16[512,256]{1,0:T(8,128)(2,1)S(1)}, u32[]{:S(2)}, u32[]{:S(2)}) collective-permute-start(bf16[512,256]{1,0:T(8,128)(2,1)S(1)} %get-tuple-element.20), channel_id=1, source_target_pairs={{5,10},{6,5},{9,6},{10,9},{7,8},{4,7},{11,4},{8,11},{13,2},{14,13}... | collective-permute-start | bytes 786440 | tf_op jit(solution)/shard_map/ppermute | solution.py:67
  151.5 2.2 %collective-permute-done.4.w1 = bf16[512,256]{1,0:T(8,128)(2,1)S(1)} collective-permute-done((bf16[512,256]{1,0:T(8,128)(2,1)S(1)}, bf16[512,256]{1,0:T(8,128)(2,1)S(1)}, u32[]{:S(2)}, u32[]{:S(2)}) %collective-permute-start.4) | collective-permute-done | bytes 262176 | tf_op jit(solution)/shard_map/ppermute | solution.py:67
  153.7 1.6 collective-permute-done.5.w2
  155.5 1.5 shard_map.131
  157.0 15.3 %all_to_all.37 = bf16[4,768,256]{2,1,0:T(8,128)(2,1)S(1)} all-to-all(bf16[4,768,256]{2,1,0:T(8,128)(2,1)S(1)} %shard_map.131), channel_id=1, replica_groups={{5,6,9,10},{7,4,11,8},{13,14,1,2},{15,12,3,0},{16,17,20,21},{18,19,22,2..., dimensions={0} | all-to-all | bytes 3145728 | tf_op jit(solution)/shard_map/all_to_all | solution.py:60
  173.4 10.4 %all-to-all-start.6 = ((bf16[32,24,256]{2,1,0:T(8,128)(2,1)}), bf16[32,24,256]{2,1,0:T(8,128)(2,1)S(1)}, u32[]{:S(2)}, u32[]{:S(2)}) async-start(bf16[32,24,256]{2,1,0:T(8,128)(2,1)} %bitcast.16), calls=%async_computation.6 | async-start | bytes 786432 | tf_op jit(solution)/shard_map/all_to_all | solution.py:258
  183.9 27.8 %all-to-all-done.6 = bf16[32,24,256]{2,1,0:T(8,128)(2,1)S(1)} async-done(((bf16[32,24,256]{2,1,0:T(8,128)(2,1)}), bf16[32,24,256]{2,1,0:T(8,128)(2,1)S(1)}, u32[]{:S(2)}, u32[]{:S(2)}) %all-to-all-start.6) | async-done | bytes 393248 | tf_op jit(solution)/shard_map/all_to_all | solution.py:258
  212.1 1.1 fusion.3
  (51 shorter events, 10.1 us)
Async XLA Ops:
  0.0 37.3 %copy-start = (bf16[2048,256]{1,0:T(8,128)(2,1)S(1)}, bf16[2048,256]{1,0:T(8,128)(2,1)}, u32[]{:S(2)}) copy-start(bf16[2048,256]{1,0:T(8,128)(2,1)} %param.18) | copy-start | bytes 3145732
  1.6 8.8 %collective-permute-start = (bf16[16,128]{1,0:T(8,128)(2,1)S(1)}, bf16[16,128]{1,0:T(8,128)(2,1)S(1)}, u32[]{:S(2)}, u32[]{:S(2)}) collective-permute-start(bf16[16,128]{1,0:T(8,128)(2,1)S(1)} %pad_maximum_fusion), channel_id=1, source_target_pairs={{0,16},{16,32},{32,48},{48,64},{64,80},{80,96},{96,112},{112,128},... | collective-permute-start | bytes 12296 | tf_op jit(solution)/shard_map/ppermute | solution.py:201
  14.0 5.0 %copy-start.8 = (s32[256,2]{0,1:T(2,128)S(1)}, s32[256,2]{0,1:T(2,128)}, u32[]{:S(2)}) copy-start(s32[256,2]{0,1:T(2,128)} %param.20) | copy-start | bytes 6148
  15.2 22.1 %copy-start.6 = (bf16[256,256]{1,0:T(8,128)(2,1)S(1)}, bf16[256,256]{1,0:T(8,128)(2,1)}, u32[]{:S(2)}) copy-start(bf16[256,256]{1,0:T(8,128)(2,1)} %param.13) | copy-start | bytes 393220
  15.2 22.1 %all-to-all-start = ((bf16[16,256,128]{2,1,0:T(8,128)(2,1)}), bf16[16,256,128]{2,1,0:T(8,128)(2,1)S(1)}, u32[]{:S(2)}, u32[]{:S(2)}) async-start(bf16[16,256,128]{2,1,0:T(8,128)(2,1)} %broadcast_in_dim.31), calls=%async_computation | async-start | bytes 2097152 | tf_op jit(solution)/shard_map/all_to_all | solution.py:249
  83.0 19.1 %copy-start.7 = (f32[4096]{0:T(1024)S(1)}, f32[4096]{0:T(1024)}, u32[]{:S(2)}) copy-start(f32[4096]{0:T(1024)} %param.19) | copy-start | bytes 49156
  83.0 29.6 %all-to-all-start.2 = ((bf16[4,768,256]{2,1,0:T(8,128)(2,1)}), bf16[4,768,256]{2,1,0:T(8,128)(2,1)S(1)}, u32[]{:S(2)}, u32[]{:S(2)}) async-start(bf16[4,768,256]{2,1,0:T(8,128)(2,1)} %broadcast_in_dim.38), calls=%async_computation.2 | async-start | bytes 3145728 | tf_op jit(solution)/shard_map/all_to_all | solution.py:60
  87.4 1.2 copy-start.1
  88.6 1.2 copy-start.2
  91.8 0.8 copy-start.4
  92.7 13.7 %collective-permute-start.1 = (bf16[1024,256]{1,0:T(8,128)(2,1)}, bf16[1024,256]{1,0:T(8,128)(2,1)}, u32[]{:S(2)}, u32[]{:S(2)}) collective-permute-start(bf16[1024,256]{1,0:T(8,128)(2,1)} %get-tuple-element.14), channel_id=1, source_target_pairs={{0,1},{1,4},{4,5},{5,0},{2,3},{3,6},{6,7},{7,2},{8,9},{9,12},{12,1... | collective-permute-start | bytes 1572872 | tf_op jit(solution)/shard_map/ppermute | solution.py:67
  95.5 17.1 %collective-permute-start.2 = (bf16[1024,256]{1,0:T(8,128)(2,1)}, bf16[1024,256]{1,0:T(8,128)(2,1)}, u32[]{:S(2)}, u32[]{:S(2)}) collective-permute-start(bf16[1024,256]{1,0:T(8,128)(2,1)} %get-tuple-element.15), channel_id=1, source_target_pairs={{0,4},{1,5},{4,0},{5,1},{2,6},{3,7},{6,2},{7,3},{8,12},{9,13},{12,... | collective-permute-start | bytes 1572872 | tf_op jit(solution)/shard_map/ppermute | solution.py:67
  97.7 14.9 %collective-permute-start.3 = (bf16[1024,256]{1,0:T(8,128)(2,1)}, bf16[1024,256]{1,0:T(8,128)(2,1)}, u32[]{:S(2)}, u32[]{:S(2)}) collective-permute-start(bf16[1024,256]{1,0:T(8,128)(2,1)} %get-tuple-element.16), channel_id=1, source_target_pairs={{0,5},{1,0},{4,1},{5,4},{2,7},{3,2},{6,3},{7,6},{8,13},{9,8},{12,9... | collective-permute-start | bytes 1572872 | tf_op jit(solution)/shard_map/ppermute | solution.py:67
  112.6 1.0 copy-start.5
  133.6 9.1 %copy-start.3 = (bf16[1,2048,256]{2,1,0:T(8,128)(2,1)S(1)}, bf16[1,2048,256]{2,1,0:T(8,128)(2,1)}, u32[]{:S(2)}) copy-start(bf16[1,2048,256]{2,1,0:T(8,128)(2,1)} %param.24) | copy-start | bytes 3145732
  134.9 20.6 %all-to-all-start.4 = ((bf16[4,768,128]{2,1,0:T(8,128)(2,1)}), bf16[4,768,128]{2,1,0:T(8,128)(2,1)S(1)}, u32[]{:S(2)}, u32[]{:S(2)}) async-start(bf16[4,768,128]{2,1,0:T(8,128)(2,1)} %shard_map.129), calls=%async_computation.4 | async-start | bytes 1572864 | tf_op jit(solution)/shard_map/all_to_all | solution.py:60
  143.3 10.3 %collective-permute-start.4 = (bf16[512,256]{1,0:T(8,128)(2,1)S(1)}, bf16[512,256]{1,0:T(8,128)(2,1)S(1)}, u32[]{:S(2)}, u32[]{:S(2)}) collective-permute-start(bf16[512,256]{1,0:T(8,128)(2,1)S(1)} %get-tuple-element.18), channel_id=1, source_target_pairs={{5,6},{6,9},{9,10},{10,5},{7,4},{4,11},{11,8},{8,7},{13,14},{14,1}... | collective-permute-start | bytes 786440 | tf_op jit(solution)/shard_map/ppermute | solution.py:67
  145.3 10.0 %collective-permute-start.5 = (bf16[512,256]{1,0:T(8,128)(2,1)S(1)}, bf16[512,256]{1,0:T(8,128)(2,1)S(1)}, u32[]{:S(2)}, u32[]{:S(2)}) collective-permute-start(bf16[512,256]{1,0:T(8,128)(2,1)S(1)} %get-tuple-element.19), channel_id=1, source_target_pairs={{5,9},{6,10},{9,5},{10,6},{7,11},{4,8},{11,7},{8,4},{13,1},{14,2},... | collective-permute-start | bytes 786440 | tf_op jit(solution)/shard_map/ppermute | solution.py:67
  147.2 8.3 %collective-permute-start.6 = (bf16[512,256]{1,0:T(8,128)(2,1)S(1)}, bf16[512,256]{1,0:T(8,128)(2,1)S(1)}, u32[]{:S(2)}, u32[]{:S(2)}) collective-permute-start(bf16[512,256]{1,0:T(8,128)(2,1)S(1)} %get-tuple-element.20), channel_id=1, source_target_pairs={{5,10},{6,5},{9,6},{10,9},{7,8},{4,7},{11,4},{8,11},{13,2},{14,13}... | collective-permute-start | bytes 786440 | tf_op jit(solution)/shard_map/ppermute | solution.py:67
  172.3 11.5 %copy-start.9 = (f32[256,2]{0,1:T(2,128)S(1)}, f32[256,2]{0,1:T(2,128)}, u32[]{:S(2)}) copy-start(f32[256,2]{0,1:T(2,128)} %param.21) | copy-start | bytes 6148
  173.4 38.3 %all-to-all-start.6 = ((bf16[32,24,256]{2,1,0:T(8,128)(2,1)}), bf16[32,24,256]{2,1,0:T(8,128)(2,1)S(1)}, u32[]{:S(2)}, u32[]{:S(2)}) async-start(bf16[32,24,256]{2,1,0:T(8,128)(2,1)} %bitcast.16), calls=%async_computation.6 | async-start | bytes 786432 | tf_op jit(solution)/shard_map/all_to_all | solution.py:258

commit v2 on v1

--- a/solution.py
+++ b/solution.py
@@ -16,6 +16,7 @@
 F32 = jnp.float32
 BF16 = jnp.bfloat16
 VMEM_BYTES = 20 * 2**20
+LARGE = 58 * 2**20
 
 
 def blocks_of(shift):
@@ -49,11 +50,11 @@
                 row += group_with(GATHER[core], scatter[(p + by) % 4])
             for by in range(4):
                 row += group_with(SCATTER[core], gather[(q + by) % 4])
-            table[core, me, :38] = row + gather + [p, q]
+            table[core, me, :39] = row + gather + [p, q, 2 ** (1 + me % 4)]
     return table
 
 
-FEATURES, HIDDEN, GAINS, IN_SCATTER, IN_GATHER = 0, 16, 32, 36, 37
+FEATURES, HIDDEN, GAINS, IN_SCATTER, IN_GATHER, SPAN, SP_INDEX = 0, 16, 32, 36, 37, 38, 39
 
 
 def a2a(blocks, groups):
@@ -72,17 +73,19 @@
     return jax.ShapeDtypeStruct(dims, dtype)
 
 
-def call(kernel, outs, *args, flops, scratch=()):
+def call(kernel, outs, *args, flops, scratch=(), vmem=VMEM_BYTES, tables=1, fetched=0):
     single = len(outs) == 1
     moved = sum(a.size * a.dtype.itemsize for a in (*args, *outs))
-    vmem = pl.BlockSpec(memory_space=pltpu.VMEM)
+    whole = pl.BlockSpec(memory_space=pltpu.VMEM)
+    specs = [pl.BlockSpec(memory_space=pltpu.SMEM)] * tables
+    specs += [whole] * (len(args) - tables - fetched) + [pl.BlockSpec(memory_space=pltpu.HBM)] * fetched
     return pl.pallas_call(
         kernel,
         out_shape=outs[0] if single else tuple(outs),
-        in_specs=[pl.BlockSpec(memory_space=pltpu.SMEM) if a.dtype == jnp.int32 else vmem for a in args],
-        out_specs=vmem if single else (vmem,) * len(outs),
+        in_specs=specs,
+        out_specs=whole if single else (whole,) * len(outs),
         scratch_shapes=list(scratch),
-        compiler_params=pltpu.CompilerParams(vmem_limit_bytes=VMEM_BYTES),
+        compiler_params=pltpu.CompilerParams(vmem_limit_bytes=vmem),
         cost_estimate=pl.CostEstimate(flops=flops, bytes_accessed=moved, transcendentals=0),
     )(*args)
 
@@ -103,7 +106,14 @@
             outs[by][pl.ds(128 * i, 128), :] = down[pl.ds(pl.multiple_of(block * 128, 128), 128), :]
 
 
-def gate_up(where, got, gain, w0, w1, w2, w3, out, rows):
+def fetches(sources, held, arrived):
+    return [pltpu.make_async_copy(w, held.at[by], arrived.at[by]) for by, w in enumerate(sources)]
+
+
+def gate_up(where, got, gain, w0, w1, w2, w3, out, rows, held, arrived):
+    copies = fetches((w0, w1, w2, w3), held, arrived)
+    for copy in copies:
+        copy.start()
     count = got.shape[1]
     ones = jnp.ones((8, 256), BF16)
     tiles = count // 256
@@ -123,12 +133,13 @@
         for j in range(4):
             out[j, pl.ds(count + 2 * i, 1), :] = high[:1]
             out[j, pl.ds(count + 2 * i + 1, 1), :] = low[:1]
-    for by, first in enumerate((w0, w1, w2, w3)):
+    for by, copy in enumerate(copies):
+        copy.wait()
         to = lax.rem(where[IN_SCATTER] + 4 - by, 4)
         out[to, pl.ds(count + 2 * tiles, 8 - 2 * tiles), :] = jnp.zeros((8 - 2 * tiles, 256), BF16)
         for i in range(tiles):
             tile = pl.ds(256 * i, 256)
-            out[to, tile, :] = jnp.dot(rows[tile, :], first[...], preferred_element_type=F32).astype(BF16)
+            out[to, tile, :] = jnp.dot(rows[tile, :], held[by], preferred_element_type=F32).astype(BF16)
 
 
 def activate(parts, out):
@@ -151,15 +162,19 @@
             out[j, tile, :] = act
 
 
-def down_rows(where, acts, w0, w1, w2, w3, out, rows):
+def down_rows(where, acts, w0, w1, w2, w3, out, rows, held, arrived):
+    copies = fetches((w0, w1, w2, w3), held, arrived)
+    for copy in copies:
+        copy.start()
     count = acts.shape[1]
     for h in range(4):
         rows[:, pl.ds(128 * h, 128)] = acts[h]
-    for by, second in enumerate((w0, w1, w2, w3)):
+    for by, copy in enumerate(copies):
+        copy.wait()
         to = lax.rem(where[IN_GATHER] + 4 - by, 4)
         for i in range(count // 256):
             tile = pl.ds(256 * i, 256)
-            out[to, tile, :] = jnp.dot(rows[tile, :], second[...], preferred_element_type=F32).astype(BF16)
+            out[to, tile, :] = jnp.dot(rows[tile, :], held[by], preferred_element_type=F32).astype(BF16)
 
 
 def experts(arrived, first, second, where, gain):
@@ -173,10 +188,11 @@
         gain,
         *first,
         flops=2**21 * count,
-        scratch=[pltpu.VMEM((count, 1024), BF16)],
+        scratch=[pltpu.VMEM((count, 1024), BF16), pltpu.VMEM((4, 1024, 256), BF16), pltpu.SemaphoreType.DMA((4,))],
+        fetched=4,
     )
     parts = a2a(part, SCATTER)
-    acts = a2a(call(activate, [shape(4, count, 128)], parts, flops=2**16 * count), SCATTER)
+    acts = a2a(call(activate, [shape(4, count, 128)], parts, flops=2**16 * count, tables=0), SCATTER)
     part = call(
         down_rows,
         [shape(4, count, 256)],
@@ -184,37 +200,36 @@
         acts,
         *second,
         flops=2**20 * count,
-        scratch=[pltpu.VMEM((count, 512), BF16)],
+        scratch=[pltpu.VMEM((count, 512), BF16), pltpu.VMEM((4, 512, 256), BF16), pltpu.SemaphoreType.DMA((4,))],
+        fetched=4,
     )
     parts = a2a(part, GATHER)
     return jnp.sum(parts.astype(F32), axis=0).astype(BF16)
 
 
-def pool(pool_in, docs, pool_weight, pool_gain):
-    length, width = pool_in.shape
-    sp_index = lax.axis_index(SP)
-    group = lax.axis_index(TP)
-    size = lax.axis_size(SP)
-    reach = 15
-    tail = docs[length - 16 :].astype(BF16)
-    edge = jnp.concatenate([pool_in[length - reach :], jnp.pad(tail, (0, width - 16))[None]], axis=0)
-    prev = lax.ppermute(edge, SP, [(i, i + 1) for i in range(size - 1)])
-    extended = jnp.concatenate([prev[:reach], pool_in], axis=0).astype(F32)
-    own_docs = docs.astype(F32)
-    ext_docs = jnp.concatenate([prev[reach, 1:16].astype(F32), own_docs])
-    places = sp_index * length + jnp.arange(length)
-    span = 2 ** (1 + group % 4)
-    totals = jnp.zeros((length, width), F32)
-    counts = jnp.zeros((length,), F32)
-    for offset in range(16):
-        shifted = extended[reach - offset : reach - offset + length]
-        prior = ext_docs[reach - offset : reach - offset + length]
-        same = ((places >= offset) & (prior == own_docs) & (offset < span)).astype(F32)
-        totals = totals + same[:, None] * shifted
-        counts = counts + same
-    diff = (totals / counts[:, None] - extended[reach:]).astype(BF16)
-    mixed = jnp.dot(diff, pool_weight[0], preferred_element_type=F32)
-    return (mixed * pool_gain).astype(BF16)
+def pool(where, own, before, docs, docs_before, weight, gain, out, extended):
+    length, width = own.shape
+    sp_index, span = where[SP_INDEX], where[SPAN]
+    extended[pl.ds(0, 16), :] = before[pl.ds(length - 16, 16), :].astype(F32)
+    extended[pl.ds(16, length), :] = own[...].astype(F32)
+    now = docs[...].astype(F32)
+    earlier = jnp.where(sp_index == 0, -1.0, docs_before[:, pl.ds(length - 128, 128)].astype(F32))
+    line = jnp.broadcast_to(jnp.concatenate([earlier, now], axis=1), (8, length + 128))
+    count = jnp.ones((8, length), F32)
+    for offset in range(1, 16):
+        count = count + (pltpu.roll(line, offset, 1)[:, 128:] == line[:, 128:]).astype(F32)
+    eighth = jnp.full((8, width), 0.125, F32)
+    count = lax.dot_general(count, eighth, (((0,), (0,)), ((), ())), preferred_element_type=F32)
+    count = jnp.minimum(count, span.astype(F32))
+    values = own[...].astype(F32)
+    totals = values
+    for offset in range(1, 16):
+        totals = totals + jnp.where(count > offset, extended[pl.ds(16 - offset, length), :], 0.0)
+    diff = (totals / count - values).astype(BF16)
+    mixed = jnp.dot(diff, weight[0], preferred_element_type=F32)
+    pooled = (mixed * gain[...]).astype(BF16)
+    for j in range(16):
+        out[j] = pooled
 
 
 def split(value):
@@ -232,7 +247,24 @@
     where = lax.dynamic_slice(
         jnp.asarray(tables()), (lax.axis_index("c"), lax.axis_index(TP), 0), (1, 1, 40)
     ).reshape(40)
-    pooled = pool(pool_in, docs, pool_weight, pool_gain)
+    where = where.at[SP_INDEX].set(lax.axis_index(SP))
+    onward = [(i, i + 1) for i in range(n_exp - 1)]
+    before = lax.ppermute(pool_in, SP, onward)
+    docs_before = lax.ppermute(docs.reshape(1, length), SP, onward)
+    pooled = call(
+        pool,
+        [shape(16, *pool_in.shape)],
+        where,
+        pool_in,
+        before,
+        docs.reshape(1, length),
+        docs_before,
+        pool_weight,
+        pool_gain.reshape(1, -1),
+        flops=2**23,
+        scratch=[pltpu.VMEM((length + 16, pool_in.shape[1]), F32)],
+        vmem=LARGE,
+    )
     ids = routes.reshape(-1)
     onehot = (ids[:, None] == jnp.arange(n_exp)[None, :]).astype(jnp.int32)
     rank = jnp.sum(onehot * (jnp.cumsum(onehot, axis=0) - 1), axis=1)
@@ -243,10 +275,10 @@
     mix = low + jnp.where(place[:, 1][:, None] == places[None, :], route_weights[:, 1][:, None], 0.0)
     mix_high, mix_low = split(mix)
 
-    cuts_first = call(cut_first, [shape(1024, 256)] * 4, where, w_gate[0], w_up[0], flops=2**22)
-    cuts_second = call(cut_second, [shape(512, 256)] * 4, where, w_down[0], flops=2**21)
-
-    pooled_all = lax.all_to_all(jnp.broadcast_to(pooled[None], (16, *pooled.shape)), TP, 0, 0, tiled=True)
+    cuts_first = call(cut_first, [shape(1024, 256)] * 4, where, w_gate[0], w_up[0], flops=2**22, vmem=LARGE)
+    cuts_second = call(cut_second, [shape(512, 256)] * 4, where, w_down[0], flops=2**21, vmem=LARGE)
+
+    pooled_all = lax.all_to_all(pooled, TP, 0, 0, tiled=True)
     proj = jnp.einsum("gtc,gcd->td", pooled_all, out_weight.reshape(16, 128, cols), preferred_element_type=F32)
     updated = (residual.astype(F32) + proj).astype(BF16)
 

time: 214 us -> 215 us (level)
  Pallas kernels: 9.51 us -> 16.7 us
  local copies, waits for them, and re-layouts: 9.15 us -> 5.52 us
  other arithmetic: 5 us -> 2.41 us
    pallas_call x5 -> x6, Pallas kernels: 9.51 us -> 16.7 us  [call(): pl.pallas_call(kernel, out_shape=outs[0] if single else tuple(outs), in_s...]
    ppermute x6, waiting for transfers between devices: 14.5 us -> 18.1 us  [turns(): got.append(lax.ppermute(cuts[by], PLANE, pairs))]
    all_to_all x1, starting transfers between devices: 10.4 us -> 8.19 us  [layer(): lax.all_to_all(made.reshape(n_exp, cap, cols), SP, 0, 0, tiled=True)]
    ppermute x1 -> x2, starting transfers between devices: 4.92 us -> 6.97 us  [the longest x1 5.05 us: layer(): docs_before = lax.ppermute(docs.reshape(1, length), SP, onward)]
    unnamed x21 -> x25, local copies, waits for them, and re-layouts: 4.47 us -> 2.78 us
  transfers between devices with their start and end apart: 11 -> 12, of which waited for: 8 -> 9; matrix products, arithmetic and copies ran while one was open for 1% -> 1% of each run, Pallas kernels for 1% -> 3%
where the time goes in v2:
time: 215 us; the launch traced here: 214 us
  blocking collectives  73.9 us (34%)
  waiting for transfers between devices  64.1 us (30%)
  starting transfers between devices  48.9 us (23%)
  Pallas kernels  16.7 us (8%)
  local copies, waits for them, and re-layouts  5.52 us (3%)
  other arithmetic  2.41 us (1%)
  matrix products  2.2 us (1%)
    all_to_all x1, blocking collectives, layer(): lax.all_to_all(send.reshape(n_exp, cap, cols), SP, 0, 0, tiled=True)  42.9 us
    all_to_all x2, blocking collectives, a2a(): lax.all_to_all(blocks, PLANE, 0, 0, tiled=True, axis_index_groups=both_co...  31 us
    all_to_all x1, waiting for transfers between devices, layer(): lax.all_to_all(made.reshape(n_exp, cap, cols), SP, 0, 0, tiled=True)  27.8 us
    ppermute x6, waiting for transfers between devices, turns(): got.append(lax.ppermute(cuts[by], PLANE, pairs))  18.1 us
    ppermute x6, starting transfers between devices, turns(): got.append(lax.ppermute(cuts[by], PLANE, pairs))  17.3 us
    pallas_call x6, Pallas kernels, call(): pl.pallas_call(kernel, out_shape=outs[0] if single else tuple(outs), in_s...  16.7 us
    all_to_all x1, waiting for transfers between devices, layer(): pooled_all = lax.all_to_all(pooled, TP, 0, 0, tiled=True)  15.3 us
    all_to_all x2, starting transfers between devices, a2a(): lax.all_to_all(blocks, PLANE, 0, 0, tiled=True, axis_index_groups=both_co...  11.5 us
  transfers between devices with their start and end apart: 12, of which 9 were waited for; matrix products, arithmetic and copies ran while one was open for 1% of the time, Pallas kernels for 3%

profile of v2, /device:TPU:1, one launch (start us, length us, event | category | flops | bytes accessed | tf_op | source)
XLA Modules:
  0.0 214.0 jit_solution(9450795835649513102)
XLA Ops:
  0.0 5.0 %collective-permute-start.1 = (s32[1,256]{1,0:T(1,128)}, s32[1,256]{1,0:T(1,128)S(1)}, u32[]{:S(2)}, u32[]{:S(2)}) collective-permute-start(s32[1,256]{1,0:T(1,128)} %bitcast.61), channel_id=1, source_target_pairs={{0,16},{16,32},{32,48},{48,64},{64,80},{80,96},{96,112},{112,128},... | collective-permute-start | bytes 3080 | tf_op jit(solution)/shard_map/ppermute | solution.py:253
  5.1 1.9 collective-permute-start
  7.7 1.4 collective-permute-done.1.docs_before
  9.1 1.4 collective-permute-done.before
  11.1 2.5 %shard_map.127 = bf16[16,256,128]{2,1,0:T(8,128)(2,1)} custom-call(s32[40]{0:T(128)} %copy-done.2, bf16[256,128]{1,0:T(8,128)(2,1)} %own.1, bf16[256,128]{1,0:T(8,128)(2,1)} %copy-done.7, s32[1,256]{1,0:T(1,128)} %bitcast.62, s32[1,256]{1,0:T(1,128)} %copy-done.11, bf16[1,128,128]{2,1,0:T(8,128)(2,1)} %weight.1, f32[1,128]{1,0:T(1,128)} %bitcast.63), custom_call_target="tpu_custom_call" | custom-call | flops 8388608 | bytes 1215136 | tf_op jit(solution)/shard_map/pallas_call | solution.py:82
  13.7 5.0 %all-to-all-start = ((bf16[16,256,128]{2,1,0:T(8,128)(2,1)}), bf16[16,256,128]{2,1,0:T(8,128)(2,1)S(1)}, u32[]{:S(2)}, u32[]{:S(2)}) async-start(bf16[16,256,128]{2,1,0:T(8,128)(2,1)} %shard_map.127), calls=%async_computation | async-start | bytes 2097152 | tf_op jit(solution)/shard_map/all_to_all | solution.py:281
  19.1 1.2 reduce-window.6
  20.9 15.3 %all-to-all-done = bf16[16,256,128]{2,1,0:T(8,128)(2,1)S(1)} async-done(((bf16[16,256,128]{2,1,0:T(8,128)(2,1)}), bf16[16,256,128]{2,1,0:T(8,128)(2,1)S(1)}, u32[]{:S(2)}, u32[]{:S(2)}) %all-to-all-start) | async-done | bytes 1048608 | tf_op jit(solution)/shard_map/all_to_all | solution.py:281
  37.0 42.9 %all_to_all.35 = bf16[32,24,256]{2,1,0:T(8,128)(2,1)S(1)} all-to-all(bf16[32,24,256]{2,1,0:T(8,128)(2,1)S(1)} %bitcast.50), channel_id=1, replica_groups=mesh['z'=16,'c'=2,'y'=4,'x'=4] {'z','c'}, dimensions={0} | all-to-all | bytes 786432 | tf_op jit(solution)/shard_map/all_to_all | solution.py:286
  79.9 1.3 broadcast_in_dim.40
  81.2 3.6 %all-to-all-start.2 = ((bf16[4,768,256]{2,1,0:T(8,128)(2,1)}), bf16[4,768,256]{2,1,0:T(8,128)(2,1)S(1)}, u32[]{:S(2)}, u32[]{:S(2)}) async-start(bf16[4,768,256]{2,1,0:T(8,128)(2,1)} %broadcast_in_dim.40), calls=%async_computation.2 | async-start | bytes 3145728 | tf_op jit(solution)/shard_map/all_to_all | solution.py:61
  84.7 3.3 %shard_map.128 = (bf16[1024,256]{1,0:T(8,128)(2,1)}, bf16[1024,256]{1,0:T(8,128)(2,1)}, bf16[1024,256]{1,0:T(8,128)(2,1)}, bf16[1024,256]{1,0:T(8,128)(2,1)}) custom-call(s32[40]{0:T(128)} %copy-done.2, bf16[4096,128]{1,0:T(8,128)(2,1)} %bitcast.45, bf16[4096,128]{1,0:T(8,128)(2,1)} %bitcast.46), custom_call_target="tpu_custom_call" | custom-call | flops 4194304 | bytes 4194464 | tf_op jit(solution)/shard_map/pallas_call | solution.py:82
  88.0 3.7 %collective-permute-start.2 = (bf16[1024,256]{1,0:T(8,128)(2,1)}, bf16[1024,256]{1,0:T(8,128)(2,1)S(1)}, u32[]{:S(2)}, u32[]{:S(2)}) collective-permute-start(bf16[1024,256]{1,0:T(8,128)(2,1)} %get-tuple-element.26), channel_id=1, source_target_pairs={{0,1},{1,4},{4,5},{5,0},{2,3},{3,6},{6,7},{7,2},{8,9},{9,12},{12,1... | collective-permute-start | bytes 1572872 | tf_op jit(solution)/shard_map/ppermute | solution.py:68
  91.7 2.8 %collective-permute-start.3 = (bf16[1024,256]{1,0:T(8,128)(2,1)}, bf16[1024,256]{1,0:T(8,128)(2,1)}, u32[]{:S(2)}, u32[]{:S(2)}) collective-permute-start(bf16[1024,256]{1,0:T(8,128)(2,1)} %get-tuple-element.27), channel_id=1, source_target_pairs={{0,4},{1,5},{4,0},{5,1},{2,6},{3,7},{6,2},{7,3},{8,12},{9,13},{12,... | collective-permute-start | bytes 1572872 | tf_op jit(solution)/shard_map/ppermute | solution.py:68
  94.6 2.7 %collective-permute-start.4 = (bf16[1024,256]{1,0:T(8,128)(2,1)}, bf16[1024,256]{1,0:T(8,128)(2,1)}, u32[]{:S(2)}, u32[]{:S(2)}) collective-permute-start(bf16[1024,256]{1,0:T(8,128)(2,1)} %get-tuple-element.28), channel_id=1, source_target_pairs={{0,5},{1,0},{4,1},{5,4},{2,7},{3,2},{6,3},{7,6},{8,13},{9,8},{12,9... | collective-permute-start | bytes 1572872 | tf_op jit(solution)/shard_map/ppermute | solution.py:68
  97.3 6.8 %collective-permute-done.2.w1 = bf16[1024,256]{1,0:T(8,128)(2,1)S(1)} collective-permute-done((bf16[1024,256]{1,0:T(8,128)(2,1)}, bf16[1024,256]{1,0:T(8,128)(2,1)S(1)}, u32[]{:S(2)}, u32[]{:S(2)}) %collective-permute-start.2) | collective-permute-done | bytes 524320 | tf_op jit(solution)/shard_map/ppermute | solution.py:68
  104.1 6.8 %collective-permute-done.3.w2 = bf16[1024,256]{1,0:T(8,128)(2,1)} collective-permute-done((bf16[1024,256]{1,0:T(8,128)(2,1)}, bf16[1024,256]{1,0:T(8,128)(2,1)}, u32[]{:S(2)}, u32[]{:S(2)}) %collective-permute-start.3) | collective-permute-done | bytes 524320 | tf_op jit(solution)/shard_map/ppermute | solution.py:68
  111.9 4.7 %shard_map.129 = bf16[4,776,256]{2,1,0:T(8,128)(2,1)S(1)} custom-call(s32[40]{0:T(128)S(1)} %copy-done.3, bf16[4,768,256]{2,1,0:T(8,128)(2,1)S(1)} %all-to-all-done.2.got, f32[16,256]{1,0:T(8,128)S(1)} %reshape.83.gain, bf16[1024,256]{1,0:T(8,128)(2,1)S(1)} %copy-done.5, bf16[1024,256]{1,0:T(8,128)(2,1)S(1)} %collective-permute-done.2.w1, ...), custom_call_target="tpu_custom_call" | custom-call | flops 1610612736 | bytes 5275808 | tf_op jit(solution)/shard_map/pallas_call | solution.py:82
  116.6 16.0 %all_to_all.36.parts = bf16[4,776,256]{2,1,0:T(8,128)(2,1)S(1)} all-to-all(bf16[4,776,256]{2,1,0:T(8,128)(2,1)S(1)} %shard_map.129), channel_id=1, replica_groups={{0,1,4,5},{2,3,6,7},{8,9,12,13},{10,11,14,15},{21,22,25,26},{23,20,27,2..., dimensions={0} | all-to-all | bytes 3178496 | tf_op jit(solution)/shard_map/all_to_all | solution.py:61
  132.7 1.3 shard_map.130
  134.0 7.9 %all-to-all-start.4 = ((bf16[4,768,128]{2,1,0:T(8,128)(2,1)}), bf16[4,768,128]{2,1,0:T(8,128)(2,1)S(1)}, u32[]{:S(2)}, u32[]{:S(2)}) async-start(bf16[4,768,128]{2,1,0:T(8,128)(2,1)} %shard_map.130), calls=%async_computation.4 | async-start | bytes 1572864 | tf_op jit(solution)/shard_map/all_to_all | solution.py:61
  141.9 2.3 %shard_map.131 = (bf16[512,256]{1,0:T(8,128)(2,1)}, bf16[512,256]{1,0:T(8,128)(2,1)}, bf16[512,256]{1,0:T(8,128)(2,1)}, bf16[512,256]{1,0:T(8,128)(2,1)}) custom-call(s32[40]{0:T(128)} %copy-done.2, bf16[2048,256]{1,0:T(8,128)(2,1)} %bitcast.47), custom_call_target="tpu_custom_call" | custom-call | flops 2097152 | bytes 2097312 | tf_op jit(solution)/shard_map/pallas_call | solution.py:82
  144.2 1.9 collective-permute-start.5
  146.2 1.9 collective-permute-start.6
  148.1 4.3 %collective-permute-start.7 = (bf16[512,256]{1,0:T(8,128)(2,1)}, bf16[512,256]{1,0:T(8,128)(2,1)S(1)}, u32[]{:S(2)}, u32[]{:S(2)}) collective-permute-start(bf16[512,256]{1,0:T(8,128)(2,1)} %get-tuple-element.32), channel_id=1, source_target_pairs={{5,10},{6,5},{9,6},{10,9},{7,8},{4,7},{11,4},{8,11},{13,2},{14,13}... | collective-permute-start | bytes 786440 | tf_op jit(solution)/shard_map/ppermute | solution.py:68
  152.6 2.7 %collective-permute-done.6.w2 = bf16[512,256]{1,0:T(8,128)(2,1)S(1)} collective-permute-done((bf16[512,256]{1,0:T(8,128)(2,1)}, bf16[512,256]{1,0:T(8,128)(2,1)S(1)}, u32[]{:S(2)}, u32[]{:S(2)}) %collective-permute-start.6) | collective-permute-done | bytes 262176 | tf_op jit(solution)/shard_map/ppermute | solution.py:68
  155.3 1.6 collective-permute-done.7.w3
  157.8 2.5 %shard_map.132 = bf16[4,768,256]{2,1,0:T(8,128)(2,1)S(1)} custom-call(s32[40]{0:T(128)S(1)} %copy-done.4, bf16[4,768,128]{2,1,0:T(8,128)(2,1)S(1)} %all-to-all-done.4.acts, bf16[512,256]{1,0:T(8,128)(2,1)S(1)} %copy-done.1, bf16[512,256]{1,0:T(8,128)(2,1)S(1)} %collective-permute-done.5.w1, bf16[512,256]{1,0:T(8,128)(2,1)S(1)} %collective-permute-done.6.w2, ...), custom_call_target="tpu_custom_call" | custom-call | flops 805306368 | bytes 3408032 | tf_op jit(solution)/shard_map/pallas_call | solution.py:82
  160.4 15.0 %all_to_all.37 = bf16[4,768,256]{2,1,0:T(8,128)(2,1)S(1)} all-to-all(bf16[4,768,256]{2,1,0:T(8,128)(2,1)S(1)} %shard_map.132), channel_id=1, replica_groups={{5,6,9,10},{7,4,11,8},{13,14,1,2},{15,12,3,0},{16,17,20,21},{18,19,22,2..., dimensions={0} | all-to-all | bytes 3145728 | tf_op jit(solution)/shard_map/all_to_all | solution.py:61
  176.5 8.2 %all-to-all-start.6 = ((bf16[32,24,256]{2,1,0:T(8,128)(2,1)}), bf16[32,24,256]{2,1,0:T(8,128)(2,1)S(1)}, u32[]{:S(2)}, u32[]{:S(2)}) async-start(bf16[32,24,256]{2,1,0:T(8,128)(2,1)} %bitcast.16), calls=%async_computation.6 | async-start | bytes 786432 | tf_op jit(solution)/shard_map/all_to_all | solution.py:290
  184.7 27.8 %all-to-all-done.6 = bf16[32,24,256]{2,1,0:T(8,128)(2,1)S(1)} async-done(((bf16[32,24,256]{2,1,0:T(8,128)(2,1)}), bf16[32,24,256]{2,1,0:T(8,128)(2,1)S(1)}, u32[]{:S(2)}, u32[]{:S(2)}) %all-to-all-start.6) | async-done | bytes 393248 | tf_op jit(solution)/shard_map/all_to_all | solution.py:290
  212.9 1.1 fusion.3
  (48 shorter events, 6.8 us)
Async XLA Ops:
  0.0 36.2 %copy-start = (bf16[2048,256]{1,0:T(8,128)(2,1)S(1)}, bf16[2048,256]{1,0:T(8,128)(2,1)}, u32[]{:S(2)}) copy-start(bf16[2048,256]{1,0:T(8,128)(2,1)} %param.20) | copy-start | bytes 3145732
  0.0 9.1 %collective-permute-start.1 = (s32[1,256]{1,0:T(1,128)}, s32[1,256]{1,0:T(1,128)S(1)}, u32[]{:S(2)}, u32[]{:S(2)}) collective-permute-start(s32[1,256]{1,0:T(1,128)} %bitcast.61), channel_id=1, source_target_pairs={{0,16},{16,32},{32,48},{48,64},{64,80},{80,96},{96,112},{112,128},... | collective-permute-start | bytes 3080 | tf_op jit(solution)/shard_map/ppermute | solution.py:253
  5.1 5.4 %collective-permute-start = (bf16[256,128]{1,0:T(8,128)(2,1)}, bf16[256,128]{1,0:T(8,128)(2,1)S(1)}, u32[]{:S(2)}, u32[]{:S(2)}) collective-permute-start(bf16[256,128]{1,0:T(8,128)(2,1)} %own.1), channel_id=1, source_target_pairs={{0,16},{16,32},{32,48},{48,64},{64,80},{80,96},{96,112},{112,128},... | collective-permute-start | bytes 196616 | tf_op jit(solution)/shard_map/ppermute | solution.py:252
  7.7 2.8 %copy-start.2 = (s32[40]{0:T(128)}, s32[40]{0:T(128)S(1)}, u32[]{:S(2)}) copy-start(s32[40]{0:T(128)S(1)} %constant_dynamic-update-slice_fusion.where) | copy-start | bytes 484
  9.1 1.4 copy-start.11
  10.5 0.6 copy-start.7
  11.1 7.6 %copy-start.9 = (s32[256,2]{0,1:T(2,128)S(1)}, s32[256,2]{0,1:T(2,128)}, u32[]{:S(2)}) copy-start(s32[256,2]{0,1:T(2,128)} %param.22) | copy-start | bytes 6148
  13.7 22.6 %copy-start.6 = (bf16[256,256]{1,0:T(8,128)(2,1)S(1)}, bf16[256,256]{1,0:T(8,128)(2,1)}, u32[]{:S(2)}) copy-start(bf16[256,256]{1,0:T(8,128)(2,1)} %param.15) | copy-start | bytes 393220
  13.7 22.6 %all-to-all-start = ((bf16[16,256,128]{2,1,0:T(8,128)(2,1)}), bf16[16,256,128]{2,1,0:T(8,128)(2,1)S(1)}, u32[]{:S(2)}, u32[]{:S(2)}) async-start(bf16[16,256,128]{2,1,0:T(8,128)(2,1)} %shard_map.127), calls=%async_computation | async-start | bytes 2097152 | tf_op jit(solution)/shard_map/all_to_all | solution.py:281
  81.2 29.7 %all-to-all-start.2 = ((bf16[4,768,256]{2,1,0:T(8,128)(2,1)}), bf16[4,768,256]{2,1,0:T(8,128)(2,1)S(1)}, u32[]{:S(2)}, u32[]{:S(2)}) async-start(bf16[4,768,256]{2,1,0:T(8,128)(2,1)} %broadcast_in_dim.40), calls=%async_computation.2 | async-start | bytes 3145728 | tf_op jit(solution)/shard_map/all_to_all | solution.py:61
  84.7 12.5 %copy-start.8 = (f32[4096]{0:T(1024)S(1)}, f32[4096]{0:T(1024)}, u32[]{:S(2)}) copy-start(f32[4096]{0:T(1024)} %param.21) | copy-start | bytes 49156
  84.7 26.2 %copy-start.3 = (s32[40]{0:T(128)S(1)}, s32[40]{0:T(128)}, u32[]{:S(2)}) copy-start(s32[40]{0:T(128)} %copy-done.2) | copy-start | bytes 484
  88.0 16.1 %collective-permute-start.2 = (bf16[1024,256]{1,0:T(8,128)(2,1)}, bf16[1024,256]{1,0:T(8,128)(2,1)S(1)}, u32[]{:S(2)}, u32[]{:S(2)}) collective-permute-start(bf16[1024,256]{1,0:T(8,128)(2,1)} %get-tuple-element.26), channel_id=1, source_target_pairs={{0,1},{1,4},{4,5},{5,0},{2,3},{3,6},{6,7},{7,2},{8,9},{9,12},{12,1... | collective-permute-start | bytes 1572872 | tf_op jit(solution)/shard_map/ppermute | solution.py:68
  91.7 19.1 %collective-permute-start.3 = (bf16[1024,256]{1,0:T(8,128)(2,1)}, bf16[1024,256]{1,0:T(8,128)(2,1)}, u32[]{:S(2)}, u32[]{:S(2)}) collective-permute-start(bf16[1024,256]{1,0:T(8,128)(2,1)} %get-tuple-element.27), channel_id=1, source_target_pairs={{0,4},{1,5},{4,0},{5,1},{2,6},{3,7},{6,2},{7,3},{8,12},{9,13},{12,... | collective-permute-start | bytes 1572872 | tf_op jit(solution)/shard_map/ppermute | solution.py:68
  94.6 16.3 %collective-permute-start.4 = (bf16[1024,256]{1,0:T(8,128)(2,1)}, bf16[1024,256]{1,0:T(8,128)(2,1)}, u32[]{:S(2)}, u32[]{:S(2)}) collective-permute-start(bf16[1024,256]{1,0:T(8,128)(2,1)} %get-tuple-element.28), channel_id=1, source_target_pairs={{0,5},{1,0},{4,1},{5,4},{2,7},{3,2},{6,3},{7,6},{8,13},{9,8},{12,9... | collective-permute-start | bytes 1572872 | tf_op jit(solution)/shard_map/ppermute | solution.py:68
  110.9 1.0 copy-start.5
  134.0 22.9 %copy-start.4 = (s32[40]{0:T(128)S(1)}, s32[40]{0:T(128)}, u32[]{:S(2)}) copy-start(s32[40]{0:T(128)} %copy-done.2) | copy-start | bytes 484
  134.0 22.9 %all-to-all-start.4 = ((bf16[4,768,128]{2,1,0:T(8,128)(2,1)}), bf16[4,768,128]{2,1,0:T(8,128)(2,1)S(1)}, u32[]{:S(2)}, u32[]{:S(2)}) async-start(bf16[4,768,128]{2,1,0:T(8,128)(2,1)} %shard_map.130), calls=%async_computation.4 | async-start | bytes 1572864 | tf_op jit(solution)/shard_map/all_to_all | solution.py:61
  144.2 8.3 %collective-permute-start.5 = (bf16[512,256]{1,0:T(8,128)(2,1)}, bf16[512,256]{1,0:T(8,128)(2,1)S(1)}, u32[]{:S(2)}, u32[]{:S(2)}) collective-permute-start(bf16[512,256]{1,0:T(8,128)(2,1)} %get-tuple-element.30), channel_id=1, source_target_pairs={{5,6},{6,9},{9,10},{10,5},{7,4},{4,11},{11,8},{8,7},{13,14},{14,1}... | collective-permute-start | bytes 786440 | tf_op jit(solution)/shard_map/ppermute | solution.py:68
  146.2 9.1 %collective-permute-start.6 = (bf16[512,256]{1,0:T(8,128)(2,1)}, bf16[512,256]{1,0:T(8,128)(2,1)S(1)}, u32[]{:S(2)}, u32[]{:S(2)}) collective-permute-start(bf16[512,256]{1,0:T(8,128)(2,1)} %get-tuple-element.31), channel_id=1, source_target_pairs={{5,9},{6,10},{9,5},{10,6},{7,11},{4,8},{11,7},{8,4},{13,1},{14,2},... | collective-permute-start | bytes 786440 | tf_op jit(solution)/shard_map/ppermute | solution.py:68
  148.1 8.8 %collective-permute-start.7 = (bf16[512,256]{1,0:T(8,128)(2,1)}, bf16[512,256]{1,0:T(8,128)(2,1)S(1)}, u32[]{:S(2)}, u32[]{:S(2)}) collective-permute-start(bf16[512,256]{1,0:T(8,128)(2,1)} %get-tuple-element.32), channel_id=1, source_target_pairs={{5,10},{6,5},{9,6},{10,9},{7,8},{4,7},{11,4},{8,11},{13,2},{14,13}... | collective-permute-start | bytes 786440 | tf_op jit(solution)/shard_map/ppermute | solution.py:68
  156.9 1.0 copy-start.1
  175.4 9.3 %copy-start.10 = (f32[256,2]{0,1:T(2,128)S(1)}, f32[256,2]{0,1:T(2,128)}, u32[]{:S(2)}) copy-start(f32[256,2]{0,1:T(2,128)} %param.23) | copy-start | bytes 6148
  176.5 36.1 %all-to-all-start.6 = ((bf16[32,24,256]{2,1,0:T(8,128)(2,1)}), bf16[32,24,256]{2,1,0:T(8,128)(2,1)S(1)}, u32[]{:S(2)}, u32[]{:S(2)}) async-start(bf16[32,24,256]{2,1,0:T(8,128)(2,1)} %bitcast.16), calls=%async_computation.6 | async-start | bytes 786432 | tf_op jit(solution)/shard_map/all_to_all | solution.py:290

commit v3 on v2

--- a/solution.py
+++ b/solution.py
@@ -31,6 +31,20 @@
 SCATTER = [blocks_of(0), blocks_of(1)]
 
 
+HALVES = [
+    [[y * 4 + x for y in (v, v + 1) for x in range(4)] for v in (0, 2)],
+    [[y * 4 + x for y in range(4) for x in (h, h + 1)] for h in (0, 2)],
+]
+
+
+def partner(core, member):
+    y, x = divmod(member, 4)
+    return (3 - y) * 4 + x if core == 0 else y * 4 + 3 - x
+
+
+PARTNERS = [(16 * core + m, 16 * core + partner(core, m)) for core in range(2) for m in range(16)]
+
+
 def both_cores(groups):
     return groups[0] + [[16 + m for m in group] for group in groups[1]]
 
@@ -40,7 +54,7 @@
 
 
 def tables():
-    table = np.zeros((2, 16, 40), np.int32)
+    table = np.zeros((2, 16, 56), np.int32)
     for core in range(2):
         for me in range(16):
             gather, scatter = group_with(GATHER[core], me), group_with(SCATTER[core], me)
@@ -50,11 +64,13 @@
                 row += group_with(GATHER[core], scatter[(p + by) % 4])
             for by in range(4):
                 row += group_with(SCATTER[core], gather[(q + by) % 4])
+            halves = group_with(HALVES[core], me) + group_with(HALVES[core], partner(core, me))
             table[core, me, :39] = row + gather + [p, q, 2 ** (1 + me % 4)]
+            table[core, me, 40:] = halves
     return table
 
 
-FEATURES, HIDDEN, GAINS, IN_SCATTER, IN_GATHER, SPAN, SP_INDEX = 0, 16, 32, 36, 37, 38, 39
+FEATURES, HIDDEN, GAINS, IN_SCATTER, IN_GATHER, SPAN, SP_INDEX, CHANNELS, OTHERS = 0, 16, 32, 36, 37, 38, 39, 40, 48
 
 
 def a2a(blocks, groups):
@@ -62,10 +78,10 @@
 
 
 def turns(cuts, groups):
-    got = [cuts[0]]
+    got = []
     for by in range(1, 4):
         pairs = [(g[i], g[(i + by) % 4]) for g in both_cores(groups) for i in range(4)]
-        got.append(lax.ppermute(cuts[by], PLANE, pairs))
+        got.append(lax.ppermute(cuts[by - 1], PLANE, pairs))
     return got
 
 
@@ -90,28 +106,61 @@
     )(*args)
 
 
+def cut_out(where, weight, out):
+    for i in range(8):
+        src = pl.ds(pl.multiple_of(where[OTHERS + i] * 128, 128), 128)
+        out[pl.ds(128 * i, 128), :] = weight[src, :]
+
+
 def cut_first(where, gate, up, *outs):
-    for by in range(4):
+    for by in range(1, 4):
         for i in range(4):
             block = where[FEATURES + 4 * by + i]
             src = pl.ds(pl.multiple_of(block * 256, 256), 256)
-            outs[by][pl.ds(256 * i, 256), pl.ds(0, 128)] = gate[src, :]
-            outs[by][pl.ds(256 * i, 256), pl.ds(128, 128)] = up[src, :]
+            outs[by - 1][pl.ds(256 * i, 256), pl.ds(0, 128)] = gate[src, :]
+            outs[by - 1][pl.ds(256 * i, 256), pl.ds(128, 128)] = up[src, :]
 
 
 def cut_second(where, down, *outs):
-    for by in range(4):
+    for by in range(1, 4):
         for i in range(4):
             block = where[HIDDEN + 4 * by + i]
-            outs[by][pl.ds(128 * i, 128), :] = down[pl.ds(pl.multiple_of(block * 128, 128), 128), :]
+            outs[by - 1][pl.ds(128 * i, 128), :] = down[pl.ds(pl.multiple_of(block * 128, 128), 128), :]
+
+
+def project(where, pooled, weight, theirs, residual, mine_out, theirs_out):
+    rows = [weight[pl.ds(pl.multiple_of(where[CHANNELS + i] * 128, 128), 128), :] for i in range(8)]
+    total = residual[...].astype(F32)
+    other = jnp.zeros(total.shape, F32)
+    for i in range(4):
+        part = jnp.concatenate([pooled[2 * i], pooled[2 * i + 1]], axis=1)
+        total = total + jnp.dot(part, jnp.concatenate(rows[2 * i : 2 * i + 2], axis=0), preferred_element_type=F32)
+        other = other + jnp.dot(part, theirs[pl.ds(256 * i, 256), :], preferred_element_type=F32)
+    mine_out[...] = total
+    theirs_out[...] = other.astype(BF16)
+
+
+def finish(mine, received, place, out, send):
+    updated = (mine[...] + received[...].astype(F32)).astype(BF16)
+    out[...] = updated
+    slots, length = send.shape[0], updated.shape[0]
+    for i in range(slots // 256):
+        slot = lax.broadcasted_iota(jnp.int32, (256, length), 0) + 256 * i
+        take = ((place[pl.ds(0, 1), :] == slot) | (place[pl.ds(1, 1), :] == slot)).astype(F32).astype(BF16)
+        send[pl.ds(256 * i, 256), :] = jnp.dot(take, updated, preferred_element_type=F32).astype(BF16)
 
 
 def fetches(sources, held, arrived):
-    return [pltpu.make_async_copy(w, held.at[by], arrived.at[by]) for by, w in enumerate(sources)]
-
-
-def gate_up(where, got, gain, w0, w1, w2, w3, out, rows, held, arrived):
-    copies = fetches((w0, w1, w2, w3), held, arrived)
+    return [pltpu.make_async_copy(w, held.at[by + 1], arrived.at[by]) for by, w in enumerate(sources)]
+
+
+def gate_up(where, got, gain, gate, up, w1, w2, w3, out, rows, held, arrived):
+    copies = fetches((w1, w2, w3), held, arrived)
+    for i in range(4):
+        src = pl.ds(pl.multiple_of(where[FEATURES + i] * 256, 256), 256)
+        to = held.at[0, pl.ds(256 * i, 256)]
+        copies.append(pltpu.make_async_copy(gate.at[src], to.at[:, pl.ds(0, 128)], arrived.at[3 + 2 * i]))
+        copies.append(pltpu.make_async_copy(up.at[src], to.at[:, pl.ds(128, 128)], arrived.at[4 + 2 * i]))
     for copy in copies:
         copy.start()
     count = got.shape[1]
@@ -133,8 +182,9 @@
         for j in range(4):
             out[j, pl.ds(count + 2 * i, 1), :] = high[:1]
             out[j, pl.ds(count + 2 * i + 1, 1), :] = low[:1]
-    for by, copy in enumerate(copies):
-        copy.wait()
+    for by in range(4):
+        for copy in copies[3:] if by == 0 else copies[by - 1 : by]:
+            copy.wait()
         to = lax.rem(where[IN_SCATTER] + 4 - by, 4)
         out[to, pl.ds(count + 2 * tiles, 8 - 2 * tiles), :] = jnp.zeros((8 - 2 * tiles, 256), BF16)
         for i in range(tiles):
@@ -162,15 +212,19 @@
             out[j, tile, :] = act
 
 
-def down_rows(where, acts, w0, w1, w2, w3, out, rows, held, arrived):
-    copies = fetches((w0, w1, w2, w3), held, arrived)
+def down_rows(where, acts, down, w1, w2, w3, out, rows, held, arrived):
+    copies = fetches((w1, w2, w3), held, arrived)
+    for i in range(4):
+        src = pl.ds(pl.multiple_of(where[HIDDEN + i] * 128, 128), 128)
+        copies.append(pltpu.make_async_copy(down.at[src], held.at[0, pl.ds(128 * i, 128)], arrived.at[3 + i]))
     for copy in copies:
         copy.start()
     count = acts.shape[1]
     for h in range(4):
         rows[:, pl.ds(128 * h, 128)] = acts[h]
-    for by, copy in enumerate(copies):
-        copy.wait()
+    for by in range(4):
+        for copy in copies[3:] if by == 0 else copies[by - 1 : by]:
+            copy.wait()
         to = lax.rem(where[IN_GATHER] + 4 - by, 4)
         for i in range(count // 256):
             tile = pl.ds(256 * i, 256)
@@ -188,8 +242,8 @@
         gain,
         *first,
         flops=2**21 * count,
-        scratch=[pltpu.VMEM((count, 1024), BF16), pltpu.VMEM((4, 1024, 256), BF16), pltpu.SemaphoreType.DMA((4,))],
-        fetched=4,
+        scratch=[pltpu.VMEM((count, 1024), BF16), pltpu.VMEM((4, 1024, 256), BF16), pltpu.SemaphoreType.DMA((11,))],
+        fetched=5,
     )
     parts = a2a(part, SCATTER)
     acts = a2a(call(activate, [shape(4, count, 128)], parts, flops=2**16 * count, tables=0), SCATTER)
@@ -200,7 +254,7 @@
         acts,
         *second,
         flops=2**20 * count,
-        scratch=[pltpu.VMEM((count, 512), BF16), pltpu.VMEM((4, 512, 256), BF16), pltpu.SemaphoreType.DMA((4,))],
+        scratch=[pltpu.VMEM((count, 512), BF16), pltpu.VMEM((4, 512, 256), BF16), pltpu.SemaphoreType.DMA((7,))],
         fetched=4,
     )
     parts = a2a(part, GATHER)
@@ -228,7 +282,7 @@
     diff = (totals / count - values).astype(BF16)
     mixed = jnp.dot(diff, weight[0], preferred_element_type=F32)
     pooled = (mixed * gain[...]).astype(BF16)
-    for j in range(16):
+    for j in range(8):
         out[j] = pooled
 
 
@@ -245,15 +299,15 @@
     cap = length * TOPK * 3 // (2 * n_exp)
     slots = n_exp * cap
     where = lax.dynamic_slice(
-        jnp.asarray(tables()), (lax.axis_index("c"), lax.axis_index(TP), 0), (1, 1, 40)
-    ).reshape(40)
+        jnp.asarray(tables()), (lax.axis_index("c"), lax.axis_index(TP), 0), (1, 1, 56)
+    ).reshape(56)
     where = where.at[SP_INDEX].set(lax.axis_index(SP))
     onward = [(i, i + 1) for i in range(n_exp - 1)]
     before = lax.ppermute(pool_in, SP, onward)
     docs_before = lax.ppermute(docs.reshape(1, length), SP, onward)
     pooled = call(
         pool,
-        [shape(16, *pool_in.shape)],
+        [shape(8, *pool_in.shape)],
         where,
         pool_in,
         before,
@@ -270,22 +324,33 @@
     rank = jnp.sum(onehot * (jnp.cumsum(onehot, axis=0) - 1), axis=1)
     place = (ids * cap + rank).reshape(length, TOPK)
     places = jnp.arange(slots)
-    take = (place[:, 0][None, :] == places[:, None]) | (place[:, 1][None, :] == places[:, None])
     low = jnp.where(place[:, 0][:, None] == places[None, :], route_weights[:, 0][:, None], 0.0)
     mix = low + jnp.where(place[:, 1][:, None] == places[None, :], route_weights[:, 1][:, None], 0.0)
     mix_high, mix_low = split(mix)
 
-    cuts_first = call(cut_first, [shape(1024, 256)] * 4, where, w_gate[0], w_up[0], flops=2**22, vmem=LARGE)
-    cuts_second = call(cut_second, [shape(512, 256)] * 4, where, w_down[0], flops=2**21, vmem=LARGE)
-
-    pooled_all = lax.all_to_all(pooled, TP, 0, 0, tiled=True)
-    proj = jnp.einsum("gtc,gcd->td", pooled_all, out_weight.reshape(16, 128, cols), preferred_element_type=F32)
-    updated = (residual.astype(F32) + proj).astype(BF16)
-
-    send = jnp.dot(take.astype(BF16), updated, preferred_element_type=F32).astype(BF16)
+    cuts_first = call(cut_first, [shape(1024, 256)] * 3, where, w_gate[0], w_up[0], flops=2**22, vmem=LARGE)
+    cuts_second = call(cut_second, [shape(512, 256)] * 3, where, w_down[0], flops=2**21, vmem=LARGE)
+
+    cut_theirs = call(cut_out, [shape(1024, cols)], where, out_weight, flops=2**20, vmem=LARGE)
+    theirs = lax.ppermute(cut_theirs, PLANE, PARTNERS)
+    pooled_half = a2a(pooled, HALVES)
+    mine, other = call(
+        project,
+        [shape(length, cols, dtype=F32), shape(length, cols)],
+        where,
+        pooled_half,
+        out_weight,
+        theirs,
+        residual,
+        flops=2**29,
+    )
+    received = lax.ppermute(other, PLANE, PARTNERS)
+    updated, send = call(
+        finish, [shape(length, cols), shape(slots, cols)], mine, received, place.T, flops=2**27, tables=0
+    )
     arrived = lax.all_to_all(send.reshape(n_exp, cap, cols), SP, 0, 0, tiled=True).reshape(slots, cols)
-    first = turns(cuts_first, SCATTER)
-    second = turns(cuts_second, GATHER)
+    first = [w_gate[0], w_up[0], *turns(cuts_first, SCATTER)]
+    second = [w_down[0], *turns(cuts_second, GATHER)]
     made = experts(arrived, first, second, where, norm_gain.reshape(16, 256))
     back = lax.all_to_all(made.reshape(n_exp, cap, cols), SP, 0, 0, tiled=True).reshape(slots, cols)
     summed = jnp.dot(mix_high, back, preferred_element_type=F32) + jnp.dot(

time: 215 us -> 221 us (1.028)
  starting transfers between devices: 48.9 us -> 56.3 us
  waiting for transfers between devices: 64.1 us -> 58.2 us
  Pallas kernels: 16.7 us -> 20.1 us
    all_to_all x1 -> x0, waiting for transfers between devices: 15.3 us -> none  [layer(): pooled_all = lax.all_to_all(pooled, TP, 0, 0, tiled=True)]
    ppermute x6 -> x8, starting transfers between devices: 17.3 us -> 25.2 us  [the longest x6 17.1 us: turns(): got.append(lax.ppermute(cuts[by - 1], PLANE, pairs))]
    all_to_all x2 -> x3, waiting for transfers between devices: 0.01 us -> 7.75 us  [a2a(): lax.all_to_all(blocks, PLANE, 0, 0, tiled=True, axis_index_groups=both_co...]
    all_to_all x1 -> x0, starting transfers between devices: 5 us -> none  [layer(): pooled_all = lax.all_to_all(pooled, TP, 0, 0, tiled=True)]
    all_to_all x2 -> x3, starting transfers between devices: 11.5 us -> 15.6 us  [a2a(): lax.all_to_all(blocks, PLANE, 0, 0, tiled=True, axis_index_groups=both_co...]
    ppermute x6 -> x8, waiting for transfers between devices: 18.1 us -> 21.9 us  [the longest x6 18.6 us: turns(): got.append(lax.ppermute(cuts[by - 1], PLANE, pairs))]
    pallas_call x6 -> x9, Pallas kernels: 16.7 us -> 20.1 us  [call(): pl.pallas_call(kernel, out_shape=outs[0] if single else tuple(outs), in_s...]
    ppermute x1, starting transfers between devices: 1.92 us -> 5.05 us  [layer(): before = lax.ppermute(pool_in, SP, onward)]
  transfers between devices with their start and end apart: 12 -> 14, of which waited for: 9 -> 9; matrix products, arithmetic and copies ran while one was open for 1% -> 1% of each run, Pallas kernels for 3% -> 4%
where the time goes in v3:
time: 221 us; the launch traced here: 220 us
  blocking collectives  76.1 us (34%)
  waiting for transfers between devices  58.2 us (26%)
  starting transfers between devices  56.3 us (25%)
  Pallas kernels  20.1 us (9%)
  local copies, waits for them, and re-layouts  5.33 us (2%)
  other arithmetic  3.09 us (1%)
    all_to_all x1, blocking collectives, layer(): lax.all_to_all(send.reshape(n_exp, cap, cols), SP, 0, 0, tiled=True)  44.9 us
    all_to_all x2, blocking collectives, a2a(): lax.all_to_all(blocks, PLANE, 0, 0, tiled=True, axis_index_groups=both_co...  31.2 us
    all_to_all x1, waiting for transfers between devices, layer(): lax.all_to_all(made.reshape(n_exp, cap, cols), SP, 0, 0, tiled=True)  27.8 us
    pallas_call x9, Pallas kernels, call(): pl.pallas_call(kernel, out_shape=outs[0] if single else tuple(outs), in_s...  20.1 us
    ppermute x6, waiting for transfers between devices, turns(): got.append(lax.ppermute(cuts[by - 1], PLANE, pairs))  18.6 us
    ppermute x6, starting transfers between devices, turns(): got.append(lax.ppermute(cuts[by - 1], PLANE, pairs))  17.1 us
    all_to_all x3, starting transfers between devices, a2a(): lax.all_to_all(blocks, PLANE, 0, 0, tiled=True, axis_index_groups=both_co...  15.6 us
    all_to_all x1, starting transfers between devices, layer(): lax.all_to_all(made.reshape(n_exp, cap, cols), SP, 0, 0, tiled=True)  8.1 us
  transfers between devices with their start and end apart: 14, of which 9 were waited for; matrix products, arithmetic and copies ran while one was open for 1% of the time, Pallas kernels for 4%

profile of v3, /device:TPU:1, one launch (start us, length us, event | category | flops | bytes accessed | tf_op | source)
XLA Modules:
  0.0 220.2 jit_solution(1417616945374936795)
XLA Ops:
  0.0 5.0 %collective-permute-start = (bf16[256,128]{1,0:T(8,128)(2,1)}, bf16[256,128]{1,0:T(8,128)(2,1)S(1)}, u32[]{:S(2)}, u32[]{:S(2)}) collective-permute-start(bf16[256,128]{1,0:T(8,128)(2,1)} %own.1), channel_id=1, source_target_pairs={{0,16},{16,32},{32,48},{48,64},{64,80},{80,96},{96,112},{112,128},... | collective-permute-start | bytes 196616 | tf_op jit(solution)/shard_map/ppermute | solution.py:306
  6.4 2.1 shard_map.128
  8.5 4.5 %collective-permute-start.2 = (bf16[1024,256]{1,0:T(8,128)(2,1)}, bf16[1024,256]{1,0:T(8,128)(2,1)S(1)}, u32[]{:S(2)}, u32[]{:S(2)}) collective-permute-start(bf16[1024,256]{1,0:T(8,128)(2,1)} %shard_map.128), channel_id=1, source_target_pairs={{0,12},{1,13},{2,14},{3,15},{4,8},{5,9},{6,10},{7,11},{8,4},{9,5},... | collective-permute-start | bytes 1572872 | tf_op jit(solution)/shard_map/ppermute | solution.py:335
  13.0 2.5 %collective-permute-start.1 = (s32[1,256]{1,0:T(1,128)S(1)}, s32[1,256]{1,0:T(1,128)S(1)}, u32[]{:S(2)}, u32[]{:S(2)}) collective-permute-start(s32[1,256]{1,0:T(1,128)S(1)} %bitcast.46), channel_id=1, source_target_pairs={{0,16},{16,32},{32,48},{48,64},{64,80},{80,96},{96,112},{112,128},... | collective-permute-start | bytes 3080 | tf_op jit(solution)/shard_map/ppermute | solution.py:307
  16.8 2.3 %shard_map.127 = bf16[8,256,128]{2,1,0:T(8,128)(2,1)} custom-call(s32[56]{0:T(128)} %copy-done.5, bf16[256,128]{1,0:T(8,128)(2,1)} %own.1, bf16[256,128]{1,0:T(8,128)(2,1)} %copy-done.9, s32[1,256]{1,0:T(1,128)} %bitcast.45, s32[1,256]{1,0:T(1,128)} %copy-done.14, bf16[1,128,128]{2,1,0:T(8,128)(2,1)} %weight.3, f32[1,128]{1,0:T(1,128)} %bitcast.55), custom_call_target="tpu_custom_call" | custom-call | flops 8388608 | bytes 690912 | tf_op jit(solution)/shard_map/pallas_call | solution.py:98
  19.1 4.1 %all-to-all-start = ((bf16[8,256,128]{2,1,0:T(8,128)(2,1)}), bf16[8,256,128]{2,1,0:T(8,128)(2,1)S(1)}, u32[]{:S(2)}, u32[]{:S(2)}) async-start(bf16[8,256,128]{2,1,0:T(8,128)(2,1)} %shard_map.127), calls=%async_computation | async-start | bytes 1048576 | tf_op jit(solution)/shard_map/all_to_all | solution.py:77
  25.4 7.7 %all-to-all-done.pooled = bf16[8,256,128]{2,1,0:T(8,128)(2,1)S(1)} async-done(((bf16[8,256,128]{2,1,0:T(8,128)(2,1)}), bf16[8,256,128]{2,1,0:T(8,128)(2,1)S(1)}, u32[]{:S(2)}, u32[]{:S(2)}) %all-to-all-start) | async-done | bytes 524320 | tf_op jit(solution)/shard_map/all_to_all | solution.py:77
  34.2 3.6 %collective-permute-start.3 = (bf16[256,256]{1,0:T(8,128)(2,1)S(1)}, bf16[256,256]{1,0:T(8,128)(2,1)S(1)}, u32[]{:S(2)}, u32[]{:S(2)}) collective-permute-start(bf16[256,256]{1,0:T(8,128)(2,1)S(1)} %get-tuple-element.28), channel_id=1, source_target_pairs={{0,12},{1,13},{2,14},{3,15},{4,8},{5,9},{6,10},{7,11},{8,4},{9,5},... | collective-permute-start | bytes 393224 | tf_op jit(solution)/shard_map/ppermute | solution.py:347
  37.8 3.3 %collective-permute-done.3.received = bf16[256,256]{1,0:T(8,128)(2,1)S(1)} collective-permute-done((bf16[256,256]{1,0:T(8,128)(2,1)S(1)}, bf16[256,256]{1,0:T(8,128)(2,1)S(1)}, u32[]{:S(2)}, u32[]{:S(2)}) %collective-permute-start.3) | collective-permute-done | bytes 131104 | tf_op jit(solution)/shard_map/ppermute | solution.py:347
  41.4 44.9 %all_to_all.35 = bf16[32,24,256]{2,1,0:T(8,128)(2,1)S(1)} all-to-all(bf16[32,24,256]{2,1,0:T(8,128)(2,1)S(1)} %bitcast.40), channel_id=1, replica_groups=mesh['z'=16,'c'=2,'y'=4,'x'=4] {'z','c'}, dimensions={0} | all-to-all | bytes 786432 | tf_op jit(solution)/shard_map/all_to_all | solution.py:351
  86.3 1.3 broadcast_in_dim.38
  87.5 3.6 %all-to-all-start.2 = ((bf16[4,768,256]{2,1,0:T(8,128)(2,1)}), bf16[4,768,256]{2,1,0:T(8,128)(2,1)S(1)}, u32[]{:S(2)}, u32[]{:S(2)}) async-start(bf16[4,768,256]{2,1,0:T(8,128)(2,1)} %broadcast_in_dim.38), calls=%async_computation.2 | async-start | bytes 3145728 | tf_op jit(solution)/shard_map/all_to_all | solution.py:77
  91.1 3.1 %shard_map.131 = (bf16[1024,256]{1,0:T(8,128)(2,1)}, bf16[1024,256]{1,0:T(8,128)(2,1)}, bf16[1024,256]{1,0:T(8,128)(2,1)}) custom-call(s32[56]{0:T(128)} %copy-done.5, bf16[4096,128]{1,0:T(8,128)(2,1)} %bitcast.36, bf16[4096,128]{1,0:T(8,128)(2,1)} %bitcast.38), custom_call_target="tpu_custom_call" | custom-call | flops 4194304 | bytes 3670240 | tf_op jit(solution)/shard_map/pallas_call | solution.py:98
  94.2 3.6 %collective-permute-start.4 = (bf16[1024,256]{1,0:T(8,128)(2,1)}, bf16[1024,256]{1,0:T(8,128)(2,1)S(1)}, u32[]{:S(2)}, u32[]{:S(2)}) collective-permute-start(bf16[1024,256]{1,0:T(8,128)(2,1)} %get-tuple-element.31), channel_id=1, source_target_pairs={{0,1},{1,4},{4,5},{5,0},{2,3},{3,6},{6,7},{7,2},{8,9},{9,12},{12,1... | collective-permute-start | bytes 1572872 | tf_op jit(solution)/shard_map/ppermute | solution.py:84
  97.8 3.4 %collective-permute-start.5 = (bf16[1024,256]{1,0:T(8,128)(2,1)}, bf16[1024,256]{1,0:T(8,128)(2,1)}, u32[]{:S(2)}, u32[]{:S(2)}) collective-permute-start(bf16[1024,256]{1,0:T(8,128)(2,1)} %get-tuple-element.32), channel_id=1, source_target_pairs={{0,4},{1,5},{4,0},{5,1},{2,6},{3,7},{6,2},{7,3},{8,12},{9,13},{12,... | collective-permute-start | bytes 1572872 | tf_op jit(solution)/shard_map/ppermute | solution.py:84
  101.2 2.0 collective-permute-start.6
  103.2 7.3 %collective-permute-done.4.w1 = bf16[1024,256]{1,0:T(8,128)(2,1)S(1)} collective-permute-done((bf16[1024,256]{1,0:T(8,128)(2,1)}, bf16[1024,256]{1,0:T(8,128)(2,1)S(1)}, u32[]{:S(2)}, u32[]{:S(2)}) %collective-permute-start.4) | collective-permute-done | bytes 524320 | tf_op jit(solution)/shard_map/ppermute | solution.py:84
  110.5 6.8 %collective-permute-done.5.w2 = bf16[1024,256]{1,0:T(8,128)(2,1)} collective-permute-done((bf16[1024,256]{1,0:T(8,128)(2,1)}, bf16[1024,256]{1,0:T(8,128)(2,1)}, u32[]{:S(2)}, u32[]{:S(2)}) %collective-permute-start.5) | collective-permute-done | bytes 524320 | tf_op jit(solution)/shard_map/ppermute | solution.py:84
  118.6 4.9 %shard_map.132 = bf16[4,776,256]{2,1,0:T(8,128)(2,1)S(1)} custom-call(s32[56]{0:T(128)S(1)} %copy-done.7, bf16[4,768,256]{2,1,0:T(8,128)(2,1)S(1)} %all-to-all-done.2.got, f32[16,256]{1,0:T(8,128)S(1)} %reshape.77.gain, bf16[4096,128]{1,0:T(8,128)(2,1)S(1)} %bitcast.37, bf16[4096,128]{1,0:T(8,128)(2,1)S(1)} %bitcast.39, ...), custom_call_target="tpu_custom_call" | custom-call | flops 1610612736 | bytes 6848736 | tf_op jit(solution)/shard_map/pallas_call | solution.py:98
  123.5 16.2 %all_to_all.36.parts = bf16[4,776,256]{2,1,0:T(8,128)(2,1)S(1)} all-to-all(bf16[4,776,256]{2,1,0:T(8,128)(2,1)S(1)} %shard_map.132), channel_id=1, replica_groups={{0,1,4,5},{2,3,6,7},{8,9,12,13},{10,11,14,15},{21,22,25,26},{23,20,27,2..., dimensions={0} | all-to-all | bytes 3178496 | tf_op jit(solution)/shard_map/all_to_all | solution.py:77
  139.7 1.3 shard_map.133
  141.0 7.9 %all-to-all-start.4 = ((bf16[4,768,128]{2,1,0:T(8,128)(2,1)}), bf16[4,768,128]{2,1,0:T(8,128)(2,1)S(1)}, u32[]{:S(2)}, u32[]{:S(2)}) async-start(bf16[4,768,128]{2,1,0:T(8,128)(2,1)} %shard_map.133), calls=%async_computation.4 | async-start | bytes 1572864 | tf_op jit(solution)/shard_map/all_to_all | solution.py:77
  148.9 2.2 shard_map.134
  151.1 1.9 collective-permute-start.7
  153.0 1.9 collective-permute-start.8
  154.9 4.3 %collective-permute-start.9 = (bf16[512,256]{1,0:T(8,128)(2,1)}, bf16[512,256]{1,0:T(8,128)(2,1)S(1)}, u32[]{:S(2)}, u32[]{:S(2)}) collective-permute-start(bf16[512,256]{1,0:T(8,128)(2,1)} %get-tuple-element.36), channel_id=1, source_target_pairs={{5,10},{6,5},{9,6},{10,9},{7,8},{4,7},{11,4},{8,11},{13,2},{14,13}... | collective-permute-start | bytes 786440 | tf_op jit(solution)/shard_map/ppermute | solution.py:84
  159.4 2.7 %collective-permute-done.8.w2 = bf16[512,256]{1,0:T(8,128)(2,1)S(1)} collective-permute-done((bf16[512,256]{1,0:T(8,128)(2,1)}, bf16[512,256]{1,0:T(8,128)(2,1)S(1)}, u32[]{:S(2)}, u32[]{:S(2)}) %collective-permute-start.8) | collective-permute-done | bytes 262176 | tf_op jit(solution)/shard_map/ppermute | solution.py:84
  162.1 1.6 collective-permute-done.9.w3
  163.7 2.9 %shard_map.135 = bf16[4,768,256]{2,1,0:T(8,128)(2,1)S(1)} custom-call(s32[56]{0:T(128)S(1)} %copy-done.8, bf16[4,768,128]{2,1,0:T(8,128)(2,1)S(1)} %all-to-all-done.4.acts, bf16[2048,256]{1,0:T(8,128)(2,1)S(1)} %bitcast.35, bf16[512,256]{1,0:T(8,128)(2,1)S(1)} %collective-permute-done.7.w1, bf16[512,256]{1,0:T(8,128)(2,1)S(1)} %collective-permute-done.8.w2, ...), custom_call_target="tpu_custom_call" | custom-call | flops 805306368 | bytes 4194528 | tf_op jit(solution)/shard_map/pallas_call | solution.py:98
  166.7 15.0 %all_to_all.37 = bf16[4,768,256]{2,1,0:T(8,128)(2,1)S(1)} all-to-all(bf16[4,768,256]{2,1,0:T(8,128)(2,1)S(1)} %shard_map.135), channel_id=1, replica_groups={{5,6,9,10},{7,4,11,8},{13,14,1,2},{15,12,3,0},{16,17,20,21},{18,19,22,2..., dimensions={0} | all-to-all | bytes 3145728 | tf_op jit(solution)/shard_map/all_to_all | solution.py:77
  182.7 8.1 %all-to-all-start.6 = ((bf16[32,24,256]{2,1,0:T(8,128)(2,1)}), bf16[32,24,256]{2,1,0:T(8,128)(2,1)S(1)}, u32[]{:S(2)}, u32[]{:S(2)}) async-start(bf16[32,24,256]{2,1,0:T(8,128)(2,1)} %bitcast.15), calls=%async_computation.6 | async-start | bytes 786432 | tf_op jit(solution)/shard_map/all_to_all | solution.py:355
  190.9 27.8 %all-to-all-done.6 = bf16[32,24,256]{2,1,0:T(8,128)(2,1)S(1)} async-done(((bf16[32,24,256]{2,1,0:T(8,128)(2,1)}), bf16[32,24,256]{2,1,0:T(8,128)(2,1)S(1)}, u32[]{:S(2)}, u32[]{:S(2)}) %all-to-all-start.6) | async-done | bytes 393248 | tf_op jit(solution)/shard_map/all_to_all | solution.py:355
  (60 shorter events, 10.2 us)
Async XLA Ops:
  0.0 13.0 %copy-start.13 = (s32[256]{0:T(256)S(1)}, s32[256]{0:T(256)}, u32[]{:S(2)}) copy-start(s32[256]{0:T(256)} %param.17) | copy-start | bytes 3076
  0.0 16.2 %collective-permute-start = (bf16[256,128]{1,0:T(8,128)(2,1)}, bf16[256,128]{1,0:T(8,128)(2,1)S(1)}, u32[]{:S(2)}, u32[]{:S(2)}) collective-permute-start(bf16[256,128]{1,0:T(8,128)(2,1)} %own.1), channel_id=1, source_target_pairs={{0,16},{16,32},{32,48},{48,64},{64,80},{80,96},{96,112},{112,128},... | collective-permute-start | bytes 196616 | tf_op jit(solution)/shard_map/ppermute | solution.py:306
  5.8 0.6 copy-start.5
  6.4 16.9 %copy-start.11 = (s32[256,2]{0,1:T(2,128)S(1)}, s32[256,2]{0,1:T(2,128)}, u32[]{:S(2)}) copy-start(s32[256,2]{0,1:T(2,128)} %param.22) | copy-start | bytes 6148
  8.5 24.7 %copy-start.1 = (bf16[2048,256]{1,0:T(8,128)(2,1)S(1)}, bf16[2048,256]{1,0:T(8,128)(2,1)}, u32[]{:S(2)}) copy-start(bf16[2048,256]{1,0:T(8,128)(2,1)} %weight.5) | copy-start | bytes 3145732
  8.5 24.7 %copy-start.4 = (bf16[256,256]{1,0:T(8,128)(2,1)S(1)}, bf16[256,256]{1,0:T(8,128)(2,1)}, u32[]{:S(2)}) copy-start(bf16[256,256]{1,0:T(8,128)(2,1)} %residual.1) | copy-start | bytes 393220
  8.5 24.7 %copy-start.6 = (s32[56]{0:T(128)S(1)}, s32[56]{0:T(128)}, u32[]{:S(2)}) copy-start(s32[56]{0:T(128)} %copy-done.5) | copy-start | bytes 676
  8.5 24.7 %collective-permute-start.2 = (bf16[1024,256]{1,0:T(8,128)(2,1)}, bf16[1024,256]{1,0:T(8,128)(2,1)S(1)}, u32[]{:S(2)}, u32[]{:S(2)}) collective-permute-start(bf16[1024,256]{1,0:T(8,128)(2,1)} %shard_map.128), channel_id=1, source_target_pairs={{0,12},{1,13},{2,14},{3,15},{4,8},{5,9},{6,10},{7,11},{8,4},{9,5},... | collective-permute-start | bytes 1572872 | tf_op jit(solution)/shard_map/ppermute | solution.py:335
  13.0 3.2 %collective-permute-start.1 = (s32[1,256]{1,0:T(1,128)S(1)}, s32[1,256]{1,0:T(1,128)S(1)}, u32[]{:S(2)}, u32[]{:S(2)}) collective-permute-start(s32[1,256]{1,0:T(1,128)S(1)} %bitcast.46), channel_id=1, source_target_pairs={{0,16},{16,32},{32,48},{48,64},{64,80},{80,96},{96,112},{112,128},... | collective-permute-start | bytes 3080 | tf_op jit(solution)/shard_map/ppermute | solution.py:307
  16.2 0.6 copy-start.14
  16.2 0.6 copy-start.9
  19.1 14.0 %all-to-all-start = ((bf16[8,256,128]{2,1,0:T(8,128)(2,1)}), bf16[8,256,128]{2,1,0:T(8,128)(2,1)S(1)}, u32[]{:S(2)}, u32[]{:S(2)}) async-start(bf16[8,256,128]{2,1,0:T(8,128)(2,1)} %shard_map.127), calls=%async_computation | async-start | bytes 1048576 | tf_op jit(solution)/shard_map/all_to_all | solution.py:77
  34.2 6.9 %collective-permute-start.3 = (bf16[256,256]{1,0:T(8,128)(2,1)S(1)}, bf16[256,256]{1,0:T(8,128)(2,1)S(1)}, u32[]{:S(2)}, u32[]{:S(2)}) collective-permute-start(bf16[256,256]{1,0:T(8,128)(2,1)S(1)} %get-tuple-element.28), channel_id=1, source_target_pairs={{0,12},{1,13},{2,14},{3,15},{4,8},{5,9},{6,10},{7,11},{8,4},{9,5},... | collective-permute-start | bytes 393224 | tf_op jit(solution)/shard_map/ppermute | solution.py:347
  87.5 29.8 %all-to-all-start.2 = ((bf16[4,768,256]{2,1,0:T(8,128)(2,1)}), bf16[4,768,256]{2,1,0:T(8,128)(2,1)S(1)}, u32[]{:S(2)}, u32[]{:S(2)}) async-start(bf16[4,768,256]{2,1,0:T(8,128)(2,1)} %broadcast_in_dim.38), calls=%async_computation.2 | async-start | bytes 3145728 | tf_op jit(solution)/shard_map/all_to_all | solution.py:77
  91.1 12.1 %copy-start.10 = (f32[4096]{0:T(1024)S(1)}, f32[4096]{0:T(1024)}, u32[]{:S(2)}) copy-start(f32[4096]{0:T(1024)} %param.21) | copy-start | bytes 49156
  91.1 26.2 %copy-start.2 = (bf16[1,4096,128]{2,1,0:T(8,128)(2,1)S(1)}, bf16[1,4096,128]{2,1,0:T(8,128)(2,1)}, u32[]{:S(2)}) copy-start(bf16[1,4096,128]{2,1,0:T(8,128)(2,1)} %param.24) | copy-start | bytes 3145732
  91.1 26.2 %copy-start.7 = (s32[56]{0:T(128)S(1)}, s32[56]{0:T(128)}, u32[]{:S(2)}) copy-start(s32[56]{0:T(128)} %copy-done.5) | copy-start | bytes 676
  94.2 16.3 %collective-permute-start.4 = (bf16[1024,256]{1,0:T(8,128)(2,1)}, bf16[1024,256]{1,0:T(8,128)(2,1)S(1)}, u32[]{:S(2)}, u32[]{:S(2)}) collective-permute-start(bf16[1024,256]{1,0:T(8,128)(2,1)} %get-tuple-element.31), channel_id=1, source_target_pairs={{0,1},{1,4},{4,5},{5,0},{2,3},{3,6},{6,7},{7,2},{8,9},{9,12},{12,1... | collective-permute-start | bytes 1572872 | tf_op jit(solution)/shard_map/ppermute | solution.py:84
  97.8 19.5 %collective-permute-start.5 = (bf16[1024,256]{1,0:T(8,128)(2,1)}, bf16[1024,256]{1,0:T(8,128)(2,1)}, u32[]{:S(2)}, u32[]{:S(2)}) collective-permute-start(bf16[1024,256]{1,0:T(8,128)(2,1)} %get-tuple-element.32), channel_id=1, source_target_pairs={{0,4},{1,5},{4,0},{5,1},{2,6},{3,7},{6,2},{7,3},{8,12},{9,13},{12,... | collective-permute-start | bytes 1572872 | tf_op jit(solution)/shard_map/ppermute | solution.py:84
  101.2 16.1 %collective-permute-start.6 = (bf16[1024,256]{1,0:T(8,128)(2,1)}, bf16[1024,256]{1,0:T(8,128)(2,1)}, u32[]{:S(2)}, u32[]{:S(2)}) collective-permute-start(bf16[1024,256]{1,0:T(8,128)(2,1)} %get-tuple-element.33), channel_id=1, source_target_pairs={{0,5},{1,0},{4,1},{5,4},{2,7},{3,2},{6,3},{7,6},{8,13},{9,8},{12,9... | collective-permute-start | bytes 1572872 | tf_op jit(solution)/shard_map/ppermute | solution.py:84
  117.4 1.2 copy-start.3
  141.0 22.7 %copy-start = (bf16[1,2048,256]{2,1,0:T(8,128)(2,1)S(1)}, bf16[1,2048,256]{2,1,0:T(8,128)(2,1)}, u32[]{:S(2)}) copy-start(bf16[1,2048,256]{2,1,0:T(8,128)(2,1)} %param.26) | copy-start | bytes 3145732
  141.0 22.7 %copy-start.8 = (s32[56]{0:T(128)S(1)}, s32[56]{0:T(128)}, u32[]{:S(2)}) copy-start(s32[56]{0:T(128)} %copy-done.5) | copy-start | bytes 676
  141.0 22.7 %all-to-all-start.4 = ((bf16[4,768,128]{2,1,0:T(8,128)(2,1)}), bf16[4,768,128]{2,1,0:T(8,128)(2,1)S(1)}, u32[]{:S(2)}, u32[]{:S(2)}) async-start(bf16[4,768,128]{2,1,0:T(8,128)(2,1)} %shard_map.133), calls=%async_computation.4 | async-start | bytes 1572864 | tf_op jit(solution)/shard_map/all_to_all | solution.py:77
  151.1 8.3 %collective-permute-start.7 = (bf16[512,256]{1,0:T(8,128)(2,1)}, bf16[512,256]{1,0:T(8,128)(2,1)S(1)}, u32[]{:S(2)}, u32[]{:S(2)}) collective-permute-start(bf16[512,256]{1,0:T(8,128)(2,1)} %get-tuple-element.34), channel_id=1, source_target_pairs={{5,6},{6,9},{9,10},{10,5},{7,4},{4,11},{11,8},{8,7},{13,14},{14,1}... | collective-permute-start | bytes 786440 | tf_op jit(solution)/shard_map/ppermute | solution.py:84
  153.0 9.1 %collective-permute-start.8 = (bf16[512,256]{1,0:T(8,128)(2,1)}, bf16[512,256]{1,0:T(8,128)(2,1)S(1)}, u32[]{:S(2)}, u32[]{:S(2)}) collective-permute-start(bf16[512,256]{1,0:T(8,128)(2,1)} %get-tuple-element.35), channel_id=1, source_target_pairs={{5,9},{6,10},{9,5},{10,6},{7,11},{4,8},{11,7},{8,4},{13,1},{14,2},... | collective-permute-start | bytes 786440 | tf_op jit(solution)/shard_map/ppermute | solution.py:84
  154.9 8.8 %collective-permute-start.9 = (bf16[512,256]{1,0:T(8,128)(2,1)}, bf16[512,256]{1,0:T(8,128)(2,1)S(1)}, u32[]{:S(2)}, u32[]{:S(2)}) collective-permute-start(bf16[512,256]{1,0:T(8,128)(2,1)} %get-tuple-element.36), channel_id=1, source_target_pairs={{5,10},{6,5},{9,6},{10,9},{7,8},{4,7},{11,4},{8,11},{13,2},{14,13}... | collective-permute-start | bytes 786440 | tf_op jit(solution)/shard_map/ppermute | solution.py:84
  181.7 9.2 %copy-start.12 = (f32[256,2]{0,1:T(2,128)S(1)}, f32[256,2]{0,1:T(2,128)}, u32[]{:S(2)}) copy-start(f32[256,2]{0,1:T(2,128)} %param.23) | copy-start | bytes 6148
  182.7 36.0 %all-to-all-start.6 = ((bf16[32,24,256]{2,1,0:T(8,128)(2,1)}), bf16[32,24,256]{2,1,0:T(8,128)(2,1)S(1)}, u32[]{:S(2)}, u32[]{:S(2)}) async-start(bf16[32,24,256]{2,1,0:T(8,128)(2,1)} %bitcast.15), calls=%async_computation.6 | async-start | bytes 786432 | tf_op jit(solution)/shard_map/all_to_all | solution.py:355

commit v4 on v2

--- a/solution.py
+++ b/solution.py
@@ -73,12 +73,12 @@
     return jax.ShapeDtypeStruct(dims, dtype)
 
 
-def call(kernel, outs, *args, flops, scratch=(), vmem=VMEM_BYTES, tables=1, fetched=0):
+def call(kernel, outs, *args, flops, scratch=(), vmem=VMEM_BYTES, tables=1):
     single = len(outs) == 1
     moved = sum(a.size * a.dtype.itemsize for a in (*args, *outs))
     whole = pl.BlockSpec(memory_space=pltpu.VMEM)
     specs = [pl.BlockSpec(memory_space=pltpu.SMEM)] * tables
-    specs += [whole] * (len(args) - tables - fetched) + [pl.BlockSpec(memory_space=pltpu.HBM)] * fetched
+    specs += [whole] * (len(args) - tables)
     return pl.pallas_call(
         kernel,
         out_shape=outs[0] if single else tuple(outs),
@@ -106,14 +106,12 @@
             outs[by][pl.ds(128 * i, 128), :] = down[pl.ds(pl.multiple_of(block * 128, 128), 128), :]
 
 
-def fetches(sources, held, arrived):
-    return [pltpu.make_async_copy(w, held.at[by], arrived.at[by]) for by, w in enumerate(sources)]
-
-
-def gate_up(where, got, gain, w0, w1, w2, w3, out, rows, held, arrived):
-    copies = fetches((w0, w1, w2, w3), held, arrived)
-    for copy in copies:
-        copy.start()
+def pack(where, w0, w1, w2, w3, out):
+    for by, block in enumerate((w0, w1, w2, w3)):
+        out[lax.rem(where[IN_SCATTER] + 4 - by, 4)] = block[...]
+
+
+def gate_up(where, got, gain, first, out, rows):
     count = got.shape[1]
     ones = jnp.ones((8, 256), BF16)
     tiles = count // 256
@@ -122,7 +120,9 @@
         total = jnp.zeros((8, 256), F32)
         for g in range(4):
             value = got[g, tile, :].astype(F32)
-            rows[tile, pl.ds(256 * g, 256)] = (value * gain[pl.ds(where[GAINS + g], 1), :]).astype(BF16)
+            for h in range(2):
+                scaled = value[:, 128 * h : 128 * h + 128] * gain[pl.ds(2 * where[GAINS + g] + h, 1), :]
+                rows[tile, pl.ds(256 * g + 128 * h, 128)] = scaled.astype(BF16)
             square = value * value
             high = square.astype(BF16)
             low = (square - high.astype(F32)).astype(BF16)
@@ -133,13 +133,11 @@
         for j in range(4):
             out[j, pl.ds(count + 2 * i, 1), :] = high[:1]
             out[j, pl.ds(count + 2 * i + 1, 1), :] = low[:1]
-    for by, copy in enumerate(copies):
-        copy.wait()
-        to = lax.rem(where[IN_SCATTER] + 4 - by, 4)
+    for to in range(4):
         out[to, pl.ds(count + 2 * tiles, 8 - 2 * tiles), :] = jnp.zeros((8 - 2 * tiles, 256), BF16)
         for i in range(tiles):
             tile = pl.ds(256 * i, 256)
-            out[to, tile, :] = jnp.dot(rows[tile, :], held[by], preferred_element_type=F32).astype(BF16)
+            out[to, tile, :] = jnp.dot(rows[tile, :], first[to], preferred_element_type=F32).astype(BF16)
 
 
 def activate(parts, out):
@@ -162,19 +160,15 @@
             out[j, tile, :] = act
 
 
-def down_rows(where, acts, w0, w1, w2, w3, out, rows, held, arrived):
-    copies = fetches((w0, w1, w2, w3), held, arrived)
-    for copy in copies:
-        copy.start()
+def down_rows(where, acts, w0, w1, w2, w3, out, rows):
     count = acts.shape[1]
     for h in range(4):
         rows[:, pl.ds(128 * h, 128)] = acts[h]
-    for by, copy in enumerate(copies):
-        copy.wait()
+    for by, second in enumerate((w0, w1, w2, w3)):
         to = lax.rem(where[IN_GATHER] + 4 - by, 4)
         for i in range(count // 256):
             tile = pl.ds(256 * i, 256)
-            out[to, tile, :] = jnp.dot(rows[tile, :], held[by], preferred_element_type=F32).astype(BF16)
+            out[to, tile, :] = jnp.dot(rows[tile, :], second[...], preferred_element_type=F32).astype(BF16)
 
 
 def experts(arrived, first, second, where, gain):
@@ -186,10 +180,9 @@
         where,
         got,
         gain,
-        *first,
+        first,
         flops=2**21 * count,
-        scratch=[pltpu.VMEM((count, 1024), BF16), pltpu.VMEM((4, 1024, 256), BF16), pltpu.SemaphoreType.DMA((4,))],
-        fetched=4,
+        scratch=[pltpu.VMEM((count, 1024), BF16)],
     )
     parts = a2a(part, SCATTER)
     acts = a2a(call(activate, [shape(4, count, 128)], parts, flops=2**16 * count, tables=0), SCATTER)
@@ -200,8 +193,7 @@
         acts,
         *second,
         flops=2**20 * count,
-        scratch=[pltpu.VMEM((count, 512), BF16), pltpu.VMEM((4, 512, 256), BF16), pltpu.SemaphoreType.DMA((4,))],
-        fetched=4,
+        scratch=[pltpu.VMEM((count, 512), BF16)],
     )
     parts = a2a(part, GATHER)
     return jnp.sum(parts.astype(F32), axis=0).astype(BF16)
@@ -286,7 +278,8 @@
     arrived = lax.all_to_all(send.reshape(n_exp, cap, cols), SP, 0, 0, tiled=True).reshape(slots, cols)
     first = turns(cuts_first, SCATTER)
     second = turns(cuts_second, GATHER)
-    made = experts(arrived, first, second, where, norm_gain.reshape(16, 256))
+    first = call(pack, [shape(4, 1024, 256)], where, *first, flops=2**22)
+    made = experts(arrived, first, second, where, norm_gain.reshape(32, 128))
     back = lax.all_to_all(made.reshape(n_exp, cap, cols), SP, 0, 0, tiled=True).reshape(slots, cols)
     summed = jnp.dot(mix_high, back, preferred_element_type=F32) + jnp.dot(
         mix_low, back, preferred_element_type=F32

time: 215 us -> 215 us (level)
    pallas_call x6 -> x7, Pallas kernels: 16.7 us -> 15.9 us  [call(): pl.pallas_call(kernel, out_shape=outs[0] if single else tuple(outs), in_s...]
where the time goes in v4:
time: 215 us; the launch traced here: 214 us
  blocking collectives  74.2 us (35%)
  waiting for transfers between devices  62.9 us (29%)
  starting transfers between devices  50.4 us (23%)
  Pallas kernels  15.9 us (7%)
  local copies, waits for them, and re-layouts  5.5 us (3%)
  other arithmetic  2.41 us (1%)
  matrix products  2.2 us (1%)
    all_to_all x1, blocking collectives, layer(): lax.all_to_all(send.reshape(n_exp, cap, cols), SP, 0, 0, tiled=True)  42.9 us
    all_to_all x2, blocking collectives, a2a(): lax.all_to_all(blocks, PLANE, 0, 0, tiled=True, axis_index_groups=both_co...  31.3 us
    all_to_all x1, waiting for transfers between devices, layer(): lax.all_to_all(made.reshape(n_exp, cap, cols), SP, 0, 0, tiled=True)  27.8 us
    ppermute x6, starting transfers between devices, turns(): got.append(lax.ppermute(cuts[by], PLANE, pairs))  17.3 us
    ppermute x6, waiting for transfers between devices, turns(): got.append(lax.ppermute(cuts[by], PLANE, pairs))  17 us
    pallas_call x7, Pallas kernels, call(): pl.pallas_call(kernel, out_shape=outs[0] if single else tuple(outs), in_s...  15.9 us
    all_to_all x1, waiting for transfers between devices, layer(): pooled_all = lax.all_to_all(pooled, TP, 0, 0, tiled=True)  15.3 us
    all_to_all x2, starting transfers between devices, a2a(): lax.all_to_all(blocks, PLANE, 0, 0, tiled=True, axis_index_groups=both_co...  12.3 us
  transfers between devices with their start and end apart: 12, of which 9 were waited for; matrix products, arithmetic and copies ran while one was open for 1% of the time, Pallas kernels for 3%

profile of v4, /device:TPU:1, one launch (start us, length us, event | category | flops | bytes accessed | tf_op | source)
XLA Modules:
  0.0 213.7 jit_solution(9388748963022629336)
XLA Ops:
  0.0 5.0 %collective-permute-start.1 = (s32[1,256]{1,0:T(1,128)}, s32[1,256]{1,0:T(1,128)S(1)}, u32[]{:S(2)}, u32[]{:S(2)}) collective-permute-start(s32[1,256]{1,0:T(1,128)} %bitcast.63), channel_id=1, source_target_pairs={{0,16},{16,32},{32,48},{48,64},{64,80},{80,96},{96,112},{112,128},... | collective-permute-start | bytes 3080 | tf_op jit(solution)/shard_map/ppermute | solution.py:245
  5.1 1.9 collective-permute-start
  7.7 1.4 collective-permute-done.1.docs_before
  9.1 1.4 collective-permute-done.before
  11.1 2.5 %shard_map.127 = bf16[16,256,128]{2,1,0:T(8,128)(2,1)} custom-call(s32[40]{0:T(128)} %copy-done.3, bf16[256,128]{1,0:T(8,128)(2,1)} %own.1, bf16[256,128]{1,0:T(8,128)(2,1)} %copy-done.8, s32[1,256]{1,0:T(1,128)} %bitcast.64, s32[1,256]{1,0:T(1,128)} %copy-done.11, bf16[1,128,128]{2,1,0:T(8,128)(2,1)} %weight.1, f32[1,128]{1,0:T(1,128)} %bitcast.65), custom_call_target="tpu_custom_call" | custom-call | flops 8388608 | bytes 1215136 | tf_op jit(solution)/shard_map/pallas_call | solution.py:82
  13.7 5.0 %all-to-all-start = ((bf16[16,256,128]{2,1,0:T(8,128)(2,1)}), bf16[16,256,128]{2,1,0:T(8,128)(2,1)S(1)}, u32[]{:S(2)}, u32[]{:S(2)}) async-start(bf16[16,256,128]{2,1,0:T(8,128)(2,1)} %shard_map.127), calls=%async_computation | async-start | bytes 2097152 | tf_op jit(solution)/shard_map/all_to_all | solution.py:273
  19.1 1.2 reduce-window.6
  20.9 15.3 %all-to-all-done = bf16[16,256,128]{2,1,0:T(8,128)(2,1)S(1)} async-done(((bf16[16,256,128]{2,1,0:T(8,128)(2,1)}), bf16[16,256,128]{2,1,0:T(8,128)(2,1)S(1)}, u32[]{:S(2)}, u32[]{:S(2)}) %all-to-all-start) | async-done | bytes 1048608 | tf_op jit(solution)/shard_map/all_to_all | solution.py:273
  37.0 42.9 %all_to_all.35 = bf16[32,24,256]{2,1,0:T(8,128)(2,1)S(1)} all-to-all(bf16[32,24,256]{2,1,0:T(8,128)(2,1)S(1)} %bitcast.52), channel_id=1, replica_groups=mesh['z'=16,'c'=2,'y'=4,'x'=4] {'z','c'}, dimensions={0} | all-to-all | bytes 786432 | tf_op jit(solution)/shard_map/all_to_all | solution.py:278
  79.9 1.2 broadcast_in_dim.40
  81.1 4.3 %all-to-all-start.2 = ((bf16[4,768,256]{2,1,0:T(8,128)(2,1)}), bf16[4,768,256]{2,1,0:T(8,128)(2,1)}, u32[]{:S(2)}, u32[]{:S(2)}) async-start(bf16[4,768,256]{2,1,0:T(8,128)(2,1)} %broadcast_in_dim.40), calls=%async_computation.2 | async-start | bytes 3145728 | tf_op jit(solution)/shard_map/all_to_all | solution.py:61
  85.5 3.3 %shard_map.128 = (bf16[1024,256]{1,0:T(8,128)(2,1)}, bf16[1024,256]{1,0:T(8,128)(2,1)}, bf16[1024,256]{1,0:T(8,128)(2,1)}, bf16[1024,256]{1,0:T(8,128)(2,1)}) custom-call(s32[40]{0:T(128)} %copy-done.3, bf16[4096,128]{1,0:T(8,128)(2,1)} %bitcast.47, bf16[4096,128]{1,0:T(8,128)(2,1)} %bitcast.48), custom_call_target="tpu_custom_call" | custom-call | flops 4194304 | bytes 4194464 | tf_op jit(solution)/shard_map/pallas_call | solution.py:82
  88.8 3.7 %collective-permute-start.2 = (bf16[1024,256]{1,0:T(8,128)(2,1)}, bf16[1024,256]{1,0:T(8,128)(2,1)S(1)}, u32[]{:S(2)}, u32[]{:S(2)}) collective-permute-start(bf16[1024,256]{1,0:T(8,128)(2,1)} %get-tuple-element.26), channel_id=1, source_target_pairs={{0,1},{1,4},{4,5},{5,0},{2,3},{3,6},{6,7},{7,2},{8,9},{9,12},{12,1... | collective-permute-start | bytes 1572872 | tf_op jit(solution)/shard_map/ppermute | solution.py:68
  92.5 2.8 %collective-permute-start.3 = (bf16[1024,256]{1,0:T(8,128)(2,1)}, bf16[1024,256]{1,0:T(8,128)(2,1)S(1)}, u32[]{:S(2)}, u32[]{:S(2)}) collective-permute-start(bf16[1024,256]{1,0:T(8,128)(2,1)} %get-tuple-element.27), channel_id=1, source_target_pairs={{0,4},{1,5},{4,0},{5,1},{2,6},{3,7},{6,2},{7,3},{8,12},{9,13},{12,... | collective-permute-start | bytes 1572872 | tf_op jit(solution)/shard_map/ppermute | solution.py:68
  95.3 2.7 %collective-permute-start.4 = (bf16[1024,256]{1,0:T(8,128)(2,1)}, bf16[1024,256]{1,0:T(8,128)(2,1)S(1)}, u32[]{:S(2)}, u32[]{:S(2)}) collective-permute-start(bf16[1024,256]{1,0:T(8,128)(2,1)} %get-tuple-element.28), channel_id=1, source_target_pairs={{0,5},{1,0},{4,1},{5,4},{2,7},{3,2},{6,3},{7,6},{8,13},{9,8},{12,9... | collective-permute-start | bytes 1572872 | tf_op jit(solution)/shard_map/ppermute | solution.py:68
  98.0 6.1 %collective-permute-done.2.w1 = bf16[1024,256]{1,0:T(8,128)(2,1)S(1)} collective-permute-done((bf16[1024,256]{1,0:T(8,128)(2,1)}, bf16[1024,256]{1,0:T(8,128)(2,1)S(1)}, u32[]{:S(2)}, u32[]{:S(2)}) %collective-permute-start.2) | collective-permute-done | bytes 524320 | tf_op jit(solution)/shard_map/ppermute | solution.py:68
  104.1 6.7 %collective-permute-done.3.w2 = bf16[1024,256]{1,0:T(8,128)(2,1)S(1)} collective-permute-done((bf16[1024,256]{1,0:T(8,128)(2,1)}, bf16[1024,256]{1,0:T(8,128)(2,1)S(1)}, u32[]{:S(2)}, u32[]{:S(2)}) %collective-permute-start.3) | collective-permute-done | bytes 524320 | tf_op jit(solution)/shard_map/ppermute | solution.py:68
  112.5 4.2 %shard_map.130 = bf16[4,776,256]{2,1,0:T(8,128)(2,1)S(1)} custom-call(s32[40]{0:T(128)S(1)} %copy-done.4, bf16[4,768,256]{2,1,0:T(8,128)(2,1)} %all-to-all-done.2.got, f32[32,128]{1,0:T(8,128)S(1)} %bitcast.45, bf16[4,1024,256]{2,1,0:T(8,128)(2,1)S(1)} %shard_map.129.first), custom_call_target="tpu_custom_call" | custom-call | flops 1610612736 | bytes 5275808 | tf_op jit(solution)/shard_map/pallas_call | solution.py:82
  116.7 16.0 %all_to_all.36.parts = bf16[4,776,256]{2,1,0:T(8,128)(2,1)S(1)} all-to-all(bf16[4,776,256]{2,1,0:T(8,128)(2,1)S(1)} %shard_map.130), channel_id=1, replica_groups={{0,1,4,5},{2,3,6,7},{8,9,12,13},{10,11,14,15},{21,22,25,26},{23,20,27,2..., dimensions={0} | all-to-all | bytes 3178496 | tf_op jit(solution)/shard_map/all_to_all | solution.py:61
  132.7 1.3 shard_map.131
  134.0 7.9 %all-to-all-start.4 = ((bf16[4,768,128]{2,1,0:T(8,128)(2,1)}), bf16[4,768,128]{2,1,0:T(8,128)(2,1)S(1)}, u32[]{:S(2)}, u32[]{:S(2)}) async-start(bf16[4,768,128]{2,1,0:T(8,128)(2,1)} %shard_map.131), calls=%async_computation.4 | async-start | bytes 1572864 | tf_op jit(solution)/shard_map/all_to_all | solution.py:61
  142.0 2.3 %shard_map.132 = (bf16[512,256]{1,0:T(8,128)(2,1)}, bf16[512,256]{1,0:T(8,128)(2,1)}, bf16[512,256]{1,0:T(8,128)(2,1)}, bf16[512,256]{1,0:T(8,128)(2,1)}) custom-call(s32[40]{0:T(128)} %copy-done.3, bf16[2048,256]{1,0:T(8,128)(2,1)} %bitcast.49), custom_call_target="tpu_custom_call" | custom-call | flops 2097152 | bytes 2097312 | tf_op jit(solution)/shard_map/pallas_call | solution.py:82
  144.3 1.9 collective-permute-start.5
  146.2 1.9 collective-permute-start.6
  148.1 4.3 %collective-permute-start.7 = (bf16[512,256]{1,0:T(8,128)(2,1)}, bf16[512,256]{1,0:T(8,128)(2,1)S(1)}, u32[]{:S(2)}, u32[]{:S(2)}) collective-permute-start(bf16[512,256]{1,0:T(8,128)(2,1)} %get-tuple-element.32), channel_id=1, source_target_pairs={{5,10},{6,5},{9,6},{10,9},{7,8},{4,7},{11,4},{8,11},{13,2},{14,13}... | collective-permute-start | bytes 786440 | tf_op jit(solution)/shard_map/ppermute | solution.py:68
  152.8 2.5 %collective-permute-done.6.w2 = bf16[512,256]{1,0:T(8,128)(2,1)S(1)} collective-permute-done((bf16[512,256]{1,0:T(8,128)(2,1)}, bf16[512,256]{1,0:T(8,128)(2,1)S(1)}, u32[]{:S(2)}, u32[]{:S(2)}) %collective-permute-start.6) | collective-permute-done | bytes 262176 | tf_op jit(solution)/shard_map/ppermute | solution.py:68
  155.3 1.3 collective-permute-done.7.w3
  157.6 1.6 shard_map.133
  159.1 15.3 %all_to_all.37 = bf16[4,768,256]{2,1,0:T(8,128)(2,1)S(1)} all-to-all(bf16[4,768,256]{2,1,0:T(8,128)(2,1)S(1)} %shard_map.133), channel_id=1, replica_groups={{5,6,9,10},{7,4,11,8},{13,14,1,2},{15,12,3,0},{16,17,20,21},{18,19,22,2..., dimensions={0} | all-to-all | bytes 3145728 | tf_op jit(solution)/shard_map/all_to_all | solution.py:61
  175.5 8.9 %all-to-all-start.6 = ((bf16[32,24,256]{2,1,0:T(8,128)(2,1)}), bf16[32,24,256]{2,1,0:T(8,128)(2,1)S(1)}, u32[]{:S(2)}, u32[]{:S(2)}) async-start(bf16[32,24,256]{2,1,0:T(8,128)(2,1)} %bitcast.17), calls=%async_computation.6 | async-start | bytes 786432 | tf_op jit(solution)/shard_map/all_to_all | solution.py:283
  184.4 27.8 %all-to-all-done.6 = bf16[32,24,256]{2,1,0:T(8,128)(2,1)S(1)} async-done(((bf16[32,24,256]{2,1,0:T(8,128)(2,1)}), bf16[32,24,256]{2,1,0:T(8,128)(2,1)S(1)}, u32[]{:S(2)}, u32[]{:S(2)}) %all-to-all-start.6) | async-done | bytes 393248 | tf_op jit(solution)/shard_map/all_to_all | solution.py:283
  212.7 1.1 fusion.3
  (48 shorter events, 7.7 us)
Async XLA Ops:
  0.0 36.2 %copy-start = (bf16[2048,256]{1,0:T(8,128)(2,1)S(1)}, bf16[2048,256]{1,0:T(8,128)(2,1)}, u32[]{:S(2)}) copy-start(bf16[2048,256]{1,0:T(8,128)(2,1)} %param.20) | copy-start | bytes 3145732
  0.0 9.1 %collective-permute-start.1 = (s32[1,256]{1,0:T(1,128)}, s32[1,256]{1,0:T(1,128)S(1)}, u32[]{:S(2)}, u32[]{:S(2)}) collective-permute-start(s32[1,256]{1,0:T(1,128)} %bitcast.63), channel_id=1, source_target_pairs={{0,16},{16,32},{32,48},{48,64},{64,80},{80,96},{96,112},{112,128},... | collective-permute-start | bytes 3080 | tf_op jit(solution)/shard_map/ppermute | solution.py:245
  5.1 5.4 %collective-permute-start = (bf16[256,128]{1,0:T(8,128)(2,1)}, bf16[256,128]{1,0:T(8,128)(2,1)S(1)}, u32[]{:S(2)}, u32[]{:S(2)}) collective-permute-start(bf16[256,128]{1,0:T(8,128)(2,1)} %own.1), channel_id=1, source_target_pairs={{0,16},{16,32},{32,48},{48,64},{64,80},{80,96},{96,112},{112,128},... | collective-permute-start | bytes 196616 | tf_op jit(solution)/shard_map/ppermute | solution.py:244
  7.7 2.8 %copy-start.3 = (s32[40]{0:T(128)}, s32[40]{0:T(128)S(1)}, u32[]{:S(2)}) copy-start(s32[40]{0:T(128)S(1)} %constant_dynamic-update-slice_fusion.where) | copy-start | bytes 484
  9.1 1.4 copy-start.11
  10.5 0.6 copy-start.8
  11.1 7.6 %copy-start.9 = (s32[256,2]{0,1:T(2,128)S(1)}, s32[256,2]{0,1:T(2,128)}, u32[]{:S(2)}) copy-start(s32[256,2]{0,1:T(2,128)} %param.22) | copy-start | bytes 6148
  13.7 22.6 %copy-start.7 = (bf16[256,256]{1,0:T(8,128)(2,1)S(1)}, bf16[256,256]{1,0:T(8,128)(2,1)}, u32[]{:S(2)}) copy-start(bf16[256,256]{1,0:T(8,128)(2,1)} %param.15) | copy-start | bytes 393220
  13.7 22.6 %all-to-all-start = ((bf16[16,256,128]{2,1,0:T(8,128)(2,1)}), bf16[16,256,128]{2,1,0:T(8,128)(2,1)S(1)}, u32[]{:S(2)}, u32[]{:S(2)}) async-start(bf16[16,256,128]{2,1,0:T(8,128)(2,1)} %shard_map.127), calls=%async_computation | async-start | bytes 2097152 | tf_op jit(solution)/shard_map/all_to_all | solution.py:273
  81.1 31.4 %all-to-all-start.2 = ((bf16[4,768,256]{2,1,0:T(8,128)(2,1)}), bf16[4,768,256]{2,1,0:T(8,128)(2,1)}, u32[]{:S(2)}, u32[]{:S(2)}) async-start(bf16[4,768,256]{2,1,0:T(8,128)(2,1)} %broadcast_in_dim.40), calls=%async_computation.2 | async-start | bytes 3145728 | tf_op jit(solution)/shard_map/all_to_all | solution.py:61
  85.5 25.3 %copy-start.4 = (s32[40]{0:T(128)S(1)}, s32[40]{0:T(128)}, u32[]{:S(2)}) copy-start(s32[40]{0:T(128)} %copy-done.3) | copy-start | bytes 484
  88.8 15.3 %collective-permute-start.2 = (bf16[1024,256]{1,0:T(8,128)(2,1)}, bf16[1024,256]{1,0:T(8,128)(2,1)S(1)}, u32[]{:S(2)}, u32[]{:S(2)}) collective-permute-start(bf16[1024,256]{1,0:T(8,128)(2,1)} %get-tuple-element.26), channel_id=1, source_target_pairs={{0,1},{1,4},{4,5},{5,0},{2,3},{3,6},{6,7},{7,2},{8,9},{9,12},{12,1... | collective-permute-start | bytes 1572872 | tf_op jit(solution)/shard_map/ppermute | solution.py:68
  92.5 18.2 %collective-permute-start.3 = (bf16[1024,256]{1,0:T(8,128)(2,1)}, bf16[1024,256]{1,0:T(8,128)(2,1)S(1)}, u32[]{:S(2)}, u32[]{:S(2)}) collective-permute-start(bf16[1024,256]{1,0:T(8,128)(2,1)} %get-tuple-element.27), channel_id=1, source_target_pairs={{0,4},{1,5},{4,0},{5,1},{2,6},{3,7},{6,2},{7,3},{8,12},{9,13},{12,... | collective-permute-start | bytes 1572872 | tf_op jit(solution)/shard_map/ppermute | solution.py:68
  95.3 15.4 %collective-permute-start.4 = (bf16[1024,256]{1,0:T(8,128)(2,1)}, bf16[1024,256]{1,0:T(8,128)(2,1)S(1)}, u32[]{:S(2)}, u32[]{:S(2)}) collective-permute-start(bf16[1024,256]{1,0:T(8,128)(2,1)} %get-tuple-element.28), channel_id=1, source_target_pairs={{0,5},{1,0},{4,1},{5,4},{2,7},{3,2},{6,3},{7,6},{8,13},{9,8},{12,9... | collective-permute-start | bytes 1572872 | tf_op jit(solution)/shard_map/ppermute | solution.py:68
  110.7 1.0 copy-start.1
  111.8 0.7 copy-start.6
  134.0 22.6 %copy-start.5 = (s32[40]{0:T(128)S(1)}, s32[40]{0:T(128)}, u32[]{:S(2)}) copy-start(s32[40]{0:T(128)} %copy-done.3) | copy-start | bytes 484
  134.0 22.6 %all-to-all-start.4 = ((bf16[4,768,128]{2,1,0:T(8,128)(2,1)}), bf16[4,768,128]{2,1,0:T(8,128)(2,1)S(1)}, u32[]{:S(2)}, u32[]{:S(2)}) async-start(bf16[4,768,128]{2,1,0:T(8,128)(2,1)} %shard_map.131), calls=%async_computation.4 | async-start | bytes 1572864 | tf_op jit(solution)/shard_map/all_to_all | solution.py:61
  144.3 8.5 %collective-permute-start.5 = (bf16[512,256]{1,0:T(8,128)(2,1)}, bf16[512,256]{1,0:T(8,128)(2,1)S(1)}, u32[]{:S(2)}, u32[]{:S(2)}) collective-permute-start(bf16[512,256]{1,0:T(8,128)(2,1)} %get-tuple-element.30), channel_id=1, source_target_pairs={{5,6},{6,9},{9,10},{10,5},{7,4},{4,11},{11,8},{8,7},{13,14},{14,1}... | collective-permute-start | bytes 786440 | tf_op jit(solution)/shard_map/ppermute | solution.py:68
  146.2 9.1 %collective-permute-start.6 = (bf16[512,256]{1,0:T(8,128)(2,1)}, bf16[512,256]{1,0:T(8,128)(2,1)S(1)}, u32[]{:S(2)}, u32[]{:S(2)}) collective-permute-start(bf16[512,256]{1,0:T(8,128)(2,1)} %get-tuple-element.31), channel_id=1, source_target_pairs={{5,9},{6,10},{9,5},{10,6},{7,11},{4,8},{11,7},{8,4},{13,1},{14,2},... | collective-permute-start | bytes 786440 | tf_op jit(solution)/shard_map/ppermute | solution.py:68
  148.1 8.5 %collective-permute-start.7 = (bf16[512,256]{1,0:T(8,128)(2,1)}, bf16[512,256]{1,0:T(8,128)(2,1)S(1)}, u32[]{:S(2)}, u32[]{:S(2)}) collective-permute-start(bf16[512,256]{1,0:T(8,128)(2,1)} %get-tuple-element.32), channel_id=1, source_target_pairs={{5,10},{6,5},{9,6},{10,9},{7,8},{4,7},{11,4},{8,11},{13,2},{14,13}... | collective-permute-start | bytes 786440 | tf_op jit(solution)/shard_map/ppermute | solution.py:68
  156.6 1.0 copy-start.2
  174.4 10.0 %copy-start.10 = (f32[256,2]{0,1:T(2,128)S(1)}, f32[256,2]{0,1:T(2,128)}, u32[]{:S(2)}) copy-start(f32[256,2]{0,1:T(2,128)} %param.23) | copy-start | bytes 6148
  175.5 36.7 %all-to-all-start.6 = ((bf16[32,24,256]{2,1,0:T(8,128)(2,1)}), bf16[32,24,256]{2,1,0:T(8,128)(2,1)S(1)}, u32[]{:S(2)}, u32[]{:S(2)}) async-start(bf16[32,24,256]{2,1,0:T(8,128)(2,1)} %bitcast.17), calls=%async_computation.6 | async-start | bytes 786432 | tf_op jit(solution)/shard_map/all_to_all | solution.py:283

commit v5 on v4

--- a/solution.py
+++ b/solution.py
@@ -117,17 +117,18 @@
     tiles = count // 256
     for i in range(tiles):
         tile = pl.ds(256 * i, 256)
-        total = jnp.zeros((8, 256), F32)
+        squares = jnp.zeros((256, 256), F32)
         for g in range(4):
             value = got[g, tile, :].astype(F32)
             for h in range(2):
                 scaled = value[:, 128 * h : 128 * h + 128] * gain[pl.ds(2 * where[GAINS + g] + h, 1), :]
                 rows[tile, pl.ds(256 * g + 128 * h, 128)] = scaled.astype(BF16)
-            square = value * value
-            high = square.astype(BF16)
-            low = (square - high.astype(F32)).astype(BF16)
-            for part in (high, low):
-                total = total + lax.dot_general(ones, part, (((1,), (1,)), ((), ())), preferred_element_type=F32)
+            squares = squares + value * value
+        high = squares.astype(BF16)
+        low = (squares - high.astype(F32)).astype(BF16)
+        total = jnp.zeros((8, 256), F32)
+        for part in (high, low):
+            total = total + lax.dot_general(ones, part, (((1,), (1,)), ((), ())), preferred_element_type=F32)
         high = total.astype(BF16)
         low = (total - high.astype(F32)).astype(BF16)
         for j in range(4):
@@ -265,7 +266,7 @@
     take = (place[:, 0][None, :] == places[:, None]) | (place[:, 1][None, :] == places[:, None])
     low = jnp.where(place[:, 0][:, None] == places[None, :], route_weights[:, 0][:, None], 0.0)
     mix = low + jnp.where(place[:, 1][:, None] == places[None, :], route_weights[:, 1][:, None], 0.0)
-    mix_high, mix_low = split(mix)
+    mix_high, mix_low = lax.optimization_barrier(split(mix))
 
     cuts_first = call(cut_first, [shape(1024, 256)] * 4, where, w_gate[0], w_up[0], flops=2**22, vmem=LARGE)
     cuts_second = call(cut_second, [shape(512, 256)] * 4, where, w_down[0], flops=2**21, vmem=LARGE)
@@ -274,7 +275,7 @@
     proj = jnp.einsum("gtc,gcd->td", pooled_all, out_weight.reshape(16, 128, cols), preferred_element_type=F32)
     updated = (residual.astype(F32) + proj).astype(BF16)
 
-    send = jnp.dot(take.astype(BF16), updated, preferred_element_type=F32).astype(BF16)
+    send = jnp.dot(lax.optimization_barrier(take.astype(BF16)), updated, preferred_element_type=F32).astype(BF16)
     arrived = lax.all_to_all(send.reshape(n_exp, cap, cols), SP, 0, 0, tiled=True).reshape(slots, cols)
     first = turns(cuts_first, SCATTER)
     second = turns(cuts_second, GATHER)

time: 215 us -> 214 us (level)
  waiting for transfers between devices: 62.9 us -> 60.4 us
  transfers between devices with their start and end apart: 12 -> 12, of which waited for: 9 -> 9; matrix products, arithmetic and copies ran while one was open for 1% -> 2% of each run, Pallas kernels for 3% -> 3%
where the time goes in v5:
time: 214 us; the launch traced here: 213 us
  blocking collectives  75.6 us (35%)
  waiting for transfers between devices  60.4 us (28%)
  starting transfers between devices  50.4 us (24%)
  Pallas kernels  15.6 us (7%)
  local copies, waits for them, and re-layouts  6.16 us (3%)
  other arithmetic  2.86 us (1%)
    all_to_all x1, blocking collectives, layer(): lax.all_to_all(send.reshape(n_exp, cap, cols), SP, 0, 0, tiled=True)  44.2 us
    all_to_all x2, blocking collectives, a2a(): lax.all_to_all(blocks, PLANE, 0, 0, tiled=True, axis_index_groups=both_co...  31.3 us
    all_to_all x1, waiting for transfers between devices, layer(): lax.all_to_all(made.reshape(n_exp, cap, cols), SP, 0, 0, tiled=True)  27.5 us
    ppermute x6, starting transfers between devices, turns(): got.append(lax.ppermute(cuts[by], PLANE, pairs))  17.3 us
    ppermute x6, waiting for transfers between devices, turns(): got.append(lax.ppermute(cuts[by], PLANE, pairs))  17 us
    pallas_call x7, Pallas kernels, call(): pl.pallas_call(kernel, out_shape=outs[0] if single else tuple(outs), in_s...  15.6 us
    all_to_all x1, waiting for transfers between devices, layer(): pooled_all = lax.all_to_all(pooled, TP, 0, 0, tiled=True)  14.1 us
    all_to_all x2, starting transfers between devices, a2a(): lax.all_to_all(blocks, PLANE, 0, 0, tiled=True, axis_index_groups=both_co...  12.3 us
  transfers between devices with their start and end apart: 12, of which 9 were waited for; matrix products, arithmetic and copies ran while one was open for 2% of the time, Pallas kernels for 3%

profile of v5, /device:TPU:1, one launch (start us, length us, event | category | flops | bytes accessed | tf_op | source)
XLA Modules:
  0.0 213.1 jit_solution(8108667265788966151)
XLA Ops:
  0.0 5.0 %collective-permute-start.1 = (s32[1,256]{1,0:T(1,128)}, s32[1,256]{1,0:T(1,128)S(1)}, u32[]{:S(2)}, u32[]{:S(2)}) collective-permute-start(s32[1,256]{1,0:T(1,128)} %bitcast.62), channel_id=1, source_target_pairs={{0,16},{16,32},{32,48},{48,64},{64,80},{80,96},{96,112},{112,128},... | collective-permute-start | bytes 3080 | tf_op jit(solution)/shard_map/ppermute | solution.py:246
  5.1 1.9 collective-permute-start
  9.1 1.4 collective-permute-done.before
  11.1 2.5 %shard_map.127 = bf16[16,256,128]{2,1,0:T(8,128)(2,1)} custom-call(s32[40]{0:T(128)} %copy-done.3, bf16[256,128]{1,0:T(8,128)(2,1)} %own.1, bf16[256,128]{1,0:T(8,128)(2,1)} %copy-done.8, s32[1,256]{1,0:T(1,128)} %bitcast.63, s32[1,256]{1,0:T(1,128)} %copy-done.11, bf16[1,128,128]{2,1,0:T(8,128)(2,1)} %weight.1, f32[1,128]{1,0:T(1,128)} %bitcast.64), custom_call_target="tpu_custom_call" | custom-call | flops 8388608 | bytes 1215136 | tf_op jit(solution)/shard_map/pallas_call | solution.py:82
  13.7 5.1 %all-to-all-start = ((bf16[16,256,128]{2,1,0:T(8,128)(2,1)}), bf16[16,256,128]{2,1,0:T(8,128)(2,1)S(1)}, u32[]{:S(2)}, u32[]{:S(2)}) async-start(bf16[16,256,128]{2,1,0:T(8,128)(2,1)} %shard_map.127), calls=%async_computation | async-start | bytes 2097152 | tf_op jit(solution)/shard_map/all_to_all | solution.py:274
  18.9 1.2 reduce-window.6
  20.9 14.1 %all-to-all-done = bf16[16,256,128]{2,1,0:T(8,128)(2,1)S(1)} async-done(((bf16[16,256,128]{2,1,0:T(8,128)(2,1)}), bf16[16,256,128]{2,1,0:T(8,128)(2,1)S(1)}, u32[]{:S(2)}, u32[]{:S(2)}) %all-to-all-start) | async-done | bytes 1048608 | tf_op jit(solution)/shard_map/all_to_all | solution.py:274
  35.7 44.2 %all_to_all.35 = bf16[32,24,256]{2,1,0:T(8,128)(2,1)S(1)} all-to-all(bf16[32,24,256]{2,1,0:T(8,128)(2,1)S(1)} %bitcast.51), channel_id=1, replica_groups=mesh['z'=16,'c'=2,'y'=4,'x'=4] {'z','c'}, dimensions={0} | all-to-all | bytes 786432 | tf_op jit(solution)/shard_map/all_to_all | solution.py:279
  79.9 1.2 broadcast_in_dim.40
  81.2 4.3 %all-to-all-start.2 = ((bf16[4,768,256]{2,1,0:T(8,128)(2,1)}), bf16[4,768,256]{2,1,0:T(8,128)(2,1)}, u32[]{:S(2)}, u32[]{:S(2)}) async-start(bf16[4,768,256]{2,1,0:T(8,128)(2,1)} %broadcast_in_dim.40), calls=%async_computation.2 | async-start | bytes 3145728 | tf_op jit(solution)/shard_map/all_to_all | solution.py:61
  85.5 3.3 %shard_map.128 = (bf16[1024,256]{1,0:T(8,128)(2,1)}, bf16[1024,256]{1,0:T(8,128)(2,1)}, bf16[1024,256]{1,0:T(8,128)(2,1)}, bf16[1024,256]{1,0:T(8,128)(2,1)}) custom-call(s32[40]{0:T(128)} %copy-done.3, bf16[4096,128]{1,0:T(8,128)(2,1)} %bitcast.53, bf16[4096,128]{1,0:T(8,128)(2,1)} %bitcast.54), custom_call_target="tpu_custom_call" | custom-call | flops 4194304 | bytes 4194464 | tf_op jit(solution)/shard_map/pallas_call | solution.py:82
  88.8 3.7 %collective-permute-start.2 = (bf16[1024,256]{1,0:T(8,128)(2,1)}, bf16[1024,256]{1,0:T(8,128)(2,1)S(1)}, u32[]{:S(2)}, u32[]{:S(2)}) collective-permute-start(bf16[1024,256]{1,0:T(8,128)(2,1)} %get-tuple-element.29), channel_id=1, source_target_pairs={{0,1},{1,4},{4,5},{5,0},{2,3},{3,6},{6,7},{7,2},{8,9},{9,12},{12,1... | collective-permute-start | bytes 1572872 | tf_op jit(solution)/shard_map/ppermute | solution.py:68
  92.6 2.8 %collective-permute-start.3 = (bf16[1024,256]{1,0:T(8,128)(2,1)}, bf16[1024,256]{1,0:T(8,128)(2,1)S(1)}, u32[]{:S(2)}, u32[]{:S(2)}) collective-permute-start(bf16[1024,256]{1,0:T(8,128)(2,1)} %get-tuple-element.30), channel_id=1, source_target_pairs={{0,4},{1,5},{4,0},{5,1},{2,6},{3,7},{6,2},{7,3},{8,12},{9,13},{12,... | collective-permute-start | bytes 1572872 | tf_op jit(solution)/shard_map/ppermute | solution.py:68
  95.4 2.7 %collective-permute-start.4 = (bf16[1024,256]{1,0:T(8,128)(2,1)}, bf16[1024,256]{1,0:T(8,128)(2,1)S(1)}, u32[]{:S(2)}, u32[]{:S(2)}) collective-permute-start(bf16[1024,256]{1,0:T(8,128)(2,1)} %get-tuple-element.31), channel_id=1, source_target_pairs={{0,5},{1,0},{4,1},{5,4},{2,7},{3,2},{6,3},{7,6},{8,13},{9,8},{12,9... | collective-permute-start | bytes 1572872 | tf_op jit(solution)/shard_map/ppermute | solution.py:68
  98.1 6.1 %collective-permute-done.2.w1 = bf16[1024,256]{1,0:T(8,128)(2,1)S(1)} collective-permute-done((bf16[1024,256]{1,0:T(8,128)(2,1)}, bf16[1024,256]{1,0:T(8,128)(2,1)S(1)}, u32[]{:S(2)}, u32[]{:S(2)}) %collective-permute-start.2) | collective-permute-done | bytes 524320 | tf_op jit(solution)/shard_map/ppermute | solution.py:68
  104.1 6.7 %collective-permute-done.3.w2 = bf16[1024,256]{1,0:T(8,128)(2,1)S(1)} collective-permute-done((bf16[1024,256]{1,0:T(8,128)(2,1)}, bf16[1024,256]{1,0:T(8,128)(2,1)S(1)}, u32[]{:S(2)}, u32[]{:S(2)}) %collective-permute-start.3) | collective-permute-done | bytes 524320 | tf_op jit(solution)/shard_map/ppermute | solution.py:68
  110.8 1.0 copy-done.1
  112.6 3.9 %shard_map.130 = bf16[4,776,256]{2,1,0:T(8,128)(2,1)S(1)} custom-call(s32[40]{0:T(128)S(1)} %copy-done.4, bf16[4,768,256]{2,1,0:T(8,128)(2,1)} %all-to-all-done.2.got, f32[32,128]{1,0:T(8,128)S(1)} %bitcast.48, bf16[4,1024,256]{2,1,0:T(8,128)(2,1)S(1)} %shard_map.129.first), custom_call_target="tpu_custom_call" | custom-call | flops 1610612736 | bytes 5275808 | tf_op jit(solution)/shard_map/pallas_call | solution.py:82
  116.5 16.0 %all_to_all.36.parts = bf16[4,776,256]{2,1,0:T(8,128)(2,1)S(1)} all-to-all(bf16[4,776,256]{2,1,0:T(8,128)(2,1)S(1)} %shard_map.130), channel_id=1, replica_groups={{0,1,4,5},{2,3,6,7},{8,9,12,13},{10,11,14,15},{21,22,25,26},{23,20,27,2..., dimensions={0} | all-to-all | bytes 3178496 | tf_op jit(solution)/shard_map/all_to_all | solution.py:61
  132.5 1.3 shard_map.131
  133.8 7.9 %all-to-all-start.4 = ((bf16[4,768,128]{2,1,0:T(8,128)(2,1)}), bf16[4,768,128]{2,1,0:T(8,128)(2,1)S(1)}, u32[]{:S(2)}, u32[]{:S(2)}) async-start(bf16[4,768,128]{2,1,0:T(8,128)(2,1)} %shard_map.131), calls=%async_computation.4 | async-start | bytes 1572864 | tf_op jit(solution)/shard_map/all_to_all | solution.py:61
  141.7 2.3 %shard_map.132 = (bf16[512,256]{1,0:T(8,128)(2,1)}, bf16[512,256]{1,0:T(8,128)(2,1)}, bf16[512,256]{1,0:T(8,128)(2,1)}, bf16[512,256]{1,0:T(8,128)(2,1)}) custom-call(s32[40]{0:T(128)} %copy-done.3, bf16[2048,256]{1,0:T(8,128)(2,1)} %bitcast.55), custom_call_target="tpu_custom_call" | custom-call | flops 2097152 | bytes 2097312 | tf_op jit(solution)/shard_map/pallas_call | solution.py:82
  144.0 1.9 collective-permute-start.5
  146.0 1.9 collective-permute-start.6
  147.9 4.3 %collective-permute-start.7 = (bf16[512,256]{1,0:T(8,128)(2,1)}, bf16[512,256]{1,0:T(8,128)(2,1)S(1)}, u32[]{:S(2)}, u32[]{:S(2)}) collective-permute-start(bf16[512,256]{1,0:T(8,128)(2,1)} %get-tuple-element.35), channel_id=1, source_target_pairs={{5,10},{6,5},{9,6},{10,9},{7,8},{4,7},{11,4},{8,11},{13,2},{14,13}... | collective-permute-start | bytes 786440 | tf_op jit(solution)/shard_map/ppermute | solution.py:68
  152.6 2.5 %collective-permute-done.6.w2 = bf16[512,256]{1,0:T(8,128)(2,1)S(1)} collective-permute-done((bf16[512,256]{1,0:T(8,128)(2,1)}, bf16[512,256]{1,0:T(8,128)(2,1)S(1)}, u32[]{:S(2)}, u32[]{:S(2)}) %collective-permute-start.6) | collective-permute-done | bytes 262176 | tf_op jit(solution)/shard_map/ppermute | solution.py:68
  155.1 1.3 collective-permute-done.7.w3
  157.3 1.6 shard_map.133
  158.9 15.3 %all_to_all.37 = bf16[4,768,256]{2,1,0:T(8,128)(2,1)S(1)} all-to-all(bf16[4,768,256]{2,1,0:T(8,128)(2,1)S(1)} %shard_map.133), channel_id=1, replica_groups={{5,6,9,10},{7,4,11,8},{13,14,1,2},{15,12,3,0},{16,17,20,21},{18,19,22,2..., dimensions={0} | all-to-all | bytes 3145728 | tf_op jit(solution)/shard_map/all_to_all | solution.py:61
  174.2 1.1 reduce_sum.25
  175.3 8.7 %all-to-all-start.6 = ((bf16[32,24,256]{2,1,0:T(8,128)(2,1)}), bf16[32,24,256]{2,1,0:T(8,128)(2,1)S(1)}, u32[]{:S(2)}, u32[]{:S(2)}) async-start(bf16[32,24,256]{2,1,0:T(8,128)(2,1)} %bitcast.17), calls=%async_computation.6 | async-start | bytes 786432 | tf_op jit(solution)/shard_map/all_to_all | solution.py:284
  184.4 27.5 %all-to-all-done.6 = bf16[32,24,256]{2,1,0:T(8,128)(2,1)S(1)} async-done(((bf16[32,24,256]{2,1,0:T(8,128)(2,1)}), bf16[32,24,256]{2,1,0:T(8,128)(2,1)S(1)}, u32[]{:S(2)}, u32[]{:S(2)}) %all-to-all-start.6) | async-done | bytes 393248 | tf_op jit(solution)/shard_map/all_to_all | solution.py:284
  (50 shorter events, 7.9 us)
Async XLA Ops:
  0.0 35.0 %copy-start = (bf16[2048,256]{1,0:T(8,128)(2,1)S(1)}, bf16[2048,256]{1,0:T(8,128)(2,1)}, u32[]{:S(2)}) copy-start(bf16[2048,256]{1,0:T(8,128)(2,1)} %param.20) | copy-start | bytes 3145732
  0.0 9.1 %collective-permute-start.1 = (s32[1,256]{1,0:T(1,128)}, s32[1,256]{1,0:T(1,128)S(1)}, u32[]{:S(2)}, u32[]{:S(2)}) collective-permute-start(s32[1,256]{1,0:T(1,128)} %bitcast.62), channel_id=1, source_target_pairs={{0,16},{16,32},{32,48},{48,64},{64,80},{80,96},{96,112},{112,128},... | collective-permute-start | bytes 3080 | tf_op jit(solution)/shard_map/ppermute | solution.py:246
  5.1 5.4 %collective-permute-start = (bf16[256,128]{1,0:T(8,128)(2,1)}, bf16[256,128]{1,0:T(8,128)(2,1)S(1)}, u32[]{:S(2)}, u32[]{:S(2)}) collective-permute-start(bf16[256,128]{1,0:T(8,128)(2,1)} %own.1), channel_id=1, source_target_pairs={{0,16},{16,32},{32,48},{48,64},{64,80},{80,96},{96,112},{112,128},... | collective-permute-start | bytes 196616 | tf_op jit(solution)/shard_map/ppermute | solution.py:245
  8.7 1.8 copy-start.3
  9.1 1.4 copy-start.11
  10.5 0.6 copy-start.8
  13.7 7.0 %copy-start.9 = (s32[256,2]{0,1:T(2,128)S(1)}, s32[256,2]{0,1:T(2,128)}, u32[]{:S(2)}) copy-start(s32[256,2]{0,1:T(2,128)} %param.22) | copy-start | bytes 6148
  13.7 21.3 %copy-start.7 = (bf16[256,256]{1,0:T(8,128)(2,1)S(1)}, bf16[256,256]{1,0:T(8,128)(2,1)}, u32[]{:S(2)}) copy-start(bf16[256,256]{1,0:T(8,128)(2,1)} %param.15) | copy-start | bytes 393220
  13.7 21.3 %all-to-all-start = ((bf16[16,256,128]{2,1,0:T(8,128)(2,1)}), bf16[16,256,128]{2,1,0:T(8,128)(2,1)S(1)}, u32[]{:S(2)}, u32[]{:S(2)}) async-start(bf16[16,256,128]{2,1,0:T(8,128)(2,1)} %shard_map.127), calls=%async_computation | async-start | bytes 2097152 | tf_op jit(solution)/shard_map/all_to_all | solution.py:274
  81.2 31.4 %all-to-all-start.2 = ((bf16[4,768,256]{2,1,0:T(8,128)(2,1)}), bf16[4,768,256]{2,1,0:T(8,128)(2,1)}, u32[]{:S(2)}, u32[]{:S(2)}) async-start(bf16[4,768,256]{2,1,0:T(8,128)(2,1)} %broadcast_in_dim.40), calls=%async_computation.2 | async-start | bytes 3145728 | tf_op jit(solution)/shard_map/all_to_all | solution.py:61
  85.5 25.3 %copy-start.4 = (s32[40]{0:T(128)S(1)}, s32[40]{0:T(128)}, u32[]{:S(2)}) copy-start(s32[40]{0:T(128)} %copy-done.3) | copy-start | bytes 484
  88.8 15.3 %collective-permute-start.2 = (bf16[1024,256]{1,0:T(8,128)(2,1)}, bf16[1024,256]{1,0:T(8,128)(2,1)S(1)}, u32[]{:S(2)}, u32[]{:S(2)}) collective-permute-start(bf16[1024,256]{1,0:T(8,128)(2,1)} %get-tuple-element.29), channel_id=1, source_target_pairs={{0,1},{1,4},{4,5},{5,0},{2,3},{3,6},{6,7},{7,2},{8,9},{9,12},{12,1... | collective-permute-start | bytes 1572872 | tf_op jit(solution)/shard_map/ppermute | solution.py:68
  92.6 18.2 %collective-permute-start.3 = (bf16[1024,256]{1,0:T(8,128)(2,1)}, bf16[1024,256]{1,0:T(8,128)(2,1)S(1)}, u32[]{:S(2)}, u32[]{:S(2)}) collective-permute-start(bf16[1024,256]{1,0:T(8,128)(2,1)} %get-tuple-element.30), channel_id=1, source_target_pairs={{0,4},{1,5},{4,0},{5,1},{2,6},{3,7},{6,2},{7,3},{8,12},{9,13},{12,... | collective-permute-start | bytes 1572872 | tf_op jit(solution)/shard_map/ppermute | solution.py:68
  95.4 15.4 %collective-permute-start.4 = (bf16[1024,256]{1,0:T(8,128)(2,1)}, bf16[1024,256]{1,0:T(8,128)(2,1)S(1)}, u32[]{:S(2)}, u32[]{:S(2)}) collective-permute-start(bf16[1024,256]{1,0:T(8,128)(2,1)} %get-tuple-element.31), channel_id=1, source_target_pairs={{0,5},{1,0},{4,1},{5,4},{2,7},{3,2},{6,3},{7,6},{8,13},{9,8},{12,9... | collective-permute-start | bytes 1572872 | tf_op jit(solution)/shard_map/ppermute | solution.py:68
  110.8 1.0 copy-start.1
  111.8 0.7 copy-start.6
  133.8 22.6 %copy-start.5 = (s32[40]{0:T(128)S(1)}, s32[40]{0:T(128)}, u32[]{:S(2)}) copy-start(s32[40]{0:T(128)} %copy-done.3) | copy-start | bytes 484
  133.8 22.6 %all-to-all-start.4 = ((bf16[4,768,128]{2,1,0:T(8,128)(2,1)}), bf16[4,768,128]{2,1,0:T(8,128)(2,1)S(1)}, u32[]{:S(2)}, u32[]{:S(2)}) async-start(bf16[4,768,128]{2,1,0:T(8,128)(2,1)} %shard_map.131), calls=%async_computation.4 | async-start | bytes 1572864 | tf_op jit(solution)/shard_map/all_to_all | solution.py:61
  144.0 8.5 %collective-permute-start.5 = (bf16[512,256]{1,0:T(8,128)(2,1)}, bf16[512,256]{1,0:T(8,128)(2,1)S(1)}, u32[]{:S(2)}, u32[]{:S(2)}) collective-permute-start(bf16[512,256]{1,0:T(8,128)(2,1)} %get-tuple-element.33), channel_id=1, source_target_pairs={{5,6},{6,9},{9,10},{10,5},{7,4},{4,11},{11,8},{8,7},{13,14},{14,1}... | collective-permute-start | bytes 786440 | tf_op jit(solution)/shard_map/ppermute | solution.py:68
  146.0 9.1 %collective-permute-start.6 = (bf16[512,256]{1,0:T(8,128)(2,1)}, bf16[512,256]{1,0:T(8,128)(2,1)S(1)}, u32[]{:S(2)}, u32[]{:S(2)}) collective-permute-start(bf16[512,256]{1,0:T(8,128)(2,1)} %get-tuple-element.34), channel_id=1, source_target_pairs={{5,9},{6,10},{9,5},{10,6},{7,11},{4,8},{11,7},{8,4},{13,1},{14,2},... | collective-permute-start | bytes 786440 | tf_op jit(solution)/shard_map/ppermute | solution.py:68
  147.9 8.5 %collective-permute-start.7 = (bf16[512,256]{1,0:T(8,128)(2,1)}, bf16[512,256]{1,0:T(8,128)(2,1)S(1)}, u32[]{:S(2)}, u32[]{:S(2)}) collective-permute-start(bf16[512,256]{1,0:T(8,128)(2,1)} %get-tuple-element.35), channel_id=1, source_target_pairs={{5,10},{6,5},{9,6},{10,9},{7,8},{4,7},{11,4},{8,11},{13,2},{14,13}... | collective-permute-start | bytes 786440 | tf_op jit(solution)/shard_map/ppermute | solution.py:68
  156.4 1.0 copy-start.2
  174.2 9.8 %copy-start.10 = (f32[256,2]{0,1:T(2,128)S(1)}, f32[256,2]{0,1:T(2,128)}, u32[]{:S(2)}) copy-start(f32[256,2]{0,1:T(2,128)} %param.23) | copy-start | bytes 6148
  175.3 36.6 %all-to-all-start.6 = ((bf16[32,24,256]{2,1,0:T(8,128)(2,1)}), bf16[32,24,256]{2,1,0:T(8,128)(2,1)S(1)}, u32[]{:S(2)}, u32[]{:S(2)}) async-start(bf16[32,24,256]{2,1,0:T(8,128)(2,1)} %bitcast.17), calls=%async_computation.6 | async-start | bytes 786432 | tf_op jit(solution)/shard_map/all_to_all | solution.py:284

commit v6 on v5

--- a/solution.py
+++ b/solution.py
@@ -59,6 +59,15 @@
 
 def a2a(blocks, groups):
     return lax.all_to_all(blocks, PLANE, 0, 0, tiled=True, axis_index_groups=both_cores(groups))
+
+
+FIRST = 24
+
+
+def exchanged(blocks):
+    size = blocks.shape[0]
+    order = [(FIRST + i) % size for i in range(size)]
+    return lax.all_to_all(blocks, SP, 0, 0, tiled=True, axis_index_groups=[order])
 
 
 def turns(cuts, groups):
@@ -261,7 +270,7 @@
     ids = routes.reshape(-1)
     onehot = (ids[:, None] == jnp.arange(n_exp)[None, :]).astype(jnp.int32)
     rank = jnp.sum(onehot * (jnp.cumsum(onehot, axis=0) - 1), axis=1)
-    place = (ids * cap + rank).reshape(length, TOPK)
+    place = ((ids + (n_exp - FIRST)) % n_exp * cap + rank).reshape(length, TOPK)
     places = jnp.arange(slots)
     take = (place[:, 0][None, :] == places[:, None]) | (place[:, 1][None, :] == places[:, None])
     low = jnp.where(place[:, 0][:, None] == places[None, :], route_weights[:, 0][:, None], 0.0)
@@ -276,12 +285,12 @@
     updated = (residual.astype(F32) + proj).astype(BF16)
 
     send = jnp.dot(lax.optimization_barrier(take.astype(BF16)), updated, preferred_element_type=F32).astype(BF16)
-    arrived = lax.all_to_all(send.reshape(n_exp, cap, cols), SP, 0, 0, tiled=True).reshape(slots, cols)
+    arrived = exchanged(send.reshape(n_exp, cap, cols)).reshape(slots, cols)
     first = turns(cuts_first, SCATTER)
     second = turns(cuts_second, GATHER)
     first = call(pack, [shape(4, 1024, 256)], where, *first, flops=2**22)
     made = experts(arrived, first, second, where, norm_gain.reshape(32, 128))
-    back = lax.all_to_all(made.reshape(n_exp, cap, cols), SP, 0, 0, tiled=True).reshape(slots, cols)
+    back = exchanged(made.reshape(n_exp, cap, cols)).reshape(slots, cols)
     summed = jnp.dot(mix_high, back, preferred_element_type=F32) + jnp.dot(
         mix_low, back, preferred_element_type=F32
     )

time: 214 us -> 211 us (0.986)
  starting transfers between devices: 50.4 us -> 57.3 us
  waiting for transfers between devices: 60.4 us -> 54.6 us
  blocking collectives: 75.6 us -> 71.2 us
    all_to_all x1, starting transfers between devices: 8.75 us -> 15.5 us  [exchanged(): lax.all_to_all(blocks, SP, 0, 0, tiled=True, axis_index_groups=[order])]
    all_to_all x1, waiting for transfers between devices: 27.5 us -> 22.8 us  [exchanged(): lax.all_to_all(blocks, SP, 0, 0, tiled=True, axis_index_groups=[order])]
    all_to_all x1, blocking collectives: 44.2 us -> 40 us  [exchanged(): lax.all_to_all(blocks, SP, 0, 0, tiled=True, axis_index_groups=[order])]
where the time goes in v6:
time: 211 us; the launch traced here: 210 us
  blocking collectives  71.2 us (34%)
  starting transfers between devices  57.3 us (27%)
  waiting for transfers between devices  54.6 us (26%)
  Pallas kernels  15.6 us (7%)
  local copies, waits for them, and re-layouts  6.16 us (3%)
  other arithmetic  2.87 us (1%)
    all_to_all x1, blocking collectives, exchanged(): lax.all_to_all(blocks, SP, 0, 0, tiled=True, axis_index_groups=[order])  40 us
    all_to_all x2, blocking collectives, a2a(): lax.all_to_all(blocks, PLANE, 0, 0, tiled=True, axis_index_groups=both_co...  31.2 us
    all_to_all x1, waiting for transfers between devices, exchanged(): lax.all_to_all(blocks, SP, 0, 0, tiled=True, axis_index_groups=[order])  22.8 us
    ppermute x6, starting transfers between devices, turns(): got.append(lax.ppermute(cuts[by], PLANE, pairs))  17.4 us
    ppermute x6, waiting for transfers between devices, turns(): got.append(lax.ppermute(cuts[by], PLANE, pairs))  16 us
    pallas_call x7, Pallas kernels, call(): pl.pallas_call(kernel, out_shape=outs[0] if single else tuple(outs), in_s...  15.6 us
    all_to_all x1, starting transfers between devices, exchanged(): lax.all_to_all(blocks, SP, 0, 0, tiled=True, axis_index_groups=[order])  15.5 us
    all_to_all x1, waiting for transfers between devices, layer(): pooled_all = lax.all_to_all(pooled, TP, 0, 0, tiled=True)  14.1 us
  transfers between devices with their start and end apart: 12, of which 9 were waited for; matrix products, arithmetic and copies ran while one was open for 2% of the time, Pallas kernels for 3%

profile of v6, /device:TPU:1, one launch (start us, length us, event | category | flops | bytes accessed | tf_op | source)
XLA Modules:
  0.0 209.9 jit_solution(5228374202544486690)
XLA Ops:
  0.0 5.0 %collective-permute-start.1 = (s32[1,256]{1,0:T(1,128)}, s32[1,256]{1,0:T(1,128)S(1)}, u32[]{:S(2)}, u32[]{:S(2)}) collective-permute-start(s32[1,256]{1,0:T(1,128)} %bitcast.62), channel_id=1, source_target_pairs={{0,16},{16,32},{32,48},{48,64},{64,80},{80,96},{96,112},{112,128},... | collective-permute-start | bytes 3080 | tf_op jit(solution)/shard_map/ppermute | solution.py:255
  5.1 1.9 collective-permute-start
  9.1 1.4 collective-permute-done.before
  11.1 2.5 %shard_map.127 = bf16[16,256,128]{2,1,0:T(8,128)(2,1)} custom-call(s32[40]{0:T(128)} %copy-done.3, bf16[256,128]{1,0:T(8,128)(2,1)} %own.1, bf16[256,128]{1,0:T(8,128)(2,1)} %copy-done.8, s32[1,256]{1,0:T(1,128)} %bitcast.63, s32[1,256]{1,0:T(1,128)} %copy-done.11, bf16[1,128,128]{2,1,0:T(8,128)(2,1)} %weight.1, f32[1,128]{1,0:T(1,128)} %bitcast.64), custom_call_target="tpu_custom_call" | custom-call | flops 8388608 | bytes 1215136 | tf_op jit(solution)/shard_map/pallas_call | solution.py:91
  13.7 5.1 %all-to-all-start = ((bf16[16,256,128]{2,1,0:T(8,128)(2,1)}), bf16[16,256,128]{2,1,0:T(8,128)(2,1)S(1)}, u32[]{:S(2)}, u32[]{:S(2)}) async-start(bf16[16,256,128]{2,1,0:T(8,128)(2,1)} %shard_map.127), calls=%async_computation | async-start | bytes 2097152 | tf_op jit(solution)/shard_map/all_to_all | solution.py:283
  18.9 1.2 reduce-window.6
  20.9 14.1 %all-to-all-done = bf16[16,256,128]{2,1,0:T(8,128)(2,1)S(1)} async-done(((bf16[16,256,128]{2,1,0:T(8,128)(2,1)}), bf16[16,256,128]{2,1,0:T(8,128)(2,1)S(1)}, u32[]{:S(2)}, u32[]{:S(2)}) %all-to-all-start) | async-done | bytes 1048608 | tf_op jit(solution)/shard_map/all_to_all | solution.py:283
  35.7 40.0 %all_to_all.35 = bf16[32,24,256]{2,1,0:T(8,128)(2,1)S(1)} all-to-all(bf16[32,24,256]{2,1,0:T(8,128)(2,1)S(1)} %bitcast.51), channel_id=1, replica_groups={{384,400,416,432,448,464,480,496,0,16,32,48,64,80,96,112,128,144,160,17..., dimensions={0} | all-to-all | bytes 786432 | tf_op jit(solution)/shard_map/all_to_all | solution.py:70
  75.7 1.2 broadcast_in_dim.40
  77.0 4.3 %all-to-all-start.2 = ((bf16[4,768,256]{2,1,0:T(8,128)(2,1)}), bf16[4,768,256]{2,1,0:T(8,128)(2,1)}, u32[]{:S(2)}, u32[]{:S(2)}) async-start(bf16[4,768,256]{2,1,0:T(8,128)(2,1)} %broadcast_in_dim.40), calls=%async_computation.2 | async-start | bytes 3145728 | tf_op jit(solution)/shard_map/all_to_all | solution.py:61
  81.3 3.3 %shard_map.128 = (bf16[1024,256]{1,0:T(8,128)(2,1)}, bf16[1024,256]{1,0:T(8,128)(2,1)}, bf16[1024,256]{1,0:T(8,128)(2,1)}, bf16[1024,256]{1,0:T(8,128)(2,1)}) custom-call(s32[40]{0:T(128)} %copy-done.3, bf16[4096,128]{1,0:T(8,128)(2,1)} %bitcast.53, bf16[4096,128]{1,0:T(8,128)(2,1)} %bitcast.54), custom_call_target="tpu_custom_call" | custom-call | flops 4194304 | bytes 4194464 | tf_op jit(solution)/shard_map/pallas_call | solution.py:91
  84.6 3.4 %collective-permute-start.2 = (bf16[1024,256]{1,0:T(8,128)(2,1)}, bf16[1024,256]{1,0:T(8,128)(2,1)S(1)}, u32[]{:S(2)}, u32[]{:S(2)}) collective-permute-start(bf16[1024,256]{1,0:T(8,128)(2,1)} %get-tuple-element.29), channel_id=1, source_target_pairs={{0,1},{1,4},{4,5},{5,0},{2,3},{3,6},{6,7},{7,2},{8,9},{9,12},{12,1... | collective-permute-start | bytes 1572872 | tf_op jit(solution)/shard_map/ppermute | solution.py:77
  88.1 3.1 %collective-permute-start.3 = (bf16[1024,256]{1,0:T(8,128)(2,1)}, bf16[1024,256]{1,0:T(8,128)(2,1)S(1)}, u32[]{:S(2)}, u32[]{:S(2)}) collective-permute-start(bf16[1024,256]{1,0:T(8,128)(2,1)} %get-tuple-element.30), channel_id=1, source_target_pairs={{0,4},{1,5},{4,0},{5,1},{2,6},{3,7},{6,2},{7,3},{8,12},{9,13},{12,... | collective-permute-start | bytes 1572872 | tf_op jit(solution)/shard_map/ppermute | solution.py:77
  91.1 2.8 %collective-permute-start.4 = (bf16[1024,256]{1,0:T(8,128)(2,1)}, bf16[1024,256]{1,0:T(8,128)(2,1)S(1)}, u32[]{:S(2)}, u32[]{:S(2)}) collective-permute-start(bf16[1024,256]{1,0:T(8,128)(2,1)} %get-tuple-element.31), channel_id=1, source_target_pairs={{0,5},{1,0},{4,1},{5,4},{2,7},{3,2},{6,3},{7,6},{8,13},{9,8},{12,9... | collective-permute-start | bytes 1572872 | tf_op jit(solution)/shard_map/ppermute | solution.py:77
  94.0 5.1 %collective-permute-done.2.w1 = bf16[1024,256]{1,0:T(8,128)(2,1)S(1)} collective-permute-done((bf16[1024,256]{1,0:T(8,128)(2,1)}, bf16[1024,256]{1,0:T(8,128)(2,1)S(1)}, u32[]{:S(2)}, u32[]{:S(2)}) %collective-permute-start.2) | collective-permute-done | bytes 524320 | tf_op jit(solution)/shard_map/ppermute | solution.py:77
  99.1 6.4 %collective-permute-done.3.w2 = bf16[1024,256]{1,0:T(8,128)(2,1)S(1)} collective-permute-done((bf16[1024,256]{1,0:T(8,128)(2,1)}, bf16[1024,256]{1,0:T(8,128)(2,1)S(1)}, u32[]{:S(2)}, u32[]{:S(2)}) %collective-permute-start.3) | collective-permute-done | bytes 524320 | tf_op jit(solution)/shard_map/ppermute | solution.py:77
  105.4 1.0 copy-done.1
  107.2 3.9 %shard_map.130 = bf16[4,776,256]{2,1,0:T(8,128)(2,1)S(1)} custom-call(s32[40]{0:T(128)S(1)} %copy-done.4, bf16[4,768,256]{2,1,0:T(8,128)(2,1)} %all-to-all-done.2.got, f32[32,128]{1,0:T(8,128)S(1)} %bitcast.48, bf16[4,1024,256]{2,1,0:T(8,128)(2,1)S(1)} %shard_map.129.first), custom_call_target="tpu_custom_call" | custom-call | flops 1610612736 | bytes 5275808 | tf_op jit(solution)/shard_map/pallas_call | solution.py:91
  111.1 16.2 %all_to_all.36.parts = bf16[4,776,256]{2,1,0:T(8,128)(2,1)S(1)} all-to-all(bf16[4,776,256]{2,1,0:T(8,128)(2,1)S(1)} %shard_map.130), channel_id=1, replica_groups={{0,1,4,5},{2,3,6,7},{8,9,12,13},{10,11,14,15},{21,22,25,26},{23,20,27,2..., dimensions={0} | all-to-all | bytes 3178496 | tf_op jit(solution)/shard_map/all_to_all | solution.py:61
  127.2 1.3 shard_map.131
  128.6 7.9 %all-to-all-start.4 = ((bf16[4,768,128]{2,1,0:T(8,128)(2,1)}), bf16[4,768,128]{2,1,0:T(8,128)(2,1)S(1)}, u32[]{:S(2)}, u32[]{:S(2)}) async-start(bf16[4,768,128]{2,1,0:T(8,128)(2,1)} %shard_map.131), calls=%async_computation.4 | async-start | bytes 1572864 | tf_op jit(solution)/shard_map/all_to_all | solution.py:61
  136.5 2.3 %shard_map.132 = (bf16[512,256]{1,0:T(8,128)(2,1)}, bf16[512,256]{1,0:T(8,128)(2,1)}, bf16[512,256]{1,0:T(8,128)(2,1)}, bf16[512,256]{1,0:T(8,128)(2,1)}) custom-call(s32[40]{0:T(128)} %copy-done.3, bf16[2048,256]{1,0:T(8,128)(2,1)} %bitcast.55), custom_call_target="tpu_custom_call" | custom-call | flops 2097152 | bytes 2097312 | tf_op jit(solution)/shard_map/pallas_call | solution.py:91
  138.8 1.9 collective-permute-start.5
  140.7 1.9 collective-permute-start.6
  142.6 4.3 %collective-permute-start.7 = (bf16[512,256]{1,0:T(8,128)(2,1)}, bf16[512,256]{1,0:T(8,128)(2,1)S(1)}, u32[]{:S(2)}, u32[]{:S(2)}) collective-permute-start(bf16[512,256]{1,0:T(8,128)(2,1)} %get-tuple-element.35), channel_id=1, source_target_pairs={{5,10},{6,5},{9,6},{10,9},{7,8},{4,7},{11,4},{8,11},{13,2},{14,13}... | collective-permute-start | bytes 786440 | tf_op jit(solution)/shard_map/ppermute | solution.py:77
  147.3 2.5 %collective-permute-done.6.w2 = bf16[512,256]{1,0:T(8,128)(2,1)S(1)} collective-permute-done((bf16[512,256]{1,0:T(8,128)(2,1)}, bf16[512,256]{1,0:T(8,128)(2,1)S(1)}, u32[]{:S(2)}, u32[]{:S(2)}) %collective-permute-start.6) | collective-permute-done | bytes 262176 | tf_op jit(solution)/shard_map/ppermute | solution.py:77
  149.8 1.6 collective-permute-done.7.w3
  152.4 1.6 shard_map.133
  154.0 15.0 %all_to_all.37 = bf16[4,768,256]{2,1,0:T(8,128)(2,1)S(1)} all-to-all(bf16[4,768,256]{2,1,0:T(8,128)(2,1)S(1)} %shard_map.133), channel_id=1, replica_groups={{5,6,9,10},{7,4,11,8},{13,14,1,2},{15,12,3,0},{16,17,20,21},{18,19,22,2..., dimensions={0} | all-to-all | bytes 3145728 | tf_op jit(solution)/shard_map/all_to_all | solution.py:61
  169.0 1.1 reduce_sum.25
  170.1 15.5 %all-to-all-start.6 = ((bf16[32,24,256]{2,1,0:T(8,128)(2,1)}), bf16[32,24,256]{2,1,0:T(8,128)(2,1)S(1)}, u32[]{:S(2)}, u32[]{:S(2)}) async-start(bf16[32,24,256]{2,1,0:T(8,128)(2,1)} %bitcast.17), calls=%async_computation.6 | async-start | bytes 786432 | tf_op jit(solution)/shard_map/all_to_all | solution.py:70
  185.9 22.8 %all-to-all-done.6 = bf16[32,24,256]{2,1,0:T(8,128)(2,1)S(1)} async-done(((bf16[32,24,256]{2,1,0:T(8,128)(2,1)}), bf16[32,24,256]{2,1,0:T(8,128)(2,1)S(1)}, u32[]{:S(2)}, u32[]{:S(2)}) %all-to-all-start.6) | async-done | bytes 393248 | tf_op jit(solution)/shard_map/all_to_all | solution.py:70
  (50 shorter events, 7.9 us)
Async XLA Ops:
  0.0 35.0 %copy-start = (bf16[2048,256]{1,0:T(8,128)(2,1)S(1)}, bf16[2048,256]{1,0:T(8,128)(2,1)}, u32[]{:S(2)}) copy-start(bf16[2048,256]{1,0:T(8,128)(2,1)} %param.20) | copy-start | bytes 3145732
  0.0 9.1 %collective-permute-start.1 = (s32[1,256]{1,0:T(1,128)}, s32[1,256]{1,0:T(1,128)S(1)}, u32[]{:S(2)}, u32[]{:S(2)}) collective-permute-start(s32[1,256]{1,0:T(1,128)} %bitcast.62), channel_id=1, source_target_pairs={{0,16},{16,32},{32,48},{48,64},{64,80},{80,96},{96,112},{112,128},... | collective-permute-start | bytes 3080 | tf_op jit(solution)/shard_map/ppermute | solution.py:255
  5.1 5.4 %collective-permute-start = (bf16[256,128]{1,0:T(8,128)(2,1)}, bf16[256,128]{1,0:T(8,128)(2,1)S(1)}, u32[]{:S(2)}, u32[]{:S(2)}) collective-permute-start(bf16[256,128]{1,0:T(8,128)(2,1)} %own.1), channel_id=1, source_target_pairs={{0,16},{16,32},{32,48},{48,64},{64,80},{80,96},{96,112},{112,128},... | collective-permute-start | bytes 196616 | tf_op jit(solution)/shard_map/ppermute | solution.py:254
  8.7 1.8 copy-start.3
  9.1 1.4 copy-start.11
  10.5 0.6 copy-start.8
  13.7 7.0 %copy-start.9 = (s32[256,2]{0,1:T(2,128)S(1)}, s32[256,2]{0,1:T(2,128)}, u32[]{:S(2)}) copy-start(s32[256,2]{0,1:T(2,128)} %param.22) | copy-start | bytes 6148
  13.7 21.3 %copy-start.7 = (bf16[256,256]{1,0:T(8,128)(2,1)S(1)}, bf16[256,256]{1,0:T(8,128)(2,1)}, u32[]{:S(2)}) copy-start(bf16[256,256]{1,0:T(8,128)(2,1)} %param.15) | copy-start | bytes 393220
  13.7 21.3 %all-to-all-start = ((bf16[16,256,128]{2,1,0:T(8,128)(2,1)}), bf16[16,256,128]{2,1,0:T(8,128)(2,1)S(1)}, u32[]{:S(2)}, u32[]{:S(2)}) async-start(bf16[16,256,128]{2,1,0:T(8,128)(2,1)} %shard_map.127), calls=%async_computation | async-start | bytes 2097152 | tf_op jit(solution)/shard_map/all_to_all | solution.py:283
  77.0 30.2 %all-to-all-start.2 = ((bf16[4,768,256]{2,1,0:T(8,128)(2,1)}), bf16[4,768,256]{2,1,0:T(8,128)(2,1)}, u32[]{:S(2)}, u32[]{:S(2)}) async-start(bf16[4,768,256]{2,1,0:T(8,128)(2,1)} %broadcast_in_dim.40), calls=%async_computation.2 | async-start | bytes 3145728 | tf_op jit(solution)/shard_map/all_to_all | solution.py:61
  81.3 24.1 %copy-start.4 = (s32[40]{0:T(128)S(1)}, s32[40]{0:T(128)}, u32[]{:S(2)}) copy-start(s32[40]{0:T(128)} %copy-done.3) | copy-start | bytes 484
  84.6 14.4 %collective-permute-start.2 = (bf16[1024,256]{1,0:T(8,128)(2,1)}, bf16[1024,256]{1,0:T(8,128)(2,1)S(1)}, u32[]{:S(2)}, u32[]{:S(2)}) collective-permute-start(bf16[1024,256]{1,0:T(8,128)(2,1)} %get-tuple-element.29), channel_id=1, source_target_pairs={{0,1},{1,4},{4,5},{5,0},{2,3},{3,6},{6,7},{7,2},{8,9},{9,12},{12,1... | collective-permute-start | bytes 1572872 | tf_op jit(solution)/shard_map/ppermute | solution.py:77
  88.1 17.3 %collective-permute-start.3 = (bf16[1024,256]{1,0:T(8,128)(2,1)}, bf16[1024,256]{1,0:T(8,128)(2,1)S(1)}, u32[]{:S(2)}, u32[]{:S(2)}) collective-permute-start(bf16[1024,256]{1,0:T(8,128)(2,1)} %get-tuple-element.30), channel_id=1, source_target_pairs={{0,4},{1,5},{4,0},{5,1},{2,6},{3,7},{6,2},{7,3},{8,12},{9,13},{12,... | collective-permute-start | bytes 1572872 | tf_op jit(solution)/shard_map/ppermute | solution.py:77
  91.1 14.3 %collective-permute-start.4 = (bf16[1024,256]{1,0:T(8,128)(2,1)}, bf16[1024,256]{1,0:T(8,128)(2,1)S(1)}, u32[]{:S(2)}, u32[]{:S(2)}) collective-permute-start(bf16[1024,256]{1,0:T(8,128)(2,1)} %get-tuple-element.31), channel_id=1, source_target_pairs={{0,5},{1,0},{4,1},{5,4},{2,7},{3,2},{6,3},{7,6},{8,13},{9,8},{12,9... | collective-permute-start | bytes 1572872 | tf_op jit(solution)/shard_map/ppermute | solution.py:77
  105.4 1.0 copy-start.1
  106.5 0.7 copy-start.6
  128.6 22.9 %copy-start.5 = (s32[40]{0:T(128)S(1)}, s32[40]{0:T(128)}, u32[]{:S(2)}) copy-start(s32[40]{0:T(128)} %copy-done.3) | copy-start | bytes 484
  128.6 22.9 %all-to-all-start.4 = ((bf16[4,768,128]{2,1,0:T(8,128)(2,1)}), bf16[4,768,128]{2,1,0:T(8,128)(2,1)S(1)}, u32[]{:S(2)}, u32[]{:S(2)}) async-start(bf16[4,768,128]{2,1,0:T(8,128)(2,1)} %shard_map.131), calls=%async_computation.4 | async-start | bytes 1572864 | tf_op jit(solution)/shard_map/all_to_all | solution.py:61
  138.8 8.5 %collective-permute-start.5 = (bf16[512,256]{1,0:T(8,128)(2,1)}, bf16[512,256]{1,0:T(8,128)(2,1)S(1)}, u32[]{:S(2)}, u32[]{:S(2)}) collective-permute-start(bf16[512,256]{1,0:T(8,128)(2,1)} %get-tuple-element.33), channel_id=1, source_target_pairs={{5,6},{6,9},{9,10},{10,5},{7,4},{4,11},{11,8},{8,7},{13,14},{14,1}... | collective-permute-start | bytes 786440 | tf_op jit(solution)/shard_map/ppermute | solution.py:77
  140.7 9.1 %collective-permute-start.6 = (bf16[512,256]{1,0:T(8,128)(2,1)}, bf16[512,256]{1,0:T(8,128)(2,1)S(1)}, u32[]{:S(2)}, u32[]{:S(2)}) collective-permute-start(bf16[512,256]{1,0:T(8,128)(2,1)} %get-tuple-element.34), channel_id=1, source_target_pairs={{5,9},{6,10},{9,5},{10,6},{7,11},{4,8},{11,7},{8,4},{13,1},{14,2},... | collective-permute-start | bytes 786440 | tf_op jit(solution)/shard_map/ppermute | solution.py:77
  142.6 8.8 %collective-permute-start.7 = (bf16[512,256]{1,0:T(8,128)(2,1)}, bf16[512,256]{1,0:T(8,128)(2,1)S(1)}, u32[]{:S(2)}, u32[]{:S(2)}) collective-permute-start(bf16[512,256]{1,0:T(8,128)(2,1)} %get-tuple-element.35), channel_id=1, source_target_pairs={{5,10},{6,5},{9,6},{10,9},{7,8},{4,7},{11,4},{8,11},{13,2},{14,13}... | collective-permute-start | bytes 786440 | tf_op jit(solution)/shard_map/ppermute | solution.py:77
  151.4 1.0 copy-start.2
  169.0 16.6 %copy-start.10 = (f32[256,2]{0,1:T(2,128)S(1)}, f32[256,2]{0,1:T(2,128)}, u32[]{:S(2)}) copy-start(f32[256,2]{0,1:T(2,128)} %param.23) | copy-start | bytes 6148
  170.1 38.6 %all-to-all-start.6 = ((bf16[32,24,256]{2,1,0:T(8,128)(2,1)}), bf16[32,24,256]{2,1,0:T(8,128)(2,1)S(1)}, u32[]{:S(2)}, u32[]{:S(2)}) async-start(bf16[32,24,256]{2,1,0:T(8,128)(2,1)} %bitcast.17), calls=%async_computation.6 | async-start | bytes 786432 | tf_op jit(solution)/shard_map/all_to_all | solution.py:70
